TPU v7x, 512 devices: a 8x2x16 block of a 8x8x16 slice. The times are simulated.
512 devices in a mesh: grp: 2 (over y), sp: 32 (over z, core), tp: 8 (over x).
Axes of the slice: x: 8, y: 2, z: 16, core: 2. Of those that a mesh axis runs over, the one named last changes fastest.
The devices are a block of a 8x8x16 slice.
Arguments:
- query_a: bfloat16 [16384, 2048], P(('grp', 'sp'), 'tp'), parts along dimension 0, may hold values from -6 to 6
- key_a: bfloat16 [16384, 2048], P(('grp', 'sp'), 'tp'), parts along dimension 0, may hold values from -6 to 6
- value_a: bfloat16 [16384, 4096], P(('grp', 'sp'), 'tp'), parts along dimension 0, may hold values from -6 to 6
- decay_a: float32 [2, 8, 16384], P(None, 'tp', ('grp', 'sp')), parts along dimension 2, may hold values from -1 to 0
- query_b: bfloat16 [16384, 1024], P(('grp', 'sp'), 'tp'), parts along dimension 0, may hold values from -6 to 6
- key_b: bfloat16 [16384, 1024], P(('grp', 'sp'), 'tp'), parts along dimension 0, may hold values from -6 to 6
- value_b: bfloat16 [16384, 1024], P(('grp', 'sp'), 'tp'), parts along dimension 0, may hold values from -6 to 6
- decay_b: float32 [2, 16, 16384], P(None, 'tp', ('grp', 'sp')), parts along dimension 2, may hold values from -1 to 0
- out_weight_a: bfloat16 [4096, 2048], P('tp'), may hold values from -0.078125 to 0.078125
- out_weight_b: bfloat16 [1024, 2048], P('tp'), may hold values from -0.078125 to 0.078125
- residual: bfloat16 [16384, 2048], P(('grp', 'sp', 'tp')), parts along dimension 0, may hold values from -6 to 6
- norm_gain: float32 [2, 2048], replicated, may hold values from 0.1 to 1.9
- route_group: int32 [16384], P(('grp', 'sp', 'tp')), parts along dimension 0, may hold values from 0 to 3
- route_expert: int32 [16384, 2], P(('grp', 'sp', 'tp')), parts along dimension 0, may hold values from 0 to 7, as said below
- route_weight: float32 [16384, 2], P(('grp', 'sp', 'tp')), parts along dimension 0, may hold values from 0.2 to 1
- expert_gate: bfloat16 [32, 2048, 1024], P('sp', None, 'tp'), may hold values from -0.125 to 0.125
- expert_up: bfloat16 [32, 2048, 1024], P('sp', None, 'tp'), may hold values from -0.125 to 0.125
- expert_down: bfloat16 [32, 1024, 2048], P('sp', 'tp'), may hold values from -0.1875 to 0.1875
Outputs:
- layer_out: bfloat16 [16384, 2048], P(('grp', 'sp', 'tp')), parts along dimension 0
There are 2 independent parts, one for each index of `grp`. A program takes and returns all parts, laid end to end along the dimension named above; an argument that names none is the same for every part. Nothing has to cross between parts.
Inputs may be any that keep to these rules, and one draw needn't show every extreme that they name: `route_expert`: the 2 entries of a row are different.
All inputs are finite; a program needn't handle non-finite values.
Results may differ from a plain program's by a relative error of at most 0.015.
Values may be sent and summed in bfloat16 or wider, within the bound.
No kernel may reach another device: no remote copies, remote signals or barrier semaphores. Data moves between devices by JAX's collectives and lax.ppermute only.
A program may use at most 128 MiB of HBM per device.

v0:
```python
import math

import jax
import jax.numpy as jnp
from jax import lax
from jax.sharding import Mesh
from jax.sharding import PartitionSpec as P

BLOCK = 128
EXPERTS = 32
TOP = 2
CAP = 2
EXP_GROUP = 8
SP = ("sp_0", "sp_1")
GRP_SP = ("grp", "sp_0", "sp_1")
GRP_SP_TP = ("grp", "sp_0", "sp_1", "tp")


RESIDUAL_SCALE = math.sqrt(2.0)
NORM_EPS = 1e-05
GROUP_EPS = 1e-06
ROPE_BASE = 10000.0


def filled_with(array, identity):
    return jax.tree.map(
        lambda a, e: jnp.broadcast_to(jnp.asarray(e, a.dtype), a.shape), array, identity
    )


def prefix_by_axis(array, axes, combine, identity):
    before = start = filled_with(array, identity)
    subtotal = array
    for axis in reversed(axes):
        size, index = (lax.axis_size(axis), lax.axis_index(axis))
        pieces = jax.tree.map(
            lambda part, kind: lax.all_gather(part.astype(kind), axis),
            subtotal,
            jax.tree.map(lambda a: jnp.bfloat16 if a.dtype == jnp.float32 else a.dtype, array),
        )
        inside, subtotal = (start, start)
        for k in range(size):
            passed = k < index
            subtotal = combine(
                subtotal, jax.tree.map(lambda part, own: part[k].astype(own.dtype), pieces, array)
            )
            inside = jax.tree.map(lambda new, old: jnp.where(passed, new, old), subtotal, inside)
        before = combine(inside, before)
    return before


def gathered_once(array, axis):
    leaves = jax.tree.leaves(array)
    order = sorted(range(len(leaves)), key=lambda k: -leaves[k].size)
    width = (1, *leaves[order[0]].shape)[-1]
    lines = [
        jnp.pad(leaves[k].reshape(-1), (0, -leaves[k].size % width)).reshape(-1, width)
        for k in order
    ]
    both, at, found = (lax.all_gather(jnp.concatenate(lines), axis), 0, {})
    for k, line in zip(order, lines):
        slab = both[:, at : at + len(line)].reshape(len(both), -1)
        found[k] = slab[:, : leaves[k].size].reshape(-1, *leaves[k].shape)
        at += len(line)
    numbers = iter(range(len(leaves)))
    return jax.tree.map(lambda _: found[next(numbers)], array)


def prefix_by_axis_2(array, axes, combine, identity):
    before = start = filled_with(array, identity)
    subtotal = array
    for axis in reversed(axes):
        size, index = (lax.axis_size(axis), lax.axis_index(axis))
        pieces = gathered_once(
            jax.tree.map(
                lambda part, kind: part.astype(kind),
                subtotal,
                jax.tree.map(lambda a: jnp.bfloat16 if a.dtype == jnp.float32 else a.dtype, array),
            ),
            axis,
        )
        inside, subtotal = (start, start)
        for k in reversed(range(size)):
            passed = k > index
            subtotal = combine(
                subtotal, jax.tree.map(lambda part, own: part[k].astype(own.dtype), pieces, array)
            )
            inside = jax.tree.map(lambda new, old: jnp.where(passed, new, old), subtotal, inside)
        before = combine(inside, before)
    return before


def cut_along(array, dim, size):
    before, after = (array.shape[:dim], array.shape[dim + 1 :])
    return jnp.moveaxis(array.reshape(*before, size, -1, *after), dim, 0)


def summed_on_arrival(array, axis, dim):
    blocks = cut_along(array, dim, lax.axis_size(axis))
    arrived = lax.all_to_all(blocks, axis, split_axis=0, concat_axis=0, tiled=True)
    return arrived.astype(jnp.float32).sum(axis=0)


def sent_to_all(array, axis):
    copies = jnp.broadcast_to(array, (lax.axis_size(axis), *array.shape))
    return lax.all_to_all(copies, axis, split_axis=0, concat_axis=0, tiled=True)


def in_order(blocks, dim):
    shape = list(blocks.shape[1:])
    shape[dim] *= blocks.shape[0]
    return jnp.moveaxis(blocks, 0, dim).reshape(shape)


def collect(array, axis, dim):
    blocks = sent_to_all(array, axis)
    return in_order(blocks, dim)


def rotate(vectors, token_positions):
    half_width = vectors.shape[-1] // 2
    frequencies = ROPE_BASE ** (-jnp.arange(half_width, dtype=jnp.float32) / half_width)
    angles = token_positions.astype(jnp.float32)[:, None] * frequencies[None, :]
    cosine = jnp.cos(angles)[:, None, :]
    sine_part = jnp.sin(angles)[:, None, :]
    first_half = vectors[..., :half_width].astype(jnp.float32)
    second = vectors[..., half_width:].astype(jnp.float32)
    return jnp.concatenate(
        [first_half * cosine - second * sine_part, first_half * sine_part + second * cosine],
        axis=-1,
    )


def prepare(query_w, key_w, value_w, number_of_heads, token_positions):
    length = query_w.shape[0]
    queries_f = rotate(query_w.reshape(length, number_of_heads, -1), token_positions)
    key_dim = queries_f.shape[-1]
    queries = queries_f.astype(jnp.bfloat16)
    keys_rot = (
        rotate(key_w.reshape(length, number_of_heads, -1), token_positions)
        * (1.0 / math.sqrt(key_dim))
    ).astype(jnp.bfloat16)
    values = value_w.reshape(length, number_of_heads, -1)
    return (queries, keys_rot, values)


def sweep_blocks(queries, keys_rot, values, log_decay, strict, state_init, span_size):
    length, number_of_heads, key_dim = queries.shape
    value_dim = values.shape[-1]
    block_count = length // span_size

    def split_blocks(array):
        return array.reshape(block_count, span_size, number_of_heads, array.shape[-1])

    decay_blocks = log_decay.reshape(number_of_heads, block_count, span_size).transpose(1, 0, 2)
    position_index = jnp.arange(span_size)
    if strict:
        allowed = position_index[:, None] > position_index[None, :]
    else:
        allowed = position_index[:, None] >= position_index[None, :]

    def advance(state_now, inputs):
        query_blk, key_blk, value_blk, decay_blk = inputs
        cumulative = jnp.cumsum(decay_blk, axis=1)
        log_gap = cumulative[:, :, None] - cumulative[:, None, :]
        weights = jnp.where(allowed[None], jnp.exp(jnp.where(allowed[None], log_gap, 0.0)), 0.0)
        scores = (
            jnp.einsum("ihd,jhd->hij", query_blk, key_blk, preferred_element_type=jnp.float32)
            * weights
        )
        weighted = scores.astype(jnp.bfloat16)
        inner_part = jnp.einsum(
            "hij,jhv->ihv", weighted, value_blk, preferred_element_type=jnp.float32
        )
        carried = (
            jnp.einsum("ihd,hdv->ihv", query_blk.astype(jnp.float32), state_now)
            * jnp.exp(cumulative).T[:, :, None]
        )
        key_scaled = (
            key_blk.astype(jnp.float32) * jnp.exp(cumulative[:, -1:] - cumulative).T[:, :, None]
        )
        state_next = state_now * jnp.exp(cumulative[:, -1])[:, None, None] + jnp.einsum(
            "jhd,jhv->hdv", key_scaled, value_blk.astype(jnp.float32)
        )
        return (state_next, inner_part + carried)

    final_state, outputs = lax.scan(
        advance,
        state_init,
        (split_blocks(queries), split_blocks(keys_rot), split_blocks(values), decay_blocks),
    )
    return (outputs.reshape(length, number_of_heads, value_dim), final_state)


def summary(keys_rot, values, log_decay):
    cumulative = jnp.cumsum(log_decay, axis=1)
    key_scaled = (
        keys_rot.astype(jnp.float32) * jnp.exp(cumulative[:, -1:] - cumulative).T[:, :, None]
    )
    return (
        jnp.exp(cumulative[:, -1]),
        jnp.einsum("lhd,lhv->hdv", key_scaled, values.astype(jnp.float32)),
    )


def chain_states(earlier, later):
    decay_a0, state_a0, decay_b0, state_b0 = earlier
    decay_a1, state_a1, decay_b1, state_b1 = later
    return (
        decay_a0 * decay_a1,
        state_a0 * decay_a1[:, None, None] + state_a1,
        decay_b0 * decay_b1,
        state_b0 * decay_b1[:, None, None] + state_b1,
    )


def neutral(parts):
    return (
        jnp.ones_like(parts[0]),
        jnp.zeros_like(parts[1]),
        jnp.ones_like(parts[2]),
        jnp.zeros_like(parts[3]),
    )


def carry_states(forward_parts, backward_parts):
    into_forward = prefix_by_axis(forward_parts, SP, chain_states, neutral(forward_parts))
    into_backward = prefix_by_axis_2(backward_parts, SP, chain_states, neutral(backward_parts))
    return (into_forward, into_backward)


def finish(forward, backward_flipped):
    total_sum = forward + backward_flipped[::-1]
    normed = total_sum * lax.rsqrt(
        jnp.mean(total_sum * total_sum, axis=-1, keepdims=True) + GROUP_EPS
    )
    return normed.reshape(total_sum.shape[0], -1).astype(jnp.bfloat16)


def layer_norm(stream, gain):
    center = stream - jnp.mean(stream, axis=-1, keepdims=True)
    spread = jnp.mean(center * center, axis=-1, keepdims=True)
    return center * lax.rsqrt(spread + NORM_EPS) * gain


def slot_table(expert_ids):
    onehot = (expert_ids[..., None] == jnp.arange(EXPERTS, dtype=jnp.int32)).astype(jnp.int32)
    earlier = jnp.cumsum(onehot, axis=-2) - onehot
    rank_order = jnp.sum(earlier * onehot, axis=-1)
    kept_mask = rank_order < CAP
    slot_index = expert_ids * CAP + jnp.minimum(rank_order, CAP - 1)
    return (slot_index, kept_mask)


def gate_up(rows, gate_w, up_w):
    gate_part = jnp.einsum("xecd,edf->xecf", rows, gate_w, preferred_element_type=jnp.float32)
    up_part = jnp.einsum("xecd,edf->xecf", rows, up_w, preferred_element_type=jnp.float32)
    return (jax.nn.silu(gate_part) * up_part).astype(jnp.bfloat16)


def shards(
    query_a,
    key_a,
    value_a,
    decay_a,
    query_b,
    key_b,
    value_b,
    decay_b,
    out_weight_a,
    out_weight_b,
    residual,
    norm_gain,
    route_group,
    route_expert,
    route_weight,
    expert_gate,
    expert_up,
    expert_down,
):
    length = query_a.shape[0]
    token_positions = lax.axis_index(SP) * length + jnp.arange(length, dtype=jnp.int32)
    heads_a = decay_a.shape[1]
    heads_b = decay_b.shape[1]
    qa_rot, ka_rot, va_all = prepare(query_a, key_a, value_a, heads_a, token_positions)
    qb_rot, kb_rot, vb_all = prepare(query_b, key_b, value_b, heads_b, token_positions)
    flip_a = (qa_rot[::-1], ka_rot[::-1], va_all[::-1], decay_a[1][:, ::-1])
    flip_b = (qb_rot[::-1], kb_rot[::-1], vb_all[::-1], decay_b[1][:, ::-1])
    forward_parts = summary(ka_rot, va_all, decay_a[0]) + summary(kb_rot, vb_all, decay_b[0])
    backward_parts = summary(flip_a[1], flip_a[2], flip_a[3]) + summary(
        flip_b[1], flip_b[2], flip_b[3]
    )
    into_forward, into_backward = carry_states(forward_parts, backward_parts)
    forward_a = sweep_blocks(qa_rot, ka_rot, va_all, decay_a[0], False, into_forward[1], BLOCK)[0]
    forward_b = sweep_blocks(qb_rot, kb_rot, vb_all, decay_b[0], False, into_forward[3], BLOCK)[0]
    backward_a = sweep_blocks(
        flip_a[0], flip_a[1], flip_a[2], flip_a[3], True, into_backward[1], BLOCK
    )[0]
    backward_b = sweep_blocks(
        flip_b[0], flip_b[1], flip_b[2], flip_b[3], True, into_backward[3], BLOCK
    )[0]
    mixed_a = finish(forward_a, backward_a)
    mixed_b = finish(forward_b, backward_b)
    rows_dev = length // lax.axis_size("tp")
    mix = summed_on_arrival(
        (
            jnp.dot(mixed_a, out_weight_a, preferred_element_type=jnp.float32)
            + jnp.dot(mixed_b, out_weight_b, preferred_element_type=jnp.float32)
        ).astype(jnp.bfloat16),
        "tp",
        0,
    )
    hidden_in = layer_norm(
        RESIDUAL_SCALE * residual.astype(jnp.float32) + mix, norm_gain[0]
    ).astype(jnp.bfloat16)
    width = hidden_in.shape[1]
    ffn_width = expert_gate.shape[2]
    sp_count = lax.axis_size(SP)
    per_device = EXPERTS // sp_count
    slots = EXPERTS * CAP
    global_ids = (route_group[:, None] * EXP_GROUP + route_expert).reshape(-1)
    slot_index, kept_mask = slot_table(global_ids)
    hits = (slot_index[:, None] == jnp.arange(slots, dtype=jnp.int32)[None, :]) & kept_mask[:, None]
    choose = jnp.sum(hits.reshape(rows_dev, TOP, slots).astype(jnp.int32), axis=1).astype(
        jnp.bfloat16
    )
    outgoing = jnp.einsum(
        "rs,rd->sd", choose, hidden_in, preferred_element_type=jnp.float32
    ).astype(jnp.bfloat16)
    outgoing = outgoing.reshape(sp_count, per_device * CAP, width)
    received = lax.all_to_all(outgoing, SP, split_axis=0, concat_axis=0, tiled=True)
    piece_rows = collect(received, "tp", 0)
    piece_count = piece_rows.shape[0]
    shaped = piece_rows.reshape(-1, per_device, CAP, width)
    hidden = gate_up(shaped, expert_gate, expert_up).reshape(
        piece_count, per_device * CAP, ffn_width
    )
    flat_hidden = hidden.reshape(-1, ffn_width)
    piece_rows = flat_hidden.reshape(-1, per_device, CAP, ffn_width)
    summed = summed_on_arrival(
        jnp.einsum("xecf,efd->xecd", piece_rows, expert_down, preferred_element_type=jnp.float32)
        .reshape(sp_count * per_device * CAP * lax.axis_size("tp"), width)
        .astype(jnp.bfloat16),
        "tp",
        0,
    )
    back_rows = summed.astype(jnp.bfloat16).reshape(sp_count, per_device * CAP, width)
    returned = lax.all_to_all(back_rows, SP, split_axis=0, concat_axis=0, tiled=True).reshape(
        slots, width
    )
    picked = (
        jnp.take(returned, slot_index, axis=0).astype(jnp.float32).reshape(rows_dev, TOP, width)
    )
    factor = jnp.where(kept_mask.reshape(rows_dev, TOP), route_weight, 0.0)
    ffn = jnp.sum(picked * factor[..., None], axis=1)
    return layer_norm(RESIDUAL_SCALE * hidden_in.astype(jnp.float32) + ffn, norm_gain[1]).astype(
        jnp.bfloat16
    )


def solution(mesh):
    finer = Mesh(
        mesh.devices.reshape(mesh.shape["grp"], 16, 2, mesh.shape["tp"]),
        ("grp", "sp_0", "sp_1", "tp"),
    )
    in_specs = (
        P(GRP_SP, "tp"),
        P(GRP_SP, "tp"),
        P(GRP_SP, "tp"),
        P(None, "tp", GRP_SP),
        P(GRP_SP, "tp"),
        P(GRP_SP, "tp"),
        P(GRP_SP, "tp"),
        P(None, "tp", GRP_SP),
        P("tp", None),
        P("tp", None),
        P(GRP_SP_TP, None),
        P(),
        P(GRP_SP_TP),
        P(GRP_SP_TP, None),
        P(GRP_SP_TP, None),
        P(SP, None, "tp"),
        P(SP, None, "tp"),
        P(SP, "tp", None),
    )
    out_specs = P(GRP_SP_TP, None)
    return jax.shard_map(
        shards, mesh=finer, in_specs=in_specs, out_specs=out_specs, check_vma=False
    )
```

profile of v0, /device:TPU:65, one launch (start us, length us, event | category | flops | bytes accessed | tf_op | source)
XLA Modules:
  0.0 532.6 jit_solution(7885453655435722723)
XLA Ops:
  6.6 1.4 slice_bitcast_fusion.62
  16.8 43.6 %all-reduce.7 = (bf16[2]{0:T(256)(128)(2,1)S(1)}, bf16[4]{0:T(256)(128)(2,1)S(1)}) all-reduce(bf16[2]{0:T(256)(128)(2,1)S(1)} %dynamic-update-slice, bf16[4]{0:T(256)(128)(2,1)S(1)} %dynamic-update-slice.2), channel_id=1, replica_groups=mesh['grp'=2,'sp_0'=16,'sp_1'=2,'tp'=8] {'sp_1'}, use_global_device_ids=true, to_apply=%add.4 | all-reduce | flops 6 | bytes 24
  61.1 2.2 fusion.214
  63.3 1.4 convolution_convert_fusion.3
  64.7 2.2 all-gather.1
  67.7 1.5 fusion.188
  69.4 3.2 reverse.3
  80.4 2.3 all-gather.6
  89.0 1.4 dynamic-update-slice.1
  90.5 22.6 %all-gather.8 = bf16[16,1,2]{2,1,0:T(2,128)(2,1)S(1)} all-gather(bf16[1,1,2]{2,1,0:T(2,128)(2,1)S(1)} %get-tuple-element.632), channel_id=1, replica_groups=mesh['grp'=2,'sp_0'=16,'sp_1'=2,'tp'=8] {'sp_0'}, dimensions={0}, use_global_device_ids=true | all-gather | bytes 68 | tf_op jit(solution)/shard_map/all_gather | solution.py:37
  113.1 23.8 %all-reduce.5 = bf16[16]{0:T(256)(128)(2,1)S(1)} all-reduce(bf16[16]{0:T(256)(128)(2,1)S(1)} %dynamic-update-slice.1), channel_id=2, replica_groups=mesh['grp'=2,'sp_0'=16,'sp_1'=2,'tp'=8] {'sp_0'}, use_global_device_ids=true, to_apply=%add.5 | all-reduce | flops 16 | bytes 64
  150.1 1.4 concatenate.108
  156.9 1.3 rev.33
  162.1 10.7 %all-gather.5 = bf16[4,64,64]{2,1,0:T(8,128)(2,1)S(1)} all-gather(bf16[2,64,64]{2,1,0:T(8,128)(2,1)S(1)} %convolution_convert_fusion.4), channel_id=7, replica_groups=mesh['grp'=2,'sp_0'=16,'sp_1'=2,'tp'=8] {'sp_1'}, dimensions={0}, use_global_device_ids=true | all-gather | bytes 49152 | tf_op jit(solution)/shard_map/all_gather | solution.py:37
  172.9 30.5 %all_gather.64 = bf16[16,2,64,64]{3,2,1,0:T(8,128)(2,1)S(1)} all-gather(bf16[1,2,64,64]{3,2,1,0:T(8,128)(2,1)S(1)} %fusion.243), channel_id=1, replica_groups=mesh['grp'=2,'sp_0'=16,'sp_1'=2,'tp'=8] {'sp_0'}, dimensions={0}, use_global_device_ids=true | all-gather | bytes 278528 | tf_op jit(solution)/shard_map/all_gather | solution.py:37
  204.4 16.3 %while.58 = (s32[]{:T(128)}, f32[2,64,64]{2,1,0:T(8,128)S(1)}, f32[2,128,2,64]{1,0,3,2:T(2,128)}, f32[2,2,128]{2,1,0:T(2,128)}, bf16[2,128,2,64]{1,3,2,0:T(8,128...) while((s32[]{:T(128)}, f32[2,64,64]{2,1,0:T(8,128)S(1)}, ...), condition=%wide.region_17.18_spmd.clone.clone, body=%wide.region_15.17_spmd.clone.clone.sunk | while | flops 12877826 | bytes 673985 | solution.py:187
  209.9 2.7 dynamic_update_slice.30
  218.0 2.7 dynamic_update_slice.30
  220.7 1.7 reshape.2281
  223.7 1.5 maximum_bitcast_fusion.2
  225.2 1.5 copy_bitcast_fusion
  226.6 1.6 copy_bitcast_fusion.1
  228.2 4.1 fusion.169
  233.2 14.0 %while.56 = (s32[]{:T(128)}, f32[1,256,512]{2,1,0:T(8,128)S(1)}, f32[2,128,1,512]{3,1,0,2:T(8,128)}, f32[2,1,128]{2,1,0:T(1,128)S(1)}, bf16[2,128,1,256]{3,1,2,0...) while((s32[]{:T(128)}, f32[1,256,512]{2,1,0:T(8,128)S(1)}, ...), condition=%wide.region_4.5_spmd.clone.clone, body=%wide.region_2.4_spmd.clone.clone.sunk | while | flops 92848128 | bytes 3941001 | solution.py:187
  259.9 1.6 slice_convert_fusion.15
  263.0 1.5 reshape.2408
  264.5 1.4 reshape.2406
  265.9 1.5 reshape.2404
  267.4 1.4 reshape.2402
  271.7 5.4 %while.59 = (s32[]{:T(128)}, f32[2,64,64]{2,1,0:T(8,128)S(1)}, f32[2,128,2,64]{1,0,3,2:T(2,128)S(1)}, f32[2,2,128]{2,1,0:T(2,128)S(1)}, bf16[2,128,2,64]{1,3,2,0...) while((s32[]{:T(128)}, f32[2,64,64]{2,1,0:T(8,128)S(1)}, ...), condition=%wide.region_20.21_spmd.clone.clone, body=%wide.region_18.20_spmd.clone.clone.sunk | while | flops 12877826 | bytes 735397 | solution.py:187
  273.0 1.3 dynamic_update_slice.31
  275.7 1.3 dynamic_update_slice.31
  278.7 3.6 select_add_fusion
  283.2 11.6 %while.57 = (s32[]{:T(128)}, f32[1,256,512]{2,1,0:T(8,128)S(1)}, f32[2,128,1,512]{3,1,0,2:T(8,128)}, f32[2,1,128]{2,1,0:T(1,128)S(1)}, bf16[2,128,1,256]{3,1,2,0...) while((s32[]{:T(128)}, f32[1,256,512]{2,1,0:T(8,128)S(1)}, ...), condition=%wide.region_11.12_spmd.clone.clone, body=%wide.region_9.11_spmd.clone.clone.sunk | while | flops 92848128 | bytes 3940493 | solution.py:187
  294.8 3.5 rev.34
  300.0 1.8 fusion.163
  301.8 7.6 %all-to-all-start = ((bf16[8,32,2048]{2,1,0:T(8,128)(2,1)}), bf16[8,32,2048]{2,1,0:T(8,128)(2,1)S(1)}, u32[]{:S(2)}, u32[]{:S(2)}) async-start(bf16[8,32,2048]{2,1,0:T(8,128)(2,1)} %bitcast.988), calls=%async_computation | async-start | bytes 2097152 | tf_op jit(solution)/shard_map/all_to_all | solution.py:100
  311.2 23.3 %all-to-all-done = bf16[8,32,2048]{2,1,0:T(8,128)(2,1)S(1)} async-done(((bf16[8,32,2048]{2,1,0:T(8,128)(2,1)}), bf16[8,32,2048]{2,1,0:T(8,128)(2,1)S(1)}, u32[]{:S(2)}, u32[]{:S(2)}) %all-to-all-start) | async-done | bytes 1048608 | tf_op jit(solution)/shard_map/all_to_all | solution.py:100
  335.6 31.4 %all_to_all.25 = bf16[32,2,2048]{2,1,0:T(2,128)(2,1)S(1)} all-to-all(bf16[32,2,2048]{2,1,0:T(2,128)(2,1)S(1)} %reshape.2289), channel_id=1, replica_groups=mesh['grp'=2,'sp_0'=16,'sp_1'=2,'tp'=8] {'sp_0','sp_1'}, dimensions={0} | all-to-all | bytes 524288 | tf_op jit(solution)/shard_map/all_to_all | solution.py:331
  367.3 53.5 %all_to_all.26 = bf16[8,32,2,2048]{3,1,2,0:T(8,128)(2,1)S(1)} all-to-all(bf16[8,32,2,2048]{3,1,2,0:T(8,128)(2,1)S(1)} %broadcast_in_dim.61), channel_id=1, replica_groups=mesh['grp'=2,'sp_0'=16,'sp_1'=2,'tp'=8] {'tp'}, dimensions={0} | all-to-all | bytes 4194304 | tf_op jit(solution)/shard_map/all_to_all | solution.py:106
  423.1 5.3 fusion.162
  428.3 5.0 copy.180
  433.4 4.1 convert_element_type.1630
  437.5 54.0 %all_to_all.27 = bf16[8,64,2048]{2,1,0:T(8,128)(2,1)} all-to-all(bf16[8,64,2048]{2,1,0:T(8,128)(2,1)} %convert_element_type.1630), channel_id=1, replica_groups=mesh['grp'=2,'sp_0'=16,'sp_1'=2,'tp'=8] {'tp'}, dimensions={0} | all-to-all | bytes 4194304 | tf_op jit(solution)/shard_map/all_to_all | solution.py:100
  491.4 2.0 reduce_sum.109
  494.3 6.3 %all-to-all-start.4 = ((bf16[32,2,2048]{2,1,0:T(2,128)(2,1)}), bf16[32,2,2048]{2,1,0:T(2,128)(2,1)S(1)}, u32[]{:S(2)}, u32[]{:S(2)}) async-start(bf16[32,2,2048]{2,1,0:T(2,128)(2,1)} %reshape.2295), calls=%async_computation.4 | async-start | bytes 524288 | tf_op jit(solution)/shard_map/all_to_all | solution.py:348
  501.1 21.0 %all-to-all-done.4 = bf16[32,2,2048]{2,1,0:T(2,128)(2,1)S(1)} async-done(((bf16[32,2,2048]{2,1,0:T(2,128)(2,1)}), bf16[32,2,2048]{2,1,0:T(2,128)(2,1)S(1)}, u32[]{:S(2)}, u32[]{:S(2)}) %all-to-all-start.4) | async-done | bytes 262176 | tf_op jit(solution)/shard_map/all_to_all | solution.py:348
  523.1 1.5 multiply_reduce_fusion
  (358 shorter events, 87.8 us)
Async XLA Ops:
  6.5 293.4 %copy-start = (bf16[512,2048]{1,0:T(8,128)(2,1)S(1)}, bf16[512,2048]{1,0:T(8,128)(2,1)}, u32[]{:S(2)}) copy-start(bf16[512,2048]{1,0:T(8,128)(2,1)} %param.34) | copy-start | bytes 6291460
  6.6 71.0 %copy-start.28 = (bf16[256,128]{1,0:T(8,128)(2,1)S(1)}, bf16[256,128]{1,0:T(8,128)(2,1)}, u32[]{:S(2)}) copy-start(bf16[256,128]{1,0:T(8,128)(2,1)} %param.30) | copy-start | bytes 196612
  6.6 71.1 %copy-start.29 = (bf16[256,128]{1,0:T(8,128)(2,1)S(1)}, bf16[256,128]{1,0:T(8,128)(2,1)}, u32[]{:S(2)}) copy-start(bf16[256,128]{1,0:T(8,128)(2,1)} %param.31) | copy-start | bytes 196612
  6.6 221.7 %all-gather.12.cloned.1.call-start = ((), (), s32[]{:S(2)}) async-start(), calls=%async_computation.5 | async-start | bytes 4456448 | tf_op jit(solution)/shard_map/all_gather | solution.py:37
  63.3 16.4 %copy-start.5 = (f32[256,1,128]{2,0,1:T(8,128)}, f32[256,1,128]{2,0,1:T(8,128)S(1)}, u32[]{:S(2)}) copy-start(f32[256,1,128]{2,0,1:T(8,128)S(1)} %get-tuple-element.610) | copy-start | bytes 393220
  63.3 16.4 %copy-start.7 = (f32[256,1,128]{2,0,1:T(8,128)}, f32[256,1,128]{2,0,1:T(8,128)S(1)}, u32[]{:S(2)}) copy-start(f32[256,1,128]{2,0,1:T(8,128)S(1)} %get-tuple-element.611) | copy-start | bytes 393220
  63.3 15.6 %copy-start.24 = (bf16[256,128]{1,0:T(8,128)(2,1)S(1)}, bf16[256,128]{1,0:T(8,128)(2,1)}, u32[]{:S(2)}) copy-start(bf16[256,128]{1,0:T(8,128)(2,1)} %param.32) | copy-start | bytes 196612
  69.3 178.1 %all-gather.14.cloned.1.call-start = ((), (), s32[]{:S(2)}) async-start(), calls=%async_computation.6 | async-start | bytes 4874240 | tf_op jit(solution)/shard_map/all_gather | solution.py:60
  72.8 3.3 copy-start.35
  78.7 1.7 copy-start.13
  78.9 1.4 copy-start.16
  79.1 1.3 copy-start.15
  82.7 76.9 %copy-start.2 = (bf16[2,274,512]{2,1,0:T(8,128)(2,1)}, bf16[2,274,512]{2,1,0:T(8,128)(2,1)S(1)}, u32[]{:S(2)}) copy-start(bf16[2,274,512]{2,1,0:T(8,128)(2,1)S(1)} %all-gather.6) | copy-start | bytes 1683460
  85.9 71.0 %copy-start.33 = (f32[2]{0:T(128)}, f32[2]{0:T(128)S(1)}, u32[]{:S(2)}) copy-start(f32[2]{0:T(128)S(1)} %get-tuple-element.607) | copy-start | bytes 28
  86.0 72.2 %copy-start.37 = (f32[2]{0:T(128)}, f32[2]{0:T(128)S(1)}, u32[]{:S(2)}) copy-start(f32[2]{0:T(128)S(1)} %fusion.308) | copy-start | bytes 28
  204.4 18.6 %copy-start.6 = (f32[256,1,128]{2,0,1:T(8,128)S(1)}, f32[256,1,128]{2,0,1:T(8,128)}, u32[]{:S(2)}) copy-start(f32[256,1,128]{2,0,1:T(8,128)} %copy-done.5) | copy-start | bytes 393220
  204.4 18.6 %copy-start.8 = (f32[256,1,128]{2,0,1:T(8,128)S(1)}, f32[256,1,128]{2,0,1:T(8,128)}, u32[]{:S(2)}) copy-start(f32[256,1,128]{2,0,1:T(8,128)} %copy-done.7) | copy-start | bytes 393220
  204.4 19.3 %copy-start.14 = (bf16[256,1,128]{2,0,1:T(8,128)(2,1)S(1)}, bf16[256,1,128]{2,0,1:T(8,128)(2,1)}, u32[]{:S(2)}) copy-start(bf16[256,1,128]{2,0,1:T(8,128)(2,1)} %get-tuple-element.541) | copy-start | bytes 196612
  204.4 23.8 %copy-start.4 = (bf16[512,512]{1,0:T(8,128)(2,1)S(1)}, bf16[512,512]{1,0:T(8,128)(2,1)}, u32[]{:S(2)}) copy-start(bf16[512,512]{1,0:T(8,128)(2,1)} %copy-done.3) | copy-start | bytes 1572868
  205.4 1.4 copy-start.27
  213.5 1.4 copy-start.27
  228.2 5.0 copy-start.43
  247.3 23.0 %copy-start.25 = (f32[2,64,64]{2,1,0:T(8,128)S(1)}, f32[2,64,64]{2,1,0:T(8,128)}, u32[]{:S(2)}) copy-start(f32[2,64,64]{2,1,0:T(8,128)} %reshape.2429) | copy-start | bytes 98308
  247.3 22.9 %copy-start.26 = (f32[2,64,64]{2,1,0:T(8,128)S(1)}, f32[2,64,64]{2,1,0:T(8,128)}, u32[]{:S(2)}) copy-start(f32[2,64,64]{2,1,0:T(8,128)} %reshape.2430) | copy-start | bytes 98308
  247.3 22.9 %copy-start.34 = (f32[2]{0:T(128)S(1)}, f32[2]{0:T(128)}, u32[]{:S(2)}) copy-start(f32[2]{0:T(128)} %copy-done.33) | copy-start | bytes 28
  247.3 22.9 %copy-start.38 = (f32[2]{0:T(128)S(1)}, f32[2]{0:T(128)}, u32[]{:S(2)}) copy-start(f32[2]{0:T(128)} %copy-done.37) | copy-start | bytes 28
  247.3 22.9 %copy-start.39 = (f32[2]{0:T(128)S(1)}, f32[2]{0:T(128)}, u32[]{:S(2)}) copy-start(f32[2]{0:T(128)} %get-tuple-element.605) | copy-start | bytes 28
  247.3 24.3 %copy-start.10 = (bf16[2,128,2,64]{1,3,2,0:T(8,128)(2,1)S(1)}, bf16[2,128,2,64]{1,3,2,0:T(8,128)(2,1)}, u32[]{:S(2)}) copy-start(bf16[2,128,2,64]{1,3,2,0:T(8,128)(2,1)} %copy_bitcast_fusion) | copy-start | bytes 196612
  247.3 24.3 %copy-start.11 = (bf16[2,128,2,64]{1,3,2,0:T(8,128)(2,1)S(1)}, bf16[2,128,2,64]{1,3,2,0:T(8,128)(2,1)}, u32[]{:S(2)}) copy-start(bf16[2,128,2,64]{1,3,2,0:T(8,128)(2,1)} %get-tuple-element.864) | copy-start | bytes 196612
  247.3 24.3 %copy-start.12 = (bf16[2,128,2,64]{1,3,2,0:T(8,128)(2,1)S(1)}, bf16[2,128,2,64]{1,3,2,0:T(8,128)(2,1)}, u32[]{:S(2)}) copy-start(bf16[2,128,2,64]{1,3,2,0:T(8,128)(2,1)} %get-tuple-element.863) | copy-start | bytes 196612
  247.3 24.3 %copy-start.31 = (f32[2,256]{1,0:T(2,128)S(1)}, f32[2,256]{1,0:T(2,128)}, u32[]{:S(2)}) copy-start(f32[2,256]{1,0:T(2,128)} %copy-done.30) | copy-start | bytes 6148
  271.6 5.7 %copy-start.18 = (f32[256,2,64]{0,2,1:T(8,128)S(1)}, f32[256,2,64]{0,2,1:T(8,128)}, u32[]{:S(2)}) copy-start(f32[256,2,64]{0,2,1:T(8,128)} %reshape.2281) | copy-start | bytes 393220
  278.7 4.5 copy-start.36
  294.7 4.7 copy-start.19
  294.8 4.7 copy-start.20
  301.8 7.6 %copy-start.46 = (s32[32]{0:T(128)S(1)}, s32[32]{0:T(128)}, u32[]{:S(2)}) copy-start(s32[32]{0:T(128)} %param.38) | copy-start | bytes 388
  301.8 7.6 %copy-start.41 = (s32[32,2]{0,1:T(2,128)S(1)}, s32[32,2]{0,1:T(2,128)}, u32[]{:S(2)}) copy-start(s32[32,2]{0,1:T(2,128)} %param.39) | copy-start | bytes 772
  301.8 9.4 %copy-start.32 = (f32[2,2048]{1,0:T(2,128)S(1)}, f32[2,2048]{1,0:T(2,128)}, u32[]{:S(2)}) copy-start(f32[2,2048]{1,0:T(2,128)} %param.37) | copy-start | bytes 49156
  301.8 32.9 %copy-start.9 = (bf16[32,2048]{1,0:T(8,128)(2,1)S(1)}, bf16[32,2048]{1,0:T(8,128)(2,1)}, u32[]{:S(2)}) copy-start(bf16[32,2048]{1,0:T(8,128)(2,1)} %param.36) | copy-start | bytes 393220
  301.8 32.8 %all-to-all-start = ((bf16[8,32,2048]{2,1,0:T(8,128)(2,1)}), bf16[8,32,2048]{2,1,0:T(8,128)(2,1)S(1)}, u32[]{:S(2)}, u32[]{:S(2)}) async-start(bf16[8,32,2048]{2,1,0:T(8,128)(2,1)} %bitcast.988), calls=%async_computation | async-start | bytes 2097152 | tf_op jit(solution)/shard_map/all_to_all | solution.py:100
  420.8 1.5 copy-start.21
  421.0 1.3 copy-start.1
  421.0 2.0 copy-start.22
  421.1 2.0 copy-start.23
  491.4 9.4 %copy-start.42 = (f32[32,2]{0,1:T(2,128)S(1)}, f32[32,2]{0,1:T(2,128)}, u32[]{:S(2)}) copy-start(f32[32,2]{0,1:T(2,128)} %param.40) | copy-start | bytes 772
  491.4 9.5 %copy-start.40 = (pred[32,2]{0,1:T(4,128)(4,1)S(1)}, pred[32,2]{0,1:T(4,128)(4,1)}, u32[]{:S(2)}) copy-start(pred[32,2]{0,1:T(4,128)(4,1)} %get-tuple-element.503) | copy-start | bytes 196
  491.4 9.6 %copy-start.45 = (s32[64]{0:T(128)S(1)}, s32[64]{0:T(128)}, u32[]{:S(2)}) copy-start(s32[64]{0:T(128)} %copy-done.44) | copy-start | bytes 772
  494.3 27.8 %all-to-all-start.4 = ((bf16[32,2,2048]{2,1,0:T(2,128)(2,1)}), bf16[32,2,2048]{2,1,0:T(2,128)(2,1)S(1)}, u32[]{:S(2)}, u32[]{:S(2)}) async-start(bf16[32,2,2048]{2,1,0:T(2,128)(2,1)} %reshape.2295), calls=%async_computation.4 | async-start | bytes 524288 | tf_op jit(solution)/shard_map/all_to_all | solution.py:348
  (4 other events, 3.6 us)
Sparse Core Ops, SparseCore 0:
  69.4 64.5 all-gather.11
  136.1 82.0 all-gather.13
where the time goes:
time: 537 us; the launch traced here: 533 us
  blocking collectives  275 us (51%)
  local copies, waits for them, and re-layouts  80 us (15%)
  waiting for transfers between devices  44.5 us (8%)
  between operations  42.5 us (8%)
  other arithmetic  42.3 us (8%)
  matrix products  31.7 us (6%)
  starting transfers between devices  14 us (3%)
    unnamed x2, blocking collectives  67.4 us
    all_gather x4, blocking collectives, prefix_by_axis(): lax.all_gather(part.astype(kind), axis)  66 us
    all_to_all x1, blocking collectives, summed_on_arrival(): lax.all_to_all(blocks, axis, split_axis=0, concat_axis=0, tiled=True)  54 us
    all_to_all x1, blocking collectives, sent_to_all(): return lax.all_to_all(copies, axis, split_axis=0, concat_axis=0, tiled=True)  53.5 us
    all_to_all x1, blocking collectives, shards(): lax.all_to_all(outgoing, SP, split_axis=0, concat_axis=0, tiled=True)  31.4 us
    all_to_all x1, waiting for transfers between devices, summed_on_arrival(): lax.all_to_all(blocks, axis, split_axis=0, concat_axis=0, tiled=True)  23.3 us
    all_to_all x1, waiting for transfers between devices, shards(): lax.all_to_all(back_rows, SP, split_axis=0, concat_axis=0, tiled=True)  21 us
    unnamed x116, local copies, waits for them, and re-layouts  12.3 us
  transfers between devices with their start and end apart: 4, of which 2 were waited for; matrix products, arithmetic and copies ran while one was open for 14% of the time, Pallas kernels for 0%

commit v1 on v0

v1 whole, which is shorter than its diff:
```python
import math

import jax
import jax.numpy as jnp
import numpy as np
from jax import lax
from jax.experimental import pallas as pl
from jax.experimental.pallas import tpu as pltpu
from jax.sharding import Mesh
from jax.sharding import PartitionSpec as P

CAP = 2
TOP = 2
EXP_GROUP = 8
SP = ("sp_0", "sp_1")
GRP_SP = ("grp", "sp_0", "sp_1")
GRP_SP_TP = ("grp", "sp_0", "sp_1", "tp")

RESIDUAL_SCALE = math.sqrt(2.0)
NORM_EPS = 1e-05
GROUP_EPS = 1e-06
ROPE_BASE = 10000.0

F32 = jnp.float32
BF16 = jnp.bfloat16
HIGHEST = lax.Precision.HIGHEST
INTERPRET = False

LANES = 128
TILE = 16


def vmem(count):
    return [pl.BlockSpec(memory_space=pltpu.VMEM)] * count


SMEM_SPEC = pl.BlockSpec(memory_space=pltpu.SMEM)


def iota(shape, dim):
    return lax.broadcasted_iota(jnp.int32, shape, dim)


def mm(a, b):
    return jnp.dot(a, b, preferred_element_type=F32)


def mm_nt(a, b, precision=None):
    return lax.dot_general(
        a, b, (((1,), (1,)), ((), ())), precision=precision, preferred_element_type=F32
    )


def split2(x):
    hi = x.astype(BF16).astype(F32)
    return hi, x - hi


def angle_tables(length, half_a, half_b, devices):
    def freqs(half):
        f = np.float32(ROPE_BASE) ** (-np.arange(half, dtype=np.float32) / np.float32(half))
        return f.astype(np.float64)

    fa = freqs(half_a)
    fb = np.tile(freqs(half_b), LANES // half_b)
    inside = np.arange(length, dtype=np.float64)[:, None]
    first = (np.arange(devices, dtype=np.float64) * length)[:, None]
    local = np.stack(
        [np.cos(inside * fa), np.sin(inside * fa), np.cos(inside * fb), np.sin(inside * fb)]
    ).astype(np.float32)
    base = np.zeros((devices, 8, LANES), np.float32)
    for k, row in enumerate(
        [np.cos(first * fa), np.sin(first * fa), np.cos(first * fb), np.sin(first * fb)]
    ):
        base[:, k, :] = row
    return local, base


def retention_body(
    qa_ref, ka_ref, va_ref, qb_ref, kb_ref, vb_ref, dec_ref, tab_ref, base_ref,
    qa_out, qb_out, loc_out, pay_out,
):
    n, dk = qa_ref.shape
    dv = va_ref.shape[1]
    half = dk // 2
    hb = qb_ref.shape[1] // 2
    hq = hb // 2
    row, col = iota((n, n), 0), iota((n, n), 1)
    dec = dec_ref[...]
    cr = jnp.dot(dec, (row <= col).astype(F32), precision=HIGHEST, preferred_element_type=F32)
    cc = mm_nt((col <= row).astype(F32), dec, HIGHEST)
    er = cr - dec
    ec = mm_nt((col < row).astype(F32), dec, HIGHEST)
    tot = cr[:, n - 1 : n]

    def pair_weights(h):
        forward = cc[:, h : h + 1] - cr[h : h + 1, :]
        backward = er[3 + h : 4 + h, :] - ec[:, 3 + h : 4 + h]
        return jnp.exp(jnp.where(col <= row, forward, backward))

    base = base_ref[...]
    cos_a = tab_ref[0] * base[0:1] - tab_ref[1] * base[1:2]
    sin_a = tab_ref[1] * base[0:1] + tab_ref[0] * base[1:2]

    def rotate_a(x, scale):
        x1, x2 = x[:, :half].astype(F32), x[:, half:].astype(F32)
        out = jnp.concatenate([x1 * cos_a - x2 * sin_a, x1 * sin_a + x2 * cos_a], axis=1)
        return (out * scale).astype(BF16)

    qa = rotate_a(qa_ref[...], 1.0)
    ka = rotate_a(ka_ref[...], 1.0 / math.sqrt(dk))
    qa_out[...] = qa

    width = 2 * hb
    lane = iota((n, width), 1)
    cos_b = tab_ref[2] * base[2:3] - tab_ref[3] * base[3:4]
    sin_b = tab_ref[3] * base[2:3] + tab_ref[2] * base[3:4]
    low = (lane % hb) < hq
    sin_b = jnp.where(low, -sin_b, sin_b)
    pr, pc = iota((width, width), 0), iota((width, width), 1)
    partner = jnp.where((pc % hb) < hq, pc + hq, pc - hq)
    swap = (pr == partner).astype(BF16)

    def rotate_b(x, scale):
        return ((x.astype(F32) * cos_b + mm(x, swap) * sin_b) * scale).astype(BF16)

    qb = rotate_b(qb_ref[...], 1.0)
    kb = rotate_b(kb_ref[...], 1.0 / math.sqrt(hb))
    qb_out[...] = qb

    va, vb = va_ref[...], vb_ref[...]
    kat = ka.astype(F32).T
    kbt = kb.astype(F32).T
    top = iota((width, n), 0) < hb
    for d in range(2):
        if d == 0:
            scale = [jnp.exp(tot[h : h + 1] - cr[h : h + 1, :]) for h in range(3)]
        else:
            scale = [jnp.exp(er[3 + h : 4 + h, :]) for h in range(3)]
        state = mm((kat * scale[0]).astype(BF16), va)
        pay_out[d, :dk, :] = state.astype(BF16)
        both = mm((kbt * jnp.where(top, scale[1], scale[2])).astype(BF16), vb)
        packed = jnp.where(iota((hb, width), 1) < hb, both[:hb], both[hb:]).astype(BF16)
        for q in range(dv // LANES):
            pay_out[d, dk : dk + TILE, q * LANES : (q + 1) * LANES] = packed[
                q * TILE : (q + 1) * TILE
            ]
        rows = iota((TILE, dv), 0)
        logs = jnp.zeros((TILE, dv), F32)
        for h in range(3):
            hi, lo = split2(tot[3 * d + h : 3 * d + h + 1])
            logs = jnp.where(rows == 2 * h, hi, jnp.where(rows == 2 * h + 1, lo, logs))
        pay_out[d, dk + TILE : dk + 2 * TILE, :] = logs.astype(BF16)
    weighted = (mm_nt(qa, ka) * pair_weights(0)).astype(BF16)
    loc_out[:, :dv] = mm(weighted, va)
    acc = jnp.zeros((n, width), F32)
    for h in range(2):
        mine = (lane < hb) if h == 0 else (lane >= hb)
        q_h = jnp.where(mine, qb.astype(F32), 0.0).astype(BF16)
        v_h = jnp.where(mine, vb.astype(F32), 0.0).astype(BF16)
        acc += mm((mm_nt(q_h, kb) * pair_weights(1 + h)).astype(BF16), v_h)
    loc_out[:, dv:] = acc


def retention_local(qa, ka, va, qb, kb, vb, dec, tab, base):
    n, dk = qa.shape
    dv, wb = va.shape[1], vb.shape[1]
    return pl.pallas_call(
        retention_body,
        out_shape=(
            jax.ShapeDtypeStruct((n, dk), BF16),
            jax.ShapeDtypeStruct((n, wb), BF16),
            jax.ShapeDtypeStruct((n, dv + wb), F32),
            jax.ShapeDtypeStruct((2, dk + 2 * TILE, dv), BF16),
        ),
        in_specs=vmem(9),
        out_specs=tuple(vmem(4)),
        interpret=INTERPRET,
        name="retention_local",
    )(qa, ka, va, qb, kb, vb, dec, tab, base)


def log_rows(ref, d, dk):
    rows = ref[d, dk + TILE : dk + 2 * TILE, :LANES].astype(F32)
    return [rows[2 * h : 2 * h + 1] + rows[2 * h + 1 : 2 * h + 2] for h in range(3)]


def pack_body(core_ref, own_ref, oth_ref, out_ref, ext_scr):
    chips = out_ref.shape[0]
    dv = own_ref.shape[2]
    dk = own_ref.shape[1] - 2 * TILE
    first = core_ref[0] == 0
    step = dk // chips
    blocks = dv // LANES // 2
    one = jnp.ones((1, LANES), F32)
    own_f, oth_f = log_rows(own_ref, 0, dk), log_rows(oth_ref, 0, dk)
    own_b, oth_b = log_rows(own_ref, 1, dk), log_rows(oth_ref, 1, dk)
    factor_own = [
        [jnp.where(first, jnp.exp(oth_f[h]), one) for h in range(3)],
        [jnp.where(first, one, jnp.exp(oth_b[h])) for h in range(3)],
    ]
    factor_oth = [
        [jnp.where(first, one, jnp.exp(own_f[h])) for h in range(3)],
        [jnp.where(first, jnp.exp(own_b[h]), one) for h in range(3)],
    ]
    lane = iota((1, LANES), 1)
    left = lane < LANES // 2
    for d in range(2):
        for q in range(blocks):
            a = slice(q * LANES, (q + 1) * LANES)
            b = slice((blocks + q) * LANES, (blocks + q + 1) * LANES)

            def mine(ref):
                return jnp.where(first, ref[d, :dk, a].astype(F32), ref[d, :dk, b].astype(F32))

            total = factor_own[d][0] * mine(own_ref) + factor_oth[d][0] * mine(oth_ref)
            at = (d * blocks + q) * step
            out_ref[:, at : at + step, :] = total.astype(BF16).reshape(chips, step, LANES)
    per = (dv // LANES) * TILE // chips
    for q in range(dv // LANES):
        part = []
        for d in range(2):
            fo = jnp.where(left, factor_own[d][1], factor_own[d][2])
            ft = jnp.where(left, factor_oth[d][1], factor_oth[d][2])
            cut = slice(q * LANES, (q + 1) * LANES)
            part.append(
                fo * own_ref[d, dk : dk + TILE, cut].astype(F32)
                + ft * oth_ref[d, dk : dk + TILE, cut].astype(F32)
            )
        part = jnp.where(first, part[0], part[1])
        for k in range(TILE // per):
            ext_scr[q * (TILE // per) + k, 0:per, :] = part[k * per : (k + 1) * per]
    rows = iota((TILE - per, LANES), 0)
    logs = jnp.zeros((TILE - per, LANES), F32)
    sums_f = [x + y for x, y in zip(own_f, oth_f)]
    sums_b = [x + y for x, y in zip(own_b, oth_b)]
    for k, value in enumerate(
        [
            sums_f[0],
            sums_b[0],
            jnp.where(left, sums_f[1], sums_f[2]),
            jnp.where(left, sums_b[1], sums_b[2]),
        ]
    ):
        hi, lo = split2(value)
        logs = jnp.where(rows == 2 * k, hi, jnp.where(rows == 2 * k + 1, lo, logs))
    ext_scr[:, per:, :] = jnp.broadcast_to(logs[None], (chips, TILE - per, LANES))
    at = 2 * blocks * step
    out_ref[:, at : at + TILE, :] = ext_scr[...].astype(BF16)


def pack_states(core, own, other, chips):
    dv = own.shape[2]
    dk = own.shape[1] - 2 * TILE
    rows = dv // LANES * (dk // chips) + TILE
    return pl.pallas_call(
        pack_body,
        out_shape=jax.ShapeDtypeStruct((chips, rows, LANES), BF16),
        in_specs=[SMEM_SPEC] + vmem(2),
        out_specs=vmem(1)[0],
        scratch_shapes=[pltpu.VMEM((chips, TILE, LANES), F32)],
        interpret=INTERPRET,
        name="pack_states",
    )(core, own, other)


def scan_body(per, core_ref, in_ref, out_ref):
    chips, rows, _ = in_ref.shape
    main = rows - TILE
    side = main // 2
    first = core_ref[0] == 0
    ext = [in_ref[i, main:, :].astype(F32) for i in range(chips)]
    decays = [
        [jnp.exp(e[per + 2 * k : per + 2 * k + 1] + e[per + 2 * k + 1 : per + 2 * k + 2]) for k in range(4)]
        for e in ext
    ]
    carry = jnp.zeros((side, LANES), F32)
    group = jnp.zeros((TILE, LANES), F32)
    into = []
    for i in range(chips):
        out_ref[i, :side, :] = carry.astype(BF16)
        into.append(group)
        carry = decays[i][0] * carry + in_ref[i, :side, :].astype(F32)
        group = decays[i][2] * group + ext[i]
    carry = jnp.zeros((side, LANES), F32)
    group = jnp.zeros((TILE, LANES), F32)
    for i in reversed(range(chips)):
        out_ref[i, side:main, :] = carry.astype(BF16)
        out_ref[i, main:, :] = jnp.where(first, into[i], group).astype(BF16)
        carry = decays[i][1] * carry + in_ref[i, side:main, :].astype(F32)
        group = decays[i][3] * group + ext[i]


def scan_states(core, pieces, per):
    def body(*refs):
        scan_body(per, *refs)

    return pl.pallas_call(
        body,
        out_shape=jax.ShapeDtypeStruct(pieces.shape, BF16),
        in_specs=[SMEM_SPEC] + vmem(1),
        out_specs=vmem(1)[0],
        interpret=INTERPRET,
        name="scan_states",
    )(core, pieces)


def mix_body(
    core_ref, qa_ref, qb_ref, loc_ref, own_ref, oth_ref, pay_ref, dec_ref, wa_ref, wb_ref,
    out_ref, grp_scr,
):
    n, dk = qa_ref.shape
    width = qb_ref.shape[1]
    hb = width // 2
    dv = loc_ref.shape[1] - width
    chips, rows, _ = own_ref.shape
    step = dk // chips
    blocks = dv // LANES // 2
    main = rows - TILE
    first = core_ref[0] == 0
    row, col = iota((n, n), 0), iota((n, n), 1)
    dec = dec_ref[...]
    cc = mm_nt((col <= row).astype(F32), dec, HIGHEST)
    rc = mm_nt((col >= row).astype(F32), dec, HIGHEST)
    col_f = [jnp.exp(cc[:, h : h + 1]) for h in range(3)]
    col_b = [jnp.exp(rc[:, 3 + h : 4 + h]) for h in range(3)]
    logs = [log_rows(pay_ref, d, dk) for d in range(2)]
    qa, qb = qa_ref[...], qb_ref[...]
    lane = iota((1, LANES), 1)
    left = lane < LANES // 2
    per = (dv // LANES) * TILE // chips
    total_a = loc_ref[:, :dv]
    total_b = loc_ref[:, dv:]
    for d in range(2):
        between = jnp.logical_not(first) if d == 0 else first
        factor = jnp.where(between, jnp.exp(logs[d][0]), jnp.ones((1, LANES), F32))
        keep = jnp.where(between, 1.0, 0.0)
        parts = []
        for b in range(2 * blocks):
            at = (d * blocks + b % blocks) * step
            own = own_ref[:, at : at + step, :].astype(F32)
            oth = oth_ref[:, at : at + step, :].astype(F32)
            use_own = first if b < blocks else jnp.logical_not(first)
            carry = jnp.where(use_own, own, oth).reshape(dk, LANES)
            near = pay_ref[d, :dk, b * LANES : (b + 1) * LANES].astype(F32)
            parts.append((factor * carry + keep * near).astype(BF16))
        state = jnp.concatenate(parts, axis=1)
        scale = col_f if d == 0 else col_b
        total_a = total_a + scale[0] * mm(qa, state)
        use_own = first if d == 0 else jnp.logical_not(first)
        ext = jnp.where(
            use_own, own_ref[:, main:, :].astype(F32), oth_ref[:, main:, :].astype(F32)
        )
        for i in range(chips):
            grp_scr[i * per : (i + 1) * per, :] = ext[i, 0:per, :]
        near = jnp.concatenate(
            [
                pay_ref[d, dk : dk + TILE, q * LANES : (q + 1) * LANES].astype(F32)
                for q in range(dv // LANES)
            ],
            axis=0,
        )
        factor = jnp.where(
            between,
            jnp.exp(jnp.where(left, logs[d][1], logs[d][2])),
            jnp.ones((1, LANES), F32),
        )
        group = factor * grp_scr[...] + keep * near
        blockdiag = jnp.concatenate(
            [jnp.where(left, group, 0.0), jnp.where(left, 0.0, group)], axis=0
        ).astype(BF16)
        total_b = total_b + jnp.where(left, scale[1], scale[2]) * mm(qb, blockdiag)
    square = jnp.mean(total_a * total_a, axis=1, keepdims=True)
    mixed_a = (total_a * lax.rsqrt(square + GROUP_EPS)).astype(BF16)
    sq = total_b * total_b
    s0 = jnp.sum(jnp.where(left, sq, 0.0), axis=1, keepdims=True) / hb
    s1 = jnp.sum(jnp.where(left, 0.0, sq), axis=1, keepdims=True) / hb
    mixed_b = (total_b * lax.rsqrt(jnp.where(left, s0, s1) + GROUP_EPS)).astype(BF16)
    out_ref[...] = (mm(mixed_a, wa_ref[...]) + mm(mixed_b, wb_ref[...])).astype(BF16)


def mix_project(core, qa, qb, loc, own, other, pay, dec, wa, wb):
    hb = qb.shape[1] // 2
    return pl.pallas_call(
        mix_body,
        out_shape=jax.ShapeDtypeStruct((qa.shape[0], wa.shape[1]), BF16),
        in_specs=[SMEM_SPEC] + vmem(9),
        out_specs=vmem(1)[0],
        scratch_shapes=[pltpu.VMEM((hb, qb.shape[1]), F32)],
        interpret=INTERPRET,
        name="mix_project",
    )(core, qa, qb, loc, own, other, pay, dec, wa, wb)


def layer_norm(stream, gain):
    center = stream - jnp.mean(stream, axis=-1, keepdims=True)
    spread = jnp.mean(center * center, axis=-1, keepdims=True)
    return center * lax.rsqrt(spread + NORM_EPS) * gain


def slots_by_route(ids):
    routes = ids.shape[1]
    row, col = iota((routes, routes), 0), iota((routes, routes), 1)
    ids_f = ids.astype(F32)
    ids_col = jnp.sum(jnp.where(row == col, ids_f, 0.0), axis=1, keepdims=True)
    same = (ids_col == ids_f) & (row < col)
    rank = jnp.sum(jnp.where(same, 1.0, 0.0), axis=0, keepdims=True)
    slot = ids_f * CAP + jnp.minimum(rank, CAP - 1.0)
    return jnp.where((row.astype(F32) == slot) & (rank < CAP), 1.0, 0.0)


def route_rows(rows, routes):
    return iota((rows, routes), 1) // TOP == iota((rows, routes), 0)


def dispatch_body(arr_ref, res_ref, gain_ref, ids_ref, hid_ref, out_ref):
    mix = jnp.sum(arr_ref[...].astype(F32), axis=0)
    stream = RESIDUAL_SCALE * res_ref[...].astype(F32) + mix
    hidden = layer_norm(stream, gain_ref[0:1, :]).astype(BF16)
    hid_ref[...] = hidden
    hot = slots_by_route(ids_ref[...])
    belongs = jnp.where(route_rows(hidden.shape[0], hot.shape[1]), 1.0, 0.0)
    choose = mm_nt(hot.astype(BF16), belongs.astype(BF16)).astype(BF16)
    out_ref[...] = mm(choose, hidden).astype(BF16)


def dispatch(arrived, residual, gain, ids):
    rows, width = residual.shape
    return pl.pallas_call(
        dispatch_body,
        out_shape=(
            jax.ShapeDtypeStruct((rows, width), BF16),
            jax.ShapeDtypeStruct((ids.shape[1], width), BF16),
        ),
        in_specs=vmem(4),
        out_specs=tuple(vmem(2)),
        interpret=INTERPRET,
        name="dispatch",
    )(arrived, residual, gain, ids)


def pack_weights_body(gate_ref, up_ref, down_ref, out_ref):
    width, units = gate_ref.shape[1:]
    pair = 2 * units
    out_ref[:width, :units] = gate_ref[0]
    out_ref[:width, units:] = up_ref[0]
    for k in range(width // pair):
        out_ref[width + k * units : width + (k + 1) * units, :] = down_ref[
            0, :, k * pair : (k + 1) * pair
        ]


def pack_weights(gate, up, down):
    _, width, units = gate.shape
    return pl.pallas_call(
        pack_weights_body,
        out_shape=jax.ShapeDtypeStruct((width + width // 2, 2 * units), BF16),
        in_specs=vmem(3),
        out_specs=vmem(1)[0],
        interpret=INTERPRET,
        name="pack_weights",
    )(gate, up, down)


def expert_body(x_ref, w_ref, out_ref, acc_ref):
    step = pl.program_id(0)
    sets, _, pair = w_ref.shape
    width = x_ref.shape[1]
    units = pair // 2

    @pl.when(step == 0)
    def _():
        acc_ref[...] = jnp.zeros_like(acc_ref)

    x = x_ref[...]
    hidden = []
    for s in range(sets):
        both = mm(x, w_ref[s, :width, :])
        gate, up = both[:, :units], both[:, units:]
        hidden.append((gate / (1.0 + jnp.exp(-gate)) * up).astype(BF16))
    hidden = jnp.concatenate(hidden, axis=1)
    for k in range(width // pair):
        at = width + k * units
        down = jnp.concatenate([w_ref[s, at : at + units, :] for s in range(sets)], axis=0)
        acc_ref[:, k * pair : (k + 1) * pair] += mm(hidden, down)

    @pl.when(step == pl.num_programs(0) - 1)
    def _():
        out_ref[...] = acc_ref[...].astype(BF16)


def experts(x, weights, sets=2):
    count, depth, pair = weights.shape
    rows, width = x.shape
    return pl.pallas_call(
        expert_body,
        grid=(count // sets,),
        out_shape=jax.ShapeDtypeStruct((rows, width), BF16),
        in_specs=[
            pl.BlockSpec((rows, width), lambda i: (0, 0)),
            pl.BlockSpec((sets, depth, pair), lambda i: (i, 0, 0)),
        ],
        out_specs=pl.BlockSpec((rows, width), lambda i: (0, 0)),
        scratch_shapes=[pltpu.VMEM((rows, width), F32)],
        interpret=INTERPRET,
        name="experts",
    )(x, weights)


def combine_body(ret_ref, hid_ref, gain_ref, ids_ref, w_ref, out_ref):
    hidden = hid_ref[...]
    hot = slots_by_route(ids_ref[...])
    factor = jnp.where(route_rows(hidden.shape[0], hot.shape[1]), w_ref[...], 0.0)
    weights = mm_nt(factor, hot, HIGHEST)
    returned = ret_ref[...]
    hi = weights.astype(BF16)
    rest = weights - hi.astype(F32)
    mid = rest.astype(BF16)
    low = (rest - mid.astype(F32)).astype(BF16)
    ffn = mm(hi, returned) + mm(mid, returned) + mm(low, returned)
    stream = RESIDUAL_SCALE * hidden.astype(F32) + ffn
    out_ref[...] = layer_norm(stream, gain_ref[1:2, :]).astype(BF16)


def combine(returned, hidden, gain, ids, weights):
    return pl.pallas_call(
        combine_body,
        out_shape=jax.ShapeDtypeStruct(hidden.shape, BF16),
        in_specs=vmem(5),
        out_specs=vmem(1)[0],
        interpret=INTERPRET,
        name="combine",
    )(returned, hidden, gain, ids, weights)


def exchange(array, axis):
    return lax.all_to_all(array, axis, split_axis=0, concat_axis=0, tiled=True)


def decay_rows(decay_a, decay_b):
    length = decay_a.shape[-1]
    return jnp.concatenate(
        [decay_a[0], decay_b[0], decay_a[1], decay_b[1], jnp.zeros((2, length), F32)], axis=0
    )


def shards(
    query_a, key_a, value_a, decay_a, query_b, key_b, value_b, decay_b, out_weight_a,
    out_weight_b, residual, norm_gain, route_group, route_expert, route_weight, expert_gate,
    expert_up, expert_down,
):
    length = query_a.shape[0]
    chips = lax.axis_size("sp_0")
    sp_count = lax.axis_size(SP)
    tp = lax.axis_size("tp")
    rows_dev, width = residual.shape
    routes = rows_dev * TOP
    weights_all = lax.all_gather(pack_weights(expert_gate, expert_up, expert_down), "tp")

    core = lax.axis_index("sp_1").astype(jnp.int32).reshape(1)
    local, base = angle_tables(
        length, query_a.shape[1] // 2, query_b.shape[1] // 4, sp_count
    )
    base = lax.dynamic_index_in_dim(jnp.asarray(base), lax.axis_index(SP), 0, keepdims=False)
    dec = decay_rows(decay_a, decay_b)
    qa, qb, loc, pay = retention_local(
        query_a, key_a, value_a, query_b, key_b, value_b, dec, jnp.asarray(local), base
    )
    swap = [(0, 1), (1, 0)]
    pay_other = lax.ppermute(pay, "sp_1", swap)
    pieces = exchange(pack_states(core, pay, pay_other, chips), "sp_0")
    per = value_a.shape[1] // LANES * TILE // chips
    carried = exchange(scan_states(core, pieces, per), "sp_0")
    carried_other = lax.ppermute(carried, "sp_1", swap)
    partial = mix_project(
        core, qa, qb, loc, carried, carried_other, pay_other, dec, out_weight_a, out_weight_b
    )
    arrived = exchange(partial.reshape(tp, rows_dev, width), "tp")
    ids = (route_group[:, None] * EXP_GROUP + route_expert).reshape(1, routes)
    hidden, outgoing = dispatch(arrived, residual, norm_gain, ids)
    slots = outgoing.shape[0]
    received = exchange(outgoing.reshape(sp_count, slots // sp_count, width), SP)
    back = experts(received.reshape(slots, width), weights_all)
    returned = exchange(back.reshape(sp_count, slots // sp_count, width), SP)
    return combine(
        returned.reshape(slots, width), hidden, norm_gain, ids, route_weight.reshape(1, routes)
    )


def solution(mesh):
    sp = mesh.shape["sp"]
    finer = Mesh(
        mesh.devices.reshape(mesh.shape["grp"], sp // 2, 2, mesh.shape["tp"]),
        ("grp", "sp_0", "sp_1", "tp"),
    )
    in_specs = (
        P(GRP_SP, "tp"),
        P(GRP_SP, "tp"),
        P(GRP_SP, "tp"),
        P(None, "tp", GRP_SP),
        P(GRP_SP, "tp"),
        P(GRP_SP, "tp"),
        P(GRP_SP, "tp"),
        P(None, "tp", GRP_SP),
        P("tp", None),
        P("tp", None),
        P(GRP_SP_TP, None),
        P(),
        P(GRP_SP_TP),
        P(GRP_SP_TP, None),
        P(GRP_SP_TP, None),
        P(SP, None, "tp"),
        P(SP, None, "tp"),
        P(SP, "tp", None),
    )
    out_specs = P(GRP_SP_TP, None)
    return jax.shard_map(
        shards, mesh=finer, in_specs=in_specs, out_specs=out_specs, check_vma=False
    )
```

time: 537 us -> 262 us (0.49)
  blocking collectives: 275 us -> 76.3 us
  local copies, waits for them, and re-layouts: 80 us -> 10.5 us
  starting transfers between devices: 14 us -> 69 us
  other arithmetic: 42.3 us -> 0.01 us
  matrix products: 31.7 us -> 0 us
  between operations: 42.5 us -> 13.5 us
  Pallas kernels: 0 us -> 28.1 us
  waiting for transfers between devices: 44.5 us -> 63.8 us
    all_gather x5 -> x0, blocking collectives: 68.3 us -> none  [the longest x4 66 us: prefix_by_axis(): lax.all_gather(part.astype(kind), axis)]
    unnamed x2 -> x0, blocking collectives: 67.4 us -> none
    all_to_all x3, blocking collectives: 139 us -> 76.3 us  [exchange(): return lax.all_to_all(array, axis, split_axis=0, concat_axis=0, tiled=True)]
    ppermute x0 -> x2, starting transfers between devices: none -> 51.9 us  [the longest x1 43.4 us: shards(): pay_other = lax.ppermute(pay, 'sp_1', swap)]
    dot_general x33 -> x0, matrix products: 31.7 us -> none  [the longest x8 7.98 us: advance(): jnp.einsum('hij,jhv->ihv', weighted, value_blk, preferred_element_type=jn...]
    pallas_call x0 -> x8, Pallas kernels: none -> 28.1 us  [the longest x1 7.31 us: experts(): pl.pallas_call(expert_body, grid=(count // sets,), out_shape=jax.ShapeDty...]
    convert_element_type x20 -> x0, local copies, waits for them, and re-layouts: 19.3 us -> none  [the longest x18 10.1 us: prefix_by_axis_2(): part[k].astype(own.dtype)]
    all_to_all x2, waiting for transfers between devices: 44.3 us -> 60.7 us  [exchange(): return lax.all_to_all(array, axis, split_axis=0, concat_axis=0, tiled=True)]
  transfers between devices with their start and end apart: 4 -> 5, of which waited for: 2 -> 4; matrix products, arithmetic and copies ran while one was open for 14% -> 2% of each run, Pallas kernels for 0% -> 6%
where the time goes in v1:
time: 262 us; the launch traced here: 261 us
  blocking collectives  76.3 us (29%)
  starting transfers between devices  69 us (26%)
  waiting for transfers between devices  63.8 us (24%)
  Pallas kernels  28.1 us (11%)
  between operations  13.5 us (5%)
  local copies, waits for them, and re-layouts  10.5 us (4%)
    all_to_all x3, blocking collectives, exchange(): return lax.all_to_all(array, axis, split_axis=0, concat_axis=0, tiled=True)  76.3 us
    all_to_all x2, waiting for transfers between devices, exchange(): return lax.all_to_all(array, axis, split_axis=0, concat_axis=0, tiled=True)  60.7 us
    ppermute x1, starting transfers between devices, shards(): pay_other = lax.ppermute(pay, 'sp_1', swap)  43.4 us
    all_to_all x2, starting transfers between devices, exchange(): return lax.all_to_all(array, axis, split_axis=0, concat_axis=0, tiled=True)  17.1 us
    ppermute x1, starting transfers between devices, shards(): carried_other = lax.ppermute(carried, 'sp_1', swap)  8.55 us
    pallas_call x1, Pallas kernels, experts(): pl.pallas_call(expert_body, grid=(count // sets,), out_shape=jax.ShapeDty...  7.31 us
    pallas_call x1, Pallas kernels, mix_project(): pl.pallas_call(mix_body, out_shape=jax.ShapeDtypeStruct((qa.shape[0], wa....  5.44 us
  transfers between devices with their start and end apart: 5, of which 4 were waited for; matrix products, arithmetic and copies ran while one was open for 2% of the time, Pallas kernels for 6%

profile of v1, /device:TPU:65, one launch (start us, length us, event | category | flops | bytes accessed | tf_op | source)
XLA Modules:
  0.0 261.3 jit_solution(7857247718731316876)
XLA Ops:
  6.5 0.0 copy-start.5
  6.5 0.0 copy-start.4
  6.6 0.0 all-gather.3.cloned.1.call-start
  6.6 2.8 %pack_weights.1 = bf16[3072,256]{1,0:T(8,128)(2,1)} custom-call(bf16[1,2048,128]{2,1,0:T(8,128)(2,1)} %gate_ref.1, bf16[1,2048,128]{2,1,0:T(8,128)(2,1)} %up_ref.1, bf16[1,128,2048]{2,1,0:T(8,128)(2,1)} %down_ref.1), custom_call_target="tpu_custom_call" | custom-call | tf_op jit(solution)/shard_map/pack_weights/pallas_call | solution.py:455
  9.3 0.1 all-gather.3.cloned.1.call-update
  9.4 0.0 copy-done.5
  9.4 0.0 copy-done.4
  9.4 0.6 concatenate.3.dec_ref
  10.1 1.3 dynamic-slice_bitcast_fusion.base_ref
  11.3 3.5 %retention_local.1 = (bf16[256,256]{1,0:T(8,128)(2,1)}, bf16[256,128]{1,0:T(8,128)(2,1)}, f32[256,640]{1,0:T(8,128)}, bf16[2,288,512]{2,1,0:T(8,128)(2,1)}) custom-call(bf16[256,256]{1,0:T(8,128)(2,1)} %qa_ref.1, bf16[256,256]{1,0:T(8,128)(2,1)} %ka_ref.1, bf16[256,512]{1,0:T(8,128)(2,1)} %va_ref.1, bf16[256,128]{1,0:T(8,128)(2,1)} %qb_ref.1, ...), custom_call_target="tpu_custom_call" | custom-call | tf_op jit(solution)/shard_map/retention_local/pallas_call | solution.py:168
  14.9 43.4 %collective-permute-start = (bf16[2,288,512]{2,1,0:T(8,128)(2,1)}, bf16[2,288,512]{2,1,0:T(8,128)(2,1)S(1)}, u32[]{:S(2)}, u32[]{:S(2)}) collective-permute-start(bf16[2,288,512]{2,1,0:T(8,128)(2,1)} %get-tuple-element.14.own_ref), channel_id=1, source_target_pairs={{0,8},{8,0},{1,9},{9,1},{2,10},{10,2},{3,11},{11,3},{4,12},{12,4},... | collective-permute-start | bytes 1769480 | tf_op jit(solution)/shard_map/ppermute | solution.py:570
  58.2 1.8 collective-permute-done.oth_ref.pay_ref
  60.0 0.0 copy-start.1
  60.0 0.8 copy-done.1
  60.9 2.2 pack_states.1
  63.0 20.1 %all_to_all.25.refs_1_ = bf16[16,80,128]{2,1,0:T(8,128)(2,1)} all-to-all(bf16[16,80,128]{2,1,0:T(8,128)(2,1)} %pack_states.1), channel_id=1, replica_groups=mesh['grp'=2,'sp_0'=16,'sp_1'=2,'tp'=8] {'sp_0'}, dimensions={0} | all-to-all | bytes 655360 | tf_op jit(solution)/shard_map/all_to_all | solution.py:537
  83.2 1.8 scan_states.1
  85.0 26.6 %all_to_all.26.own_ref = bf16[16,80,128]{2,1,0:T(8,128)(2,1)S(1)} all-to-all(bf16[16,80,128]{2,1,0:T(8,128)(2,1)} %scan_states.1), channel_id=1, replica_groups=mesh['grp'=2,'sp_0'=16,'sp_1'=2,'tp'=8] {'sp_0'}, dimensions={0} | all-to-all | bytes 655360 | tf_op jit(solution)/shard_map/all_to_all | solution.py:537
  111.6 0.0 copy-start.2
  111.6 8.5 %collective-permute-start.1 = (bf16[16,80,128]{2,1,0:T(8,128)(2,1)S(1)}, bf16[16,80,128]{2,1,0:T(8,128)(2,1)S(1)}, u32[]{:S(2)}, u32[]{:S(2)}) collective-permute-start(bf16[16,80,128]{2,1,0:T(8,128)(2,1)S(1)} %all_to_all.26.own_ref), channel_id=1, source_target_pairs={{0,8},{8,0},{1,9},{9,1},{2,10},{10,2},{3,11},{11,3},{4,12},{12,4},... | collective-permute-start | bytes 983048 | tf_op jit(solution)/shard_map/ppermute | solution.py:574
  120.2 1.2 collective-permute-done.1.oth_ref
  121.4 0.0 copy-start.3
  121.4 0.0 copy-done.2
  121.4 0.7 copy-done.3
  122.1 5.4 %mix_project.1 = bf16[256,2048]{1,0:T(8,128)(2,1)} custom-call(s32[1]{0:T(128)} %bitcast.core_ref.refs_0_, bf16[256,256]{1,0:T(8,128)(2,1)} %get-tuple-element.11.qa_ref, bf16[256,128]{1,0:T(8,128)(2,1)} %get-tuple-element.12.qb_ref, f32[256,640]{1,0:T(8,128)} %get-tuple-element.13.loc_ref, bf16[16,80,128]{2,1,0:T(8,128)(2,1)} %copy-done.2, ...), custom_call_target="tpu_custom_call" | custom-call | tf_op jit(solution)/shard_map/mix_project/pallas_call | solution.py:384
  127.6 0.0 copy-start.8
  127.6 0.0 copy-start.7
  127.6 6.1 %all-to-all-start.2 = ((bf16[8,32,2048]{2,1,0:T(8,128)(2,1)}), bf16[8,32,2048]{2,1,0:T(8,128)(2,1)S(1)}, u32[]{:S(2)}, u32[]{:S(2)}) async-start(bf16[8,32,2048]{2,1,0:T(8,128)(2,1)} %bitcast.14), calls=%async_computation.2 | async-start | bytes 2097152 | tf_op jit(solution)/shard_map/all_to_all | solution.py:537
  133.6 0.0 copy-done.8
  133.7 0.0 copy-done.7
  133.7 0.1 copy.23
  133.8 0.6 reshape.28.ids_ref
  134.4 39.4 %all-to-all-done.2.arr_ref = bf16[8,32,2048]{2,1,0:T(8,128)(2,1)S(1)} async-done(((bf16[8,32,2048]{2,1,0:T(8,128)(2,1)}), bf16[8,32,2048]{2,1,0:T(8,128)(2,1)S(1)}, u32[]{:S(2)}, u32[]{:S(2)}) %all-to-all-start.2) | async-done | bytes 1048608 | tf_op jit(solution)/shard_map/all_to_all | solution.py:537
  173.8 0.0 copy-start
  173.8 1.0 copy-done
  174.8 2.6 dispatch.1
  177.4 1.1 reshape.29
  178.5 29.6 %all_to_all.27 = bf16[32,2,2048]{2,1,0:T(2,128)(2,1)S(1)} all-to-all(bf16[32,2,2048]{2,1,0:T(2,128)(2,1)S(1)} %reshape.29), channel_id=1, replica_groups=mesh['grp'=2,'sp_0'=16,'sp_1'=2,'tp'=8] {'sp_0','sp_1'}, dimensions={0} | all-to-all | bytes 524288 | tf_op jit(solution)/shard_map/all_to_all | solution.py:537
  208.1 0.8 reshape.30.x_ref
  208.9 7.3 %experts.1 = bf16[64,2048]{1,0:T(8,128)(2,1)} custom-call(bf16[64,2048]{1,0:T(8,128)(2,1)} %reshape.30.x_ref, bf16[8,3072,256]{2,1,0:T(8,128)(2,1)} %bitcast.13), custom_call_target="tpu_custom_call" | custom-call | tf_op jit(solution)/shard_map/experts/pallas_call | solution.py:495
  216.2 1.8 reshape.31
  218.0 11.0 %all-to-all-start.4 = ((bf16[32,2,2048]{2,1,0:T(2,128)(2,1)}), bf16[32,2,2048]{2,1,0:T(2,128)(2,1)S(1)}, u32[]{:S(2)}, u32[]{:S(2)}) async-start(bf16[32,2,2048]{2,1,0:T(2,128)(2,1)} %reshape.31), calls=%async_computation.4 | async-start | bytes 524288 | tf_op jit(solution)/shard_map/all_to_all | solution.py:537
  229.0 0.0 copy-done.6
  229.1 0.1 copy.24
  229.1 0.7 reshape.33.w_ref
  229.8 21.3 %all-to-all-done.4 = bf16[32,2,2048]{2,1,0:T(2,128)(2,1)S(1)} async-done(((bf16[32,2,2048]{2,1,0:T(2,128)(2,1)}), bf16[32,2,2048]{2,1,0:T(2,128)(2,1)S(1)}, u32[]{:S(2)}, u32[]{:S(2)}) %all-to-all-start.4) | async-done | bytes 262176 | tf_op jit(solution)/shard_map/all_to_all | solution.py:537
  251.2 0.8 reshape.32.ret_ref
  251.9 2.5 combine.1
  (7 shorter events, 0.0 us)
Async XLA Ops:
  6.5 2.9 %copy-start.5 = (f32[2,1,256]{2,1,0:T(1,128)S(1)}, f32[2,1,256]{2,1,0:T(1,128)}, u32[]{:S(2)}) copy-start(f32[2,1,256]{2,1,0:T(1,128)} %param.23) | copy-start | bytes 6148
  6.5 2.9 %copy-start.4 = (f32[2,2,256]{2,1,0:T(2,128)S(1)}, f32[2,2,256]{2,1,0:T(2,128)}, u32[]{:S(2)}) copy-start(f32[2,2,256]{2,1,0:T(2,128)} %param.27) | copy-start | bytes 12292
  6.6 202.4 %all-gather.3.cloned.1.call-start = ((), (), s32[]{:S(2)}) async-start(), calls=%async_computation.5 | async-start | bytes 14155776 | tf_op jit(solution)/shard_map/all_gather | solution.py:558
  14.9 45.2 %collective-permute-start = (bf16[2,288,512]{2,1,0:T(8,128)(2,1)}, bf16[2,288,512]{2,1,0:T(8,128)(2,1)S(1)}, u32[]{:S(2)}, u32[]{:S(2)}) collective-permute-start(bf16[2,288,512]{2,1,0:T(8,128)(2,1)} %get-tuple-element.14.own_ref), channel_id=1, source_target_pairs={{0,8},{8,0},{1,9},{9,1},{2,10},{10,2},{3,11},{11,3},{4,12},{12,4},... | collective-permute-start | bytes 1769480 | tf_op jit(solution)/shard_map/ppermute | solution.py:570
  60.0 0.8 copy-start.1
  111.6 9.8 %copy-start.2 = (bf16[16,80,128]{2,1,0:T(8,128)(2,1)}, bf16[16,80,128]{2,1,0:T(8,128)(2,1)S(1)}, u32[]{:S(2)}) copy-start(bf16[16,80,128]{2,1,0:T(8,128)(2,1)S(1)} %all_to_all.26.own_ref) | copy-start | bytes 983044
  111.6 9.8 %collective-permute-start.1 = (bf16[16,80,128]{2,1,0:T(8,128)(2,1)S(1)}, bf16[16,80,128]{2,1,0:T(8,128)(2,1)S(1)}, u32[]{:S(2)}, u32[]{:S(2)}) collective-permute-start(bf16[16,80,128]{2,1,0:T(8,128)(2,1)S(1)} %all_to_all.26.own_ref), channel_id=1, source_target_pairs={{0,8},{8,0},{1,9},{9,1},{2,10},{10,2},{3,11},{11,3},{4,12},{12,4},... | collective-permute-start | bytes 983048 | tf_op jit(solution)/shard_map/ppermute | solution.py:574
  121.4 0.7 copy-start.3
  127.6 6.1 %copy-start.8 = (s32[32]{0:T(128)S(1)}, s32[32]{0:T(128)}, u32[]{:S(2)}) copy-start(s32[32]{0:T(128)} %param.32) | copy-start | bytes 388
  127.6 6.1 %copy-start.7 = (s32[32,2]{0,1:T(2,128)S(1)}, s32[32,2]{0,1:T(2,128)}, u32[]{:S(2)}) copy-start(s32[32,2]{0,1:T(2,128)} %param.33) | copy-start | bytes 772
  127.6 46.2 %all-to-all-start.2 = ((bf16[8,32,2048]{2,1,0:T(8,128)(2,1)}), bf16[8,32,2048]{2,1,0:T(8,128)(2,1)S(1)}, u32[]{:S(2)}, u32[]{:S(2)}) async-start(bf16[8,32,2048]{2,1,0:T(8,128)(2,1)} %bitcast.14), calls=%async_computation.2 | async-start | bytes 2097152 | tf_op jit(solution)/shard_map/all_to_all | solution.py:537
  173.8 1.0 copy-start
  208.9 20.1 %copy-start.6 = (f32[32,2]{0,1:T(2,128)S(1)}, f32[32,2]{0,1:T(2,128)}, u32[]{:S(2)}) copy-start(f32[32,2]{0,1:T(2,128)} %param.34) | copy-start | bytes 772
  218.0 33.1 %all-to-all-start.4 = ((bf16[32,2,2048]{2,1,0:T(2,128)(2,1)}), bf16[32,2,2048]{2,1,0:T(2,128)(2,1)S(1)}, u32[]{:S(2)}, u32[]{:S(2)}) async-start(bf16[32,2,2048]{2,1,0:T(2,128)(2,1)} %reshape.31), calls=%async_computation.4 | async-start | bytes 524288 | tf_op jit(solution)/shard_map/all_to_all | solution.py:537
Sparse Core Ops, SparseCore 0:
  9.5 196.3 all-gather.2

commit v2 on v1

--- a/solution.py
+++ b/solution.py
@@ -35,6 +35,7 @@
 
 
 SMEM_SPEC = pl.BlockSpec(memory_space=pltpu.SMEM)
+ANY_SPEC = pl.BlockSpec(memory_space=pl.ANY)
 
 
 def iota(shape, dim):
@@ -291,18 +292,26 @@
         group = decays[i][3] * group + ext[i]
 
 
-def scan_states(core, pieces, per):
-    def body(*refs):
-        scan_body(per, *refs)
-
-    return pl.pallas_call(
+def passed_through(arrays, inputs, outputs):
+    shapes = tuple(jax.ShapeDtypeStruct(x.shape, x.dtype) for x in arrays)
+    return shapes, [ANY_SPEC] * len(arrays), {inputs + k: outputs + k for k in range(len(arrays))}
+
+
+def scan_states(core, pieces, per, held):
+    def body(core_ref, in_ref, *refs):
+        scan_body(per, core_ref, in_ref, refs[len(held)])
+
+    shapes, specs, aliases = passed_through(held, 2, 1)
+    out = pl.pallas_call(
         body,
-        out_shape=jax.ShapeDtypeStruct(pieces.shape, BF16),
-        in_specs=[SMEM_SPEC] + vmem(1),
-        out_specs=vmem(1)[0],
+        out_shape=(jax.ShapeDtypeStruct(pieces.shape, BF16),) + shapes,
+        in_specs=[SMEM_SPEC] + vmem(1) + specs,
+        out_specs=tuple(vmem(1) + specs),
+        input_output_aliases=aliases,
         interpret=INTERPRET,
         name="scan_states",
-    )(core, pieces)
+    )(core, pieces, *held)
+    return out[0], out[1:]
 
 
 def mix_body(
@@ -379,17 +388,24 @@
     out_ref[...] = (mm(mixed_a, wa_ref[...]) + mm(mixed_b, wb_ref[...])).astype(BF16)
 
 
-def mix_project(core, qa, qb, loc, own, other, pay, dec, wa, wb):
+def mix_project(core, qa, qb, loc, own, other, pay, dec, wa, wb, held):
     hb = qb.shape[1] // 2
-    return pl.pallas_call(
-        mix_body,
-        out_shape=jax.ShapeDtypeStruct((qa.shape[0], wa.shape[1]), BF16),
-        in_specs=[SMEM_SPEC] + vmem(9),
-        out_specs=vmem(1)[0],
+
+    def body(*refs):
+        mix_body(*refs[:10], refs[10 + len(held)], refs[-1])
+
+    shapes, specs, aliases = passed_through(held, 10, 1)
+    out = pl.pallas_call(
+        body,
+        out_shape=(jax.ShapeDtypeStruct((qa.shape[0], wa.shape[1]), BF16),) + shapes,
+        in_specs=[SMEM_SPEC] + vmem(9) + specs,
+        out_specs=tuple(vmem(1) + specs),
         scratch_shapes=[pltpu.VMEM((hb, qb.shape[1]), F32)],
+        input_output_aliases=aliases,
         interpret=INTERPRET,
         name="mix_project",
-    )(core, qa, qb, loc, own, other, pay, dec, wa, wb)
+    )(core, qa, qb, loc, own, other, pay, dec, wa, wb, *held)
+    return out[0], out[1:]
 
 
 def layer_norm(stream, gain):
@@ -413,7 +429,17 @@
     return iota((rows, routes), 1) // TOP == iota((rows, routes), 0)
 
 
-def dispatch_body(arr_ref, res_ref, gain_ref, ids_ref, hid_ref, out_ref):
+def dispatch_body(
+    arr_ref, res_ref, gain_ref, ids_ref, up_ref, down_ref,
+    hid_ref, out_ref, up_half, down_half, up_out, down_out, sems,
+):
+    half = up_half.shape[0]
+    copies = [
+        pltpu.make_async_copy(up_ref.at[pl.ds(0, half), :], up_half, sems.at[0]),
+        pltpu.make_async_copy(down_ref.at[pl.ds(half, half), :], down_half, sems.at[1]),
+    ]
+    for copy in copies:
+        copy.start()
     mix = jnp.sum(arr_ref[...].astype(F32), axis=0)
     stream = RESIDUAL_SCALE * res_ref[...].astype(F32) + mix
     hidden = layer_norm(stream, gain_ref[0:1, :]).astype(BF16)
@@ -422,21 +448,30 @@
     belongs = jnp.where(route_rows(hidden.shape[0], hot.shape[1]), 1.0, 0.0)
     choose = mm_nt(hot.astype(BF16), belongs.astype(BF16)).astype(BF16)
     out_ref[...] = mm(choose, hidden).astype(BF16)
-
-
-def dispatch(arrived, residual, gain, ids):
+    for copy in copies:
+        copy.wait()
+
+
+def dispatch(arrived, residual, gain, ids, held):
     rows, width = residual.shape
+    depth, pair = held[0].shape
+    shapes, specs, aliases = passed_through(held, 4, 4)
+    half = jax.ShapeDtypeStruct((depth // 2, pair), BF16)
     return pl.pallas_call(
         dispatch_body,
         out_shape=(
             jax.ShapeDtypeStruct((rows, width), BF16),
             jax.ShapeDtypeStruct((ids.shape[1], width), BF16),
-        ),
-        in_specs=vmem(4),
-        out_specs=tuple(vmem(2)),
+            half,
+            half,
+        ) + shapes,
+        in_specs=vmem(4) + specs,
+        out_specs=tuple(vmem(2) + [ANY_SPEC] * 2 + specs),
+        scratch_shapes=[pltpu.SemaphoreType.DMA((2,))],
+        input_output_aliases=aliases,
         interpret=INTERPRET,
         name="dispatch",
-    )(arrived, residual, gain, ids)
+    )(arrived, residual, gain, ids, *held)
 
 
 def pack_weights_body(gate_ref, up_ref, down_ref, out_ref):
@@ -462,49 +497,66 @@
     )(gate, up, down)
 
 
-def expert_body(x_ref, w_ref, out_ref, acc_ref):
-    step = pl.program_id(0)
-    sets, _, pair = w_ref.shape
+def expert_body(x_ref, *refs):
+    *blocks, top_ref, bottom_ref, out_ref, w_scr, acc_ref, sems = refs
+    count, depth, pair = w_scr.shape
     width = x_ref.shape[1]
     units = pair // 2
-
-    @pl.when(step == 0)
-    def _():
-        acc_ref[...] = jnp.zeros_like(acc_ref)
-
+    half = depth // 2
+    copies = [
+        [pltpu.make_async_copy(ref, w_scr.at[k], sems.at[k])] for k, ref in enumerate(blocks)
+    ]
+    copies.append(
+        [
+            pltpu.make_async_copy(top_ref, w_scr.at[count - 1, pl.ds(0, half), :], sems.at[count - 1]),
+            pltpu.make_async_copy(bottom_ref, w_scr.at[count - 1, pl.ds(half, half), :], sems.at[count]),
+        ]
+    )
+    for group in copies:
+        for copy in group:
+            copy.start()
     x = x_ref[...]
-    hidden = []
-    for s in range(sets):
-        both = mm(x, w_ref[s, :width, :])
-        gate, up = both[:, :units], both[:, units:]
-        hidden.append((gate / (1.0 + jnp.exp(-gate)) * up).astype(BF16))
-    hidden = jnp.concatenate(hidden, axis=1)
-    for k in range(width // pair):
-        at = width + k * units
-        down = jnp.concatenate([w_ref[s, at : at + units, :] for s in range(sets)], axis=0)
-        acc_ref[:, k * pair : (k + 1) * pair] += mm(hidden, down)
-
-    @pl.when(step == pl.num_programs(0) - 1)
-    def _():
-        out_ref[...] = acc_ref[...].astype(BF16)
-
-
-def experts(x, weights, sets=2):
-    count, depth, pair = weights.shape
+    for first in range(0, count, 2):
+        hidden = []
+        for k in (first, first + 1):
+            for copy in copies[k]:
+                copy.wait()
+            both = mm(x, w_scr[k, :width, :])
+            gate, up = both[:, :units], both[:, units:]
+            hidden.append((gate / (1.0 + jnp.exp(-gate)) * up).astype(BF16))
+        hidden = jnp.concatenate(hidden, axis=1)
+        for c in range(width // pair):
+            at = width + c * units
+            cut = slice(c * pair, (c + 1) * pair)
+            down = jnp.concatenate(
+                [w_scr[k, at : at + units, :] for k in (first, first + 1)], axis=0
+            )
+            part = mm(hidden, down)
+            if first == 0:
+                acc_ref[:, cut] = part
+            elif first < count - 2:
+                acc_ref[:, cut] += part
+            else:
+                out_ref[:, cut] = (acc_ref[:, cut] + part).astype(BF16)
+
+
+def experts(x, blocks):
+    depth, pair = blocks[0].shape
+    count = len(blocks) - 1
     rows, width = x.shape
     return pl.pallas_call(
         expert_body,
-        grid=(count // sets,),
         out_shape=jax.ShapeDtypeStruct((rows, width), BF16),
-        in_specs=[
-            pl.BlockSpec((rows, width), lambda i: (0, 0)),
-            pl.BlockSpec((sets, depth, pair), lambda i: (i, 0, 0)),
+        in_specs=vmem(1) + [ANY_SPEC] * len(blocks),
+        out_specs=vmem(1)[0],
+        scratch_shapes=[
+            pltpu.VMEM((count, depth, pair), BF16),
+            pltpu.VMEM((rows, width), F32),
+            pltpu.SemaphoreType.DMA((count + 1,)),
         ],
-        out_specs=pl.BlockSpec((rows, width), lambda i: (0, 0)),
-        scratch_shapes=[pltpu.VMEM((rows, width), F32)],
         interpret=INTERPRET,
         name="experts",
-    )(x, weights)
+    )(x, *blocks)
 
 
 def combine_body(ret_ref, hid_ref, gain_ref, ids_ref, w_ref, out_ref):
@@ -555,7 +607,17 @@
     tp = lax.axis_size("tp")
     rows_dev, width = residual.shape
     routes = rows_dev * TOP
-    weights_all = lax.all_gather(pack_weights(expert_gate, expert_up, expert_down), "tp")
+    blocks = [pack_weights(expert_gate, expert_up, expert_down)]
+    up_ring = [(k, (k + 1) % tp) for k in range(tp)]
+    down_ring = [(k, (k - 1) % tp) for k in range(tp)]
+
+    def passed_on(going_up, going_down):
+        return (
+            lax.ppermute(going_up, "tp", up_ring),
+            lax.ppermute(going_down, "tp", down_ring),
+        )
+
+    held = passed_on(blocks[0], blocks[0])
 
     core = lax.axis_index("sp_1").astype(jnp.int32).reshape(1)
     local, base = angle_tables(
@@ -570,17 +632,26 @@
     pay_other = lax.ppermute(pay, "sp_1", swap)
     pieces = exchange(pack_states(core, pay, pay_other, chips), "sp_0")
     per = value_a.shape[1] // LANES * TILE // chips
-    carried = exchange(scan_states(core, pieces, per), "sp_0")
+    scanned, held = scan_states(core, pieces, per, held)
+    blocks += held
+    held = passed_on(*held)
+    carried = exchange(scanned, "sp_0")
     carried_other = lax.ppermute(carried, "sp_1", swap)
-    partial = mix_project(
-        core, qa, qb, loc, carried, carried_other, pay_other, dec, out_weight_a, out_weight_b
-    )
+    partial, held = mix_project(
+        core, qa, qb, loc, carried, carried_other, pay_other, dec, out_weight_a, out_weight_b, held
+    )
+    blocks += held
+    held = passed_on(*held)
     arrived = exchange(partial.reshape(tp, rows_dev, width), "tp")
     ids = (route_group[:, None] * EXP_GROUP + route_expert).reshape(1, routes)
-    hidden, outgoing = dispatch(arrived, residual, norm_gain, ids)
+    hidden, outgoing, up_half, down_half, *held = dispatch(
+        arrived, residual, norm_gain, ids, held
+    )
+    blocks += held
+    blocks += passed_on(up_half, down_half)
     slots = outgoing.shape[0]
     received = exchange(outgoing.reshape(sp_count, slots // sp_count, width), SP)
-    back = experts(received.reshape(slots, width), weights_all)
+    back = experts(received.reshape(slots, width), blocks)
     returned = exchange(back.reshape(sp_count, slots // sp_count, width), SP)
     return combine(
         returned.reshape(slots, width), hidden, norm_gain, ids, route_weight.reshape(1, routes)

time: 262 us -> 343 us (1.31)
  blocking collectives: 76.3 us -> 19 us
  waiting for transfers between devices: 63.8 us -> 121 us
  Pallas kernels: 28.1 us -> 76.5 us
  starting transfers between devices: 69 us -> 110 us
  between operations: 13.5 us -> 0.21 us
  local copies, waits for them, and re-layouts: 10.5 us -> 15.3 us
    ppermute x0 -> x8, waiting for transfers between devices: none -> 82.8 us  [the longest x4 80.7 us: passed_on(): lax.ppermute(going_up, 'tp', up_ring)]
    all_to_all x3 -> x1, blocking collectives: 76.3 us -> 19 us  [exchange(): return lax.all_to_all(array, axis, split_axis=0, concat_axis=0, tiled=True)]
    pallas_call x1, Pallas kernels: 2.61 us -> 50.8 us  [dispatch(): pl.pallas_call(dispatch_body, out_shape=(jax.ShapeDtypeStruct((rows, widt...]
    ppermute x0 -> x8, starting transfers between devices: none -> 27.2 us  [the longest x4 18 us: passed_on(): lax.ppermute(going_down, 'tp', down_ring)]
    all_to_all x2 -> x4, waiting for transfers between devices: 60.7 us -> 36.9 us  [exchange(): return lax.all_to_all(array, axis, split_axis=0, concat_axis=0, tiled=True)]
    all_to_all x2 -> x4, starting transfers between devices: 17.1 us -> 30.5 us  [exchange(): return lax.all_to_all(array, axis, split_axis=0, concat_axis=0, tiled=True)]
  transfers between devices with their start and end apart: 5 -> 14, of which waited for: 4 -> 8; matrix products, arithmetic and copies ran while one was open for 2% -> 1% of each run, Pallas kernels for 6% -> 1%
where the time goes in v2:
time: 343 us; the launch traced here: 342 us
  waiting for transfers between devices  121 us (35%)
  starting transfers between devices  110 us (32%)
  Pallas kernels  76.5 us (22%)
  blocking collectives  19 us (6%)
  local copies, waits for them, and re-layouts  15.3 us (4%)
    ppermute x4, waiting for transfers between devices, passed_on(): lax.ppermute(going_up, 'tp', up_ring)  80.7 us
    pallas_call x1, Pallas kernels, dispatch(): pl.pallas_call(dispatch_body, out_shape=(jax.ShapeDtypeStruct((rows, widt...  50.8 us
    ppermute x1, starting transfers between devices, shards(): pay_other = lax.ppermute(pay, 'sp_1', swap)  43.4 us
    all_to_all x4, waiting for transfers between devices, exchange(): return lax.all_to_all(array, axis, split_axis=0, concat_axis=0, tiled=True)  36.9 us
    all_to_all x4, starting transfers between devices, exchange(): return lax.all_to_all(array, axis, split_axis=0, concat_axis=0, tiled=True)  30.5 us
    all_to_all x1, blocking collectives, exchange(): return lax.all_to_all(array, axis, split_axis=0, concat_axis=0, tiled=True)  19 us
    ppermute x4, starting transfers between devices, passed_on(): lax.ppermute(going_down, 'tp', down_ring)  18 us
    ppermute x4, starting transfers between devices, passed_on(): lax.ppermute(going_up, 'tp', up_ring)  9.21 us
  transfers between devices with their start and end apart: 14, of which 8 were waited for; matrix products, arithmetic and copies ran while one was open for 1% of the time, Pallas kernels for 1%

profile of v2, /device:TPU:65, one launch (start us, length us, event | category | flops | bytes accessed | tf_op | source)
XLA Modules:
  0.0 342.2 jit_solution(10839298670905732807)
XLA Ops:
  0.0 0.7 slice_bitcast_fusion
  0.7 0.7 slice_bitcast_fusion.2
  1.4 1.3 dynamic-slice_bitcast_fusion.base_ref
  2.7 0.6 concatenate.3.dec_ref.refs_7_
  3.3 3.6 %retention_local.1 = (bf16[256,256]{1,0:T(8,128)(2,1)}, bf16[256,128]{1,0:T(8,128)(2,1)}, f32[256,640]{1,0:T(8,128)}, bf16[2,288,512]{2,1,0:T(8,128)(2,1)}) custom-call(bf16[256,256]{1,0:T(8,128)(2,1)} %qa_ref.1, bf16[256,256]{1,0:T(8,128)(2,1)} %ka_ref.1, bf16[256,512]{1,0:T(8,128)(2,1)} %va_ref.1, bf16[256,128]{1,0:T(8,128)(2,1)} %qb_ref.1, ...), custom_call_target="tpu_custom_call" | custom-call | tf_op jit(solution)/shard_map/retention_local/pallas_call | solution.py:169
  6.8 43.4 %collective-permute-start = (bf16[2,288,512]{2,1,0:T(8,128)(2,1)}, bf16[2,288,512]{2,1,0:T(8,128)(2,1)}, u32[]{:S(2)}, u32[]{:S(2)}) collective-permute-start(bf16[2,288,512]{2,1,0:T(8,128)(2,1)} %get-tuple-element.24.own_ref), channel_id=1, source_target_pairs={{0,8},{8,0},{1,9},{9,1},{2,10},{10,2},{3,11},{11,3},{4,12},{12,4},... | collective-permute-start | bytes 1769480 | tf_op jit(solution)/shard_map/ppermute | solution.py:632
  50.2 2.8 pack_weights.1.refs_0_
  53.0 1.9 collective-permute-start.1
  54.9 4.6 %collective-permute-start.2 = (bf16[3072,256]{1,0:T(8,128)(2,1)}, bf16[3072,256]{1,0:T(8,128)(2,1)S(1)}, u32[]{:S(2)}, u32[]{:S(2)}) collective-permute-start(bf16[3072,256]{1,0:T(8,128)(2,1)} %pack_weights.1.refs_0_), channel_id=1, source_target_pairs={{0,7},{1,0},{2,1},{3,2},{4,3},{5,4},{6,5},{7,6},{8,15},{9,8},{10,9... | collective-permute-start | bytes 4718600 | tf_op jit(solution)/shard_map/ppermute | solution.py:617
  59.5 2.2 pack_states.1
  61.7 4.3 %all-to-all-start = ((bf16[16,80,128]{2,1,0:T(8,128)(2,1)}), bf16[16,80,128]{2,1,0:T(8,128)(2,1)S(1)}, u32[]{:S(2)}, u32[]{:S(2)}) async-start(bf16[16,80,128]{2,1,0:T(8,128)(2,1)} %pack_states.1), calls=%async_computation | async-start | bytes 655360 | tf_op jit(solution)/shard_map/all_to_all | solution.py:589
  66.0 26.2 %collective-permute-done.1.refs_0_ = bf16[3072,256]{1,0:T(8,128)(2,1)S(1)} collective-permute-done((bf16[3072,256]{1,0:T(8,128)(2,1)}, bf16[3072,256]{1,0:T(8,128)(2,1)S(1)}, u32[]{:S(2)}, u32[]{:S(2)}) %collective-permute-start.1) | collective-permute-done | bytes 1572896 | tf_op jit(solution)/shard_map/ppermute | solution.py:616
  92.2 1.0 collective-permute-done.2.refs_1_
  93.3 0.2 copy-done.3
  93.5 1.0 copy-done.5
  94.4 0.7 copy-done.7
  95.2 1.8 scan_states.1
  97.0 1.9 collective-permute-start.4
  98.9 5.2 %collective-permute-start.5 = (bf16[3072,256]{1,0:T(8,128)(2,1)}, bf16[3072,256]{1,0:T(8,128)(2,1)S(1)}, u32[]{:S(2)}, u32[]{:S(2)}) collective-permute-start(bf16[3072,256]{1,0:T(8,128)(2,1)} %get-tuple-element.27.refs_2_), channel_id=1, source_target_pairs={{0,7},{1,0},{2,1},{3,2},{4,3},{5,4},{6,5},{7,6},{8,15},{9,8},{10,9... | collective-permute-start | bytes 4718600 | tf_op jit(solution)/shard_map/ppermute | solution.py:617
  104.2 19.0 %all_to_all.25.refs_4_ = bf16[16,80,128]{2,1,0:T(8,128)(2,1)S(1)} all-to-all(bf16[16,80,128]{2,1,0:T(8,128)(2,1)} %get-tuple-element.25), channel_id=1, replica_groups=mesh['grp'=2,'sp_0'=16,'sp_1'=2,'tp'=8] {'sp_0'}, dimensions={0} | all-to-all | bytes 655360 | tf_op jit(solution)/shard_map/all_to_all | solution.py:589
  123.2 9.2 %collective-permute-start.3 = (bf16[16,80,128]{2,1,0:T(8,128)(2,1)S(1)}, bf16[16,80,128]{2,1,0:T(8,128)(2,1)S(1)}, u32[]{:S(2)}, u32[]{:S(2)}) collective-permute-start(bf16[16,80,128]{2,1,0:T(8,128)(2,1)S(1)} %all_to_all.25.refs_4_), channel_id=1, source_target_pairs={{0,8},{8,0},{1,9},{9,1},{2,10},{10,2},{3,11},{11,3},{4,12},{12,4},... | collective-permute-start | bytes 983048 | tf_op jit(solution)/shard_map/ppermute | solution.py:639
  132.3 1.2 collective-permute-done.3.refs_5_
  133.6 2.5 collective-permute-done.4.refs_10_
  136.0 1.0 collective-permute-done.5.refs_11_
  137.2 1.0 copy-done.4
  138.2 5.5 %mix_project.1 = (bf16[256,2048]{1,0:T(8,128)(2,1)}, bf16[3072,256]{1,0:T(8,128)(2,1)}, bf16[3072,256]{1,0:T(8,128)(2,1)}) custom-call(s32[1]{0:T(128)} %bitcast.core_ref.refs_0_, bf16[256,256]{1,0:T(8,128)(2,1)} %get-tuple-element.21.refs_1_, bf16[256,128]{1,0:T(8,128)(2,1)} %get-tuple-element.22.refs_2_, ...), custom_call_target="tpu_custom_call", output_to_operand_aliasing={{1}: (10, {}), {2}: (11, {})} | custom-call | tf_op jit(solution)/shard_map/mix_project/pallas_call | solution.py:398
  143.7 4.7 %all-to-all-start.2 = ((bf16[8,32,2048]{2,1,0:T(8,128)(2,1)}), bf16[8,32,2048]{2,1,0:T(8,128)(2,1)}, u32[]{:S(2)}, u32[]{:S(2)}) async-start(bf16[8,32,2048]{2,1,0:T(8,128)(2,1)} %bitcast.12), calls=%async_computation.2 | async-start | bytes 2097152 | tf_op jit(solution)/shard_map/all_to_all | solution.py:589
  148.4 3.4 collective-permute-start.6
  151.8 3.5 %collective-permute-start.7 = (bf16[3072,256]{1,0:T(8,128)(2,1)}, bf16[3072,256]{1,0:T(8,128)(2,1)}, u32[]{:S(2)}, u32[]{:S(2)}) collective-permute-start(bf16[3072,256]{1,0:T(8,128)(2,1)} %get-tuple-element.30.refs_4_), channel_id=1, source_target_pairs={{0,7},{1,0},{2,1},{3,2},{4,3},{5,4},{6,5},{7,6},{8,15},{9,8},{10,9... | collective-permute-start | bytes 4718600 | tf_op jit(solution)/shard_map/ppermute | solution.py:617
  155.5 0.6 reshape.28.ids_ref
  156.1 52.0 %collective-permute-done.6.up_ref = bf16[3072,256]{1,0:T(8,128)(2,1)S(1)} collective-permute-done((bf16[3072,256]{1,0:T(8,128)(2,1)S(1)}, bf16[3072,256]{1,0:T(8,128)(2,1)S(1)}, u32[]{:S(2)}, u32[]{:S(2)}) %collective-permute-start.6) | collective-permute-done | bytes 1572896 | tf_op jit(solution)/shard_map/ppermute | solution.py:616
  208.2 1.2 copy-done.2
  209.3 50.8 %dispatch.1 = (bf16[32,2048]{1,0:T(8,128)(2,1)}, bf16[64,2048]{1,0:T(8,128)(2,1)}, bf16[1536,256]{1,0:T(8,128)(2,1)}, bf16[1536,256]{1,0:T(8,128)(2,1)}, bf16[30...) custom-call(bf16[8,32,2048]{2,1,0:T(8,128)(2,1)} %all-to-all-done.2.arr_ref, ...), custom_call_target="tpu_custom_call", output_to_operand_aliasing={{4}: (4, {}), {5}: (5, {})} | custom-call | tf_op jit(solution)/shard_map/dispatch/pallas_call | solution.py:460
  260.2 1.8 reshape.29
  262.0 8.1 %all-to-all-start.3 = ((bf16[32,2,2048]{2,1,0:T(2,128)(2,1)}), bf16[32,2,2048]{2,1,0:T(2,128)(2,1)S(1)}, u32[]{:S(2)}, u32[]{:S(2)}) async-start(bf16[32,2,2048]{2,1,0:T(2,128)(2,1)} %reshape.29), calls=%async_computation.3 | async-start | bytes 524288 | tf_op jit(solution)/shard_map/all_to_all | solution.py:589
  270.1 2.0 collective-permute-start.8
  272.0 4.6 %collective-permute-start.9 = (bf16[1536,256]{1,0:T(8,128)(2,1)}, bf16[1536,256]{1,0:T(8,128)(2,1)S(1)}, u32[]{:S(2)}, u32[]{:S(2)}) collective-permute-start(bf16[1536,256]{1,0:T(8,128)(2,1)} %get-tuple-element.35), channel_id=1, source_target_pairs={{0,7},{1,0},{2,1},{3,2},{4,3},{5,4},{6,5},{7,6},{8,15},{9,8},{10,9... | collective-permute-start | bytes 2359304 | tf_op jit(solution)/shard_map/ppermute | solution.py:617
  276.7 15.5 %all-to-all-done.3 = bf16[32,2,2048]{2,1,0:T(2,128)(2,1)S(1)} async-done(((bf16[32,2,2048]{2,1,0:T(2,128)(2,1)}), bf16[32,2,2048]{2,1,0:T(2,128)(2,1)S(1)}, u32[]{:S(2)}, u32[]{:S(2)}) %all-to-all-start.3) | async-done | bytes 262176 | tf_op jit(solution)/shard_map/all_to_all | solution.py:589
  292.2 0.8 reshape.30.x_ref
  293.0 0.9 copy-done.8
  293.9 0.3 copy-done.9
  294.2 7.4 %experts.1 = bf16[64,2048]{1,0:T(8,128)(2,1)} custom-call(bf16[64,2048]{1,0:T(8,128)(2,1)} %reshape.30.x_ref, bf16[3072,256]{1,0:T(8,128)(2,1)} %pack_weights.1.refs_0_, bf16[3072,256]{1,0:T(8,128)(2,1)} %get-tuple-element.26.refs_1_, bf16[3072,256]{1,0:T(8,128)(2,1)} %get-tuple-element.27.refs_2_, bf16[3072,256]{1,0:T(8,128)(2,1)} %get-tuple-element.29.refs_3_, ...), custom_call_target="tpu_custom_call" | custom-call | tf_op jit(solution)/shard_map/experts/pallas_call | solution.py:547
  301.6 1.8 reshape.31
  303.4 13.4 %all-to-all-start.4 = ((bf16[32,2,2048]{2,1,0:T(2,128)(2,1)}), bf16[32,2,2048]{2,1,0:T(2,128)(2,1)S(1)}, u32[]{:S(2)}, u32[]{:S(2)}) async-start(bf16[32,2,2048]{2,1,0:T(2,128)(2,1)} %reshape.31), calls=%async_computation.4 | async-start | bytes 524288 | tf_op jit(solution)/shard_map/all_to_all | solution.py:589
  316.9 0.6 reshape.33.w_ref
  317.6 21.4 %all-to-all-done.4 = bf16[32,2,2048]{2,1,0:T(2,128)(2,1)S(1)} async-done(((bf16[32,2,2048]{2,1,0:T(2,128)(2,1)}), bf16[32,2,2048]{2,1,0:T(2,128)(2,1)S(1)}, u32[]{:S(2)}, u32[]{:S(2)}) %all-to-all-start.4) | async-done | bytes 262176 | tf_op jit(solution)/shard_map/all_to_all | solution.py:589
  339.0 0.8 reshape.32.ret_ref
  339.7 2.5 combine.1
  (32 shorter events, 0.3 us)
Async XLA Ops:
  6.8 52.7 %collective-permute-start = (bf16[2,288,512]{2,1,0:T(8,128)(2,1)}, bf16[2,288,512]{2,1,0:T(8,128)(2,1)}, u32[]{:S(2)}, u32[]{:S(2)}) collective-permute-start(bf16[2,288,512]{2,1,0:T(8,128)(2,1)} %get-tuple-element.24.own_ref), channel_id=1, source_target_pairs={{0,8},{8,0},{1,9},{9,1},{2,10},{10,2},{3,11},{11,3},{4,12},{12,4},... | collective-permute-start | bytes 1769480 | tf_op jit(solution)/shard_map/ppermute | solution.py:632
  53.0 39.3 %collective-permute-start.1 = (bf16[3072,256]{1,0:T(8,128)(2,1)}, bf16[3072,256]{1,0:T(8,128)(2,1)S(1)}, u32[]{:S(2)}, u32[]{:S(2)}) collective-permute-start(bf16[3072,256]{1,0:T(8,128)(2,1)} %pack_weights.1.refs_0_), channel_id=1, source_target_pairs={{0,1},{1,2},{2,3},{3,4},{4,5},{5,6},{6,7},{7,0},{8,9},{9,10},{10,1... | collective-permute-start | bytes 4718600 | tf_op jit(solution)/shard_map/ppermute | solution.py:616
  54.9 38.4 %collective-permute-start.2 = (bf16[3072,256]{1,0:T(8,128)(2,1)}, bf16[3072,256]{1,0:T(8,128)(2,1)S(1)}, u32[]{:S(2)}, u32[]{:S(2)}) collective-permute-start(bf16[3072,256]{1,0:T(8,128)(2,1)} %pack_weights.1.refs_0_), channel_id=1, source_target_pairs={{0,7},{1,0},{2,1},{3,2},{4,3},{5,4},{6,5},{7,6},{8,15},{9,8},{10,9... | collective-permute-start | bytes 4718600 | tf_op jit(solution)/shard_map/ppermute | solution.py:617
  61.7 31.6 %all-to-all-start = ((bf16[16,80,128]{2,1,0:T(8,128)(2,1)}), bf16[16,80,128]{2,1,0:T(8,128)(2,1)S(1)}, u32[]{:S(2)}, u32[]{:S(2)}) async-start(bf16[16,80,128]{2,1,0:T(8,128)(2,1)} %pack_states.1), calls=%async_computation | async-start | bytes 655360 | tf_op jit(solution)/shard_map/all_to_all | solution.py:589
  92.2 1.2 copy-start.3
  93.3 1.1 copy-start.5
  94.4 0.7 copy-start.7
  97.0 39.1 %collective-permute-start.4 = (bf16[3072,256]{1,0:T(8,128)(2,1)}, bf16[3072,256]{1,0:T(8,128)(2,1)S(1)}, u32[]{:S(2)}, u32[]{:S(2)}) collective-permute-start(bf16[3072,256]{1,0:T(8,128)(2,1)} %get-tuple-element.26.refs_1_), channel_id=1, source_target_pairs={{0,1},{1,2},{2,3},{3,4},{4,5},{5,6},{6,7},{7,0},{8,9},{9,10},{10,1... | collective-permute-start | bytes 4718600 | tf_op jit(solution)/shard_map/ppermute | solution.py:616
  98.9 38.1 %collective-permute-start.5 = (bf16[3072,256]{1,0:T(8,128)(2,1)}, bf16[3072,256]{1,0:T(8,128)(2,1)S(1)}, u32[]{:S(2)}, u32[]{:S(2)}) collective-permute-start(bf16[3072,256]{1,0:T(8,128)(2,1)} %get-tuple-element.27.refs_2_), channel_id=1, source_target_pairs={{0,7},{1,0},{2,1},{3,2},{4,3},{5,4},{6,5},{7,6},{8,15},{9,8},{10,9... | collective-permute-start | bytes 4718600 | tf_op jit(solution)/shard_map/ppermute | solution.py:617
  123.2 13.9 %copy-start.6 = (bf16[16,80,128]{2,1,0:T(8,128)(2,1)}, bf16[16,80,128]{2,1,0:T(8,128)(2,1)S(1)}, u32[]{:S(2)}) copy-start(bf16[16,80,128]{2,1,0:T(8,128)(2,1)S(1)} %all_to_all.25.refs_4_) | copy-start | bytes 983044
  123.2 10.4 %collective-permute-start.3 = (bf16[16,80,128]{2,1,0:T(8,128)(2,1)S(1)}, bf16[16,80,128]{2,1,0:T(8,128)(2,1)S(1)}, u32[]{:S(2)}, u32[]{:S(2)}) collective-permute-start(bf16[16,80,128]{2,1,0:T(8,128)(2,1)S(1)} %all_to_all.25.refs_4_), channel_id=1, source_target_pairs={{0,8},{8,0},{1,9},{9,1},{2,10},{10,2},{3,11},{11,3},{4,12},{12,4},... | collective-permute-start | bytes 983048 | tf_op jit(solution)/shard_map/ppermute | solution.py:639
  133.6 3.5 %copy-start.10 = (bf16[16,80,128]{2,1,0:T(8,128)(2,1)}, bf16[16,80,128]{2,1,0:T(8,128)(2,1)S(1)}, u32[]{:S(2)}) copy-start(bf16[16,80,128]{2,1,0:T(8,128)(2,1)S(1)} %collective-permute-done.3.refs_5_) | copy-start | bytes 983044
  136.0 1.2 copy-start
  137.1 1.1 copy-start.4
  143.7 4.8 %copy-start.1 = (bf16[3072,256]{1,0:T(8,128)(2,1)S(1)}, bf16[3072,256]{1,0:T(8,128)(2,1)}, u32[]{:S(2)}) copy-start(bf16[3072,256]{1,0:T(8,128)(2,1)} %get-tuple-element.29.refs_3_) | copy-start | bytes 4718596
  143.7 11.7 %copy-start.13 = (s32[32]{0:T(128)S(1)}, s32[32]{0:T(128)}, u32[]{:S(2)}) copy-start(s32[32]{0:T(128)} %param.32) | copy-start | bytes 388
  143.7 11.7 %copy-start.12 = (s32[32,2]{0,1:T(2,128)S(1)}, s32[32,2]{0,1:T(2,128)}, u32[]{:S(2)}) copy-start(s32[32,2]{0,1:T(2,128)} %param.33) | copy-start | bytes 772
  143.7 64.5 %all-to-all-start.2 = ((bf16[8,32,2048]{2,1,0:T(8,128)(2,1)}), bf16[8,32,2048]{2,1,0:T(8,128)(2,1)}, u32[]{:S(2)}, u32[]{:S(2)}) async-start(bf16[8,32,2048]{2,1,0:T(8,128)(2,1)} %bitcast.12), calls=%async_computation.2 | async-start | bytes 2097152 | tf_op jit(solution)/shard_map/all_to_all | solution.py:589
  148.4 59.7 %collective-permute-start.6 = (bf16[3072,256]{1,0:T(8,128)(2,1)S(1)}, bf16[3072,256]{1,0:T(8,128)(2,1)S(1)}, u32[]{:S(2)}, u32[]{:S(2)}) collective-permute-start(bf16[3072,256]{1,0:T(8,128)(2,1)S(1)} %copy-done.1), channel_id=1, source_target_pairs={{0,1},{1,2},{2,3},{3,4},{4,5},{5,6},{6,7},{7,0},{8,9},{9,10},{10,1... | collective-permute-start | bytes 4718600 | tf_op jit(solution)/shard_map/ppermute | solution.py:616
  151.8 56.3 %collective-permute-start.7 = (bf16[3072,256]{1,0:T(8,128)(2,1)}, bf16[3072,256]{1,0:T(8,128)(2,1)}, u32[]{:S(2)}, u32[]{:S(2)}) collective-permute-start(bf16[3072,256]{1,0:T(8,128)(2,1)} %get-tuple-element.30.refs_4_), channel_id=1, source_target_pairs={{0,7},{1,0},{2,1},{3,2},{4,3},{5,4},{6,5},{7,6},{8,15},{9,8},{10,9... | collective-permute-start | bytes 4718600 | tf_op jit(solution)/shard_map/ppermute | solution.py:617
  208.1 1.2 copy-start.2
  262.0 30.2 %all-to-all-start.3 = ((bf16[32,2,2048]{2,1,0:T(2,128)(2,1)}), bf16[32,2,2048]{2,1,0:T(2,128)(2,1)S(1)}, u32[]{:S(2)}, u32[]{:S(2)}) async-start(bf16[32,2,2048]{2,1,0:T(2,128)(2,1)} %reshape.29), calls=%async_computation.3 | async-start | bytes 524288 | tf_op jit(solution)/shard_map/all_to_all | solution.py:589
  270.1 22.9 %collective-permute-start.8 = (bf16[1536,256]{1,0:T(8,128)(2,1)}, bf16[1536,256]{1,0:T(8,128)(2,1)S(1)}, u32[]{:S(2)}, u32[]{:S(2)}) collective-permute-start(bf16[1536,256]{1,0:T(8,128)(2,1)} %get-tuple-element.34), channel_id=1, source_target_pairs={{0,1},{1,2},{2,3},{3,4},{4,5},{5,6},{6,7},{7,0},{8,9},{9,10},{10,1... | collective-permute-start | bytes 2359304 | tf_op jit(solution)/shard_map/ppermute | solution.py:616
  272.0 21.0 %collective-permute-start.9 = (bf16[1536,256]{1,0:T(8,128)(2,1)}, bf16[1536,256]{1,0:T(8,128)(2,1)S(1)}, u32[]{:S(2)}, u32[]{:S(2)}) collective-permute-start(bf16[1536,256]{1,0:T(8,128)(2,1)} %get-tuple-element.35), channel_id=1, source_target_pairs={{0,7},{1,0},{2,1},{3,2},{4,3},{5,4},{6,5},{7,6},{8,15},{9,8},{10,9... | collective-permute-start | bytes 2359304 | tf_op jit(solution)/shard_map/ppermute | solution.py:617
  293.0 0.9 copy-start.8
  293.0 1.2 copy-start.9
  294.2 22.7 %copy-start.11 = (f32[32,2]{0,1:T(2,128)S(1)}, f32[32,2]{0,1:T(2,128)}, u32[]{:S(2)}) copy-start(f32[32,2]{0,1:T(2,128)} %param.34) | copy-start | bytes 772
  303.4 35.5 %all-to-all-start.4 = ((bf16[32,2,2048]{2,1,0:T(2,128)(2,1)}), bf16[32,2,2048]{2,1,0:T(2,128)(2,1)S(1)}, u32[]{:S(2)}, u32[]{:S(2)}) async-start(bf16[32,2,2048]{2,1,0:T(2,128)(2,1)} %reshape.31), calls=%async_computation.4 | async-start | bytes 524288 | tf_op jit(solution)/shard_map/all_to_all | solution.py:589

commit v3 on v1

--- a/solution.py
+++ b/solution.py
@@ -35,6 +35,7 @@
 
 
 SMEM_SPEC = pl.BlockSpec(memory_space=pltpu.SMEM)
+ANY_SPEC = pl.BlockSpec(memory_space=pl.ANY)
 
 
 def iota(shape, dim):
@@ -413,7 +414,23 @@
     return iota((rows, routes), 1) // TOP == iota((rows, routes), 0)
 
 
-def dispatch_body(arr_ref, res_ref, gain_ref, ids_ref, hid_ref, out_ref):
+def store_chunks(value, out_ref, scr):
+    rows, width = value.shape
+    cuts = width // LANES
+    for k in range(cuts):
+        scr[pl.ds(k, rows, stride=cuts), :] = value[:, k * LANES : (k + 1) * LANES]
+    out_ref[...] = scr[...].astype(BF16).reshape(out_ref.shape)
+
+
+def load_chunks(ref, rows, scr):
+    cuts = scr.shape[0] // rows
+    scr[...] = ref[...].reshape(scr.shape).astype(F32)
+    return jnp.concatenate(
+        [scr[pl.ds(k, rows, stride=cuts), :] for k in range(cuts)], axis=1
+    ).astype(BF16)
+
+
+def dispatch_body(arr_ref, res_ref, gain_ref, ids_ref, hid_ref, out_ref, scr):
     mix = jnp.sum(arr_ref[...].astype(F32), axis=0)
     stream = RESIDUAL_SCALE * res_ref[...].astype(F32) + mix
     hidden = layer_norm(stream, gain_ref[0:1, :]).astype(BF16)
@@ -421,98 +438,155 @@
     hot = slots_by_route(ids_ref[...])
     belongs = jnp.where(route_rows(hidden.shape[0], hot.shape[1]), 1.0, 0.0)
     choose = mm_nt(hot.astype(BF16), belongs.astype(BF16)).astype(BF16)
-    out_ref[...] = mm(choose, hidden).astype(BF16)
-
-
-def dispatch(arrived, residual, gain, ids):
+    store_chunks(mm(choose, hidden), out_ref, scr)
+
+
+def dispatch(arrived, residual, gain, ids, peers):
     rows, width = residual.shape
+    lines = ids.shape[1] * width // LANES
     return pl.pallas_call(
         dispatch_body,
         out_shape=(
             jax.ShapeDtypeStruct((rows, width), BF16),
-            jax.ShapeDtypeStruct((ids.shape[1], width), BF16),
+            jax.ShapeDtypeStruct((peers, lines // peers, LANES), BF16),
         ),
         in_specs=vmem(4),
         out_specs=tuple(vmem(2)),
+        scratch_shapes=[pltpu.VMEM((lines, LANES), F32)],
         interpret=INTERPRET,
         name="dispatch",
     )(arrived, residual, gain, ids)
 
 
-def pack_weights_body(gate_ref, up_ref, down_ref, out_ref):
-    width, units = gate_ref.shape[1:]
-    pair = 2 * units
-    out_ref[:width, :units] = gate_ref[0]
-    out_ref[:width, units:] = up_ref[0]
-    for k in range(width // pair):
-        out_ref[width + k * units : width + (k + 1) * units, :] = down_ref[
-            0, :, k * pair : (k + 1) * pair
+def pack_weights_body(part_ref, gate_ref, up_ref, down_ref, out_ref):
+    _, width, units = gate_ref.shape
+    half = units // 2
+    part = part_ref[0]
+    low = part == 0
+    left = iota((width, units), 1) < half
+    gate = gate_ref[0].astype(F32)
+    up = up_ref[0].astype(F32)
+    gate = jnp.where(low, gate, pltpu.roll(gate, half, 1))
+    up = jnp.where(low, pltpu.roll(up, half, 1), up)
+    out_ref[:width, :] = jnp.where(left, gate, up).astype(BF16)
+    rows = pl.ds(pl.multiple_of(part * half, half), half)
+    for k in range(width // units):
+        out_ref[width + k * half : width + (k + 1) * half, :] = down_ref[
+            0, rows, k * units : (k + 1) * units
         ]
 
 
-def pack_weights(gate, up, down):
+def pack_weights(part, gate, up, down):
     _, width, units = gate.shape
     return pl.pallas_call(
         pack_weights_body,
-        out_shape=jax.ShapeDtypeStruct((width + width // 2, 2 * units), BF16),
-        in_specs=vmem(3),
+        out_shape=jax.ShapeDtypeStruct((width + width // 2, units), BF16),
+        in_specs=[SMEM_SPEC] + vmem(3),
         out_specs=vmem(1)[0],
         interpret=INTERPRET,
         name="pack_weights",
-    )(gate, up, down)
-
-
-def expert_body(x_ref, w_ref, out_ref, acc_ref):
-    step = pl.program_id(0)
-    sets, _, pair = w_ref.shape
-    width = x_ref.shape[1]
-    units = pair // 2
-
-    @pl.when(step == 0)
-    def _():
-        acc_ref[...] = jnp.zeros_like(acc_ref)
-
-    x = x_ref[...]
-    hidden = []
-    for s in range(sets):
-        both = mm(x, w_ref[s, :width, :])
-        gate, up = both[:, :units], both[:, units:]
-        hidden.append((gate / (1.0 + jnp.exp(-gate)) * up).astype(BF16))
-    hidden = jnp.concatenate(hidden, axis=1)
-    for k in range(width // pair):
-        at = width + k * units
-        down = jnp.concatenate([w_ref[s, at : at + units, :] for s in range(sets)], axis=0)
-        acc_ref[:, k * pair : (k + 1) * pair] += mm(hidden, down)
-
-    @pl.when(step == pl.num_programs(0) - 1)
-    def _():
-        out_ref[...] = acc_ref[...].astype(BF16)
-
-
-def experts(x, weights, sets=2):
-    count, depth, pair = weights.shape
-    rows, width = x.shape
+    )(part, gate, up, down)
+
+
+def expert_body(own_ref, oth_ref, w_ref, mine_ref, send_ref, x_scr, w_scr, acc_ref, sems):
+    count, depth, units = w_scr.shape
+    rows = mine_ref.shape[0]
+    width = mine_ref.shape[1]
+    half = units // 2
+    copies = [
+        pltpu.make_async_copy(w_ref.at[k], w_scr.at[k], sems.at[k]) for k in range(count)
+    ]
+    for copy in copies:
+        copy.start()
+    x = jnp.concatenate(
+        [load_chunks(own_ref, rows, x_scr), load_chunks(oth_ref, rows, x_scr)], axis=0
+    )
+    left = iota((2 * rows, units), 1) < half
+
+    def silu(v):
+        return v / (1.0 + jnp.exp(-v))
+
+    group = 4
+    for first in range(0, count, group):
+        hidden = []
+        for k in range(first, first + group, 2):
+            copies[k].wait()
+            copies[k + 1].wait()
+            both = mm(x, jnp.concatenate([w_scr[k, :width, :], w_scr[k + 1, :width, :]], axis=1))
+            one, two = both[:, :units], both[:, units:]
+            one = silu(one) * pltpu.roll(one, half, 1)
+            two = silu(pltpu.roll(two, half, 1)) * two
+            hidden.append(jnp.where(left, one, two).astype(BF16))
+        hidden = jnp.concatenate(hidden, axis=1)
+        for c in range(0, width // units, 2):
+            cols = []
+            for j in (c, c + 1):
+                at = width + j * half
+                cols.append(
+                    jnp.concatenate(
+                        [w_scr[k, at : at + half, :] for k in range(first, first + group)], axis=0
+                    )
+                )
+            part = mm(hidden, jnp.concatenate(cols, axis=1))
+            cut = slice(c * units, (c + 2) * units)
+            if first == 0:
+                acc_ref[:, cut] = part
+            elif first < count - group:
+                acc_ref[:, cut] += part
+            else:
+                part = acc_ref[:, cut] + part
+                mine_ref[:, cut] = part[:rows]
+                send_ref[:, cut] = part[rows:].astype(BF16)
+
+
+def experts(own, other, weights):
+    count, depth, units = weights.shape
+    width = depth * 2 // 3
+    lines = own.shape[0] * own.shape[1]
+    rows = lines * LANES // width
     return pl.pallas_call(
         expert_body,
-        grid=(count // sets,),
-        out_shape=jax.ShapeDtypeStruct((rows, width), BF16),
-        in_specs=[
-            pl.BlockSpec((rows, width), lambda i: (0, 0)),
-            pl.BlockSpec((sets, depth, pair), lambda i: (i, 0, 0)),
+        out_shape=(
+            jax.ShapeDtypeStruct((rows, width), F32),
+            jax.ShapeDtypeStruct((rows, width), BF16),
+        ),
+        in_specs=vmem(2) + [ANY_SPEC],
+        out_specs=tuple(vmem(2)),
+        scratch_shapes=[
+            pltpu.VMEM((lines, LANES), F32),
+            pltpu.VMEM((count, depth, units), BF16),
+            pltpu.VMEM((2 * rows, width), F32),
+            pltpu.SemaphoreType.DMA((count,)),
         ],
-        out_specs=pl.BlockSpec((rows, width), lambda i: (0, 0)),
-        scratch_shapes=[pltpu.VMEM((rows, width), F32)],
         interpret=INTERPRET,
         name="experts",
-    )(x, weights)
-
-
-def combine_body(ret_ref, hid_ref, gain_ref, ids_ref, w_ref, out_ref):
+    )(own, other, weights)
+
+
+def finish_body(mine_ref, arrived_ref, out_ref, scr):
+    store_chunks(mine_ref[...] + arrived_ref[...].astype(F32), out_ref, scr)
+
+
+def finish(mine, arrived, peers):
+    rows, width = mine.shape
+    lines = rows * width // LANES
+    return pl.pallas_call(
+        finish_body,
+        out_shape=jax.ShapeDtypeStruct((peers, lines // peers, LANES), BF16),
+        in_specs=vmem(2),
+        out_specs=vmem(1)[0],
+        scratch_shapes=[pltpu.VMEM((lines, LANES), F32)],
+        interpret=INTERPRET,
+        name="finish",
+    )(mine, arrived)
+
+
+def combine_body(ret_ref, hid_ref, gain_ref, ids_ref, w_ref, out_ref, scr):
     hidden = hid_ref[...]
     hot = slots_by_route(ids_ref[...])
     factor = jnp.where(route_rows(hidden.shape[0], hot.shape[1]), w_ref[...], 0.0)
     weights = mm_nt(factor, hot, HIGHEST)
-    returned = ret_ref[...]
+    returned = load_chunks(ret_ref, hot.shape[0], scr)
     hi = weights.astype(BF16)
     rest = weights - hi.astype(F32)
     mid = rest.astype(BF16)
@@ -523,11 +597,13 @@
 
 
 def combine(returned, hidden, gain, ids, weights):
+    lines = returned.shape[0] * returned.shape[1]
     return pl.pallas_call(
         combine_body,
         out_shape=jax.ShapeDtypeStruct(hidden.shape, BF16),
         in_specs=vmem(5),
         out_specs=vmem(1)[0],
+        scratch_shapes=[pltpu.VMEM((lines, LANES), F32)],
         interpret=INTERPRET,
         name="combine",
     )(returned, hidden, gain, ids, weights)
@@ -555,7 +631,11 @@
     tp = lax.axis_size("tp")
     rows_dev, width = residual.shape
     routes = rows_dev * TOP
-    weights_all = lax.all_gather(pack_weights(expert_gate, expert_up, expert_down), "tp")
+    part = (lax.axis_index("grp") % 2).astype(jnp.int32).reshape(1)
+    partner = [(k, k ^ 1) for k in range(lax.axis_size("grp"))]
+    weights_all = lax.all_gather(
+        pack_weights(part, expert_gate, expert_up, expert_down), "tp"
+    )
 
     core = lax.axis_index("sp_1").astype(jnp.int32).reshape(1)
     local, base = angle_tables(
@@ -577,14 +657,13 @@
     )
     arrived = exchange(partial.reshape(tp, rows_dev, width), "tp")
     ids = (route_group[:, None] * EXP_GROUP + route_expert).reshape(1, routes)
-    hidden, outgoing = dispatch(arrived, residual, norm_gain, ids)
-    slots = outgoing.shape[0]
-    received = exchange(outgoing.reshape(sp_count, slots // sp_count, width), SP)
-    back = experts(received.reshape(slots, width), weights_all)
-    returned = exchange(back.reshape(sp_count, slots // sp_count, width), SP)
-    return combine(
-        returned.reshape(slots, width), hidden, norm_gain, ids, route_weight.reshape(1, routes)
-    )
+    hidden, outgoing = dispatch(arrived, residual, norm_gain, ids, sp_count)
+    received = exchange(outgoing, SP)
+    received_other = lax.ppermute(received, "grp", partner)
+    mine, send = experts(received, received_other, weights_all)
+    back = finish(mine, lax.ppermute(send, "grp", partner), sp_count)
+    returned = exchange(back, SP)
+    return combine(returned, hidden, norm_gain, ids, route_weight.reshape(1, routes))
 
 
 def solution(mesh):

time: 262 us -> 264 us (level)
    ppermute x0 -> x2, waiting for transfers between devices: none -> 11.8 us  [the longest x1 6.08 us: shards(): received_other = lax.ppermute(received, 'grp', partner)]
    all_to_all x2, waiting for transfers between devices: 60.7 us -> 49.2 us  [exchange(): return lax.all_to_all(array, axis, split_axis=0, concat_axis=0, tiled=True)]
    ppermute x0 -> x2, starting transfers between devices: none -> 7.53 us  [the longest x1 4.42 us: shards(): received_other = lax.ppermute(received, 'grp', partner)]
    all_to_all x2, starting transfers between devices: 17.1 us -> 11.7 us  [exchange(): return lax.all_to_all(array, axis, split_axis=0, concat_axis=0, tiled=True)]
    reshape x4 -> x0, local copies, waits for them, and re-layouts: 4.55 us -> none  [the longest x1 1.83 us: shards(): returned = exchange(back.reshape(sp_count, slots // sp_count, width), SP)]
    pallas_call x1 -> x2, Pallas kernels: 7.31 us -> 7.78 us  [the longest x1 5.78 us: experts(): pl.pallas_call(expert_body, out_shape=(jax.ShapeDtypeStruct((rows, width)...]
  transfers between devices with their start and end apart: 5 -> 7, of which waited for: 4 -> 6; matrix products, arithmetic and copies ran while one was open for 2% -> 2% of each run, Pallas kernels for 6% -> 6%
where the time goes in v3:
time: 264 us; the launch traced here: 263 us
  blocking collectives  75.7 us (29%)
  starting transfers between devices  71.2 us (27%)
  waiting for transfers between devices  64.1 us (24%)
  Pallas kernels  28.8 us (11%)
  between operations  13.5 us (5%)
  local copies, waits for them, and re-layouts  9.37 us (4%)
    all_to_all x3, blocking collectives, exchange(): return lax.all_to_all(array, axis, split_axis=0, concat_axis=0, tiled=True)  75.7 us
    all_to_all x2, waiting for transfers between devices, exchange(): return lax.all_to_all(array, axis, split_axis=0, concat_axis=0, tiled=True)  49.2 us
    ppermute x1, starting transfers between devices, shards(): pay_other = lax.ppermute(pay, 'sp_1', swap)  43.4 us
    all_to_all x2, starting transfers between devices, exchange(): return lax.all_to_all(array, axis, split_axis=0, concat_axis=0, tiled=True)  11.7 us
    ppermute x1, starting transfers between devices, shards(): carried_other = lax.ppermute(carried, 'sp_1', swap)  8.55 us
    ppermute x1, waiting for transfers between devices, shards(): received_other = lax.ppermute(received, 'grp', partner)  6.08 us
    pallas_call x1, Pallas kernels, experts(): pl.pallas_call(expert_body, out_shape=(jax.ShapeDtypeStruct((rows, width)...  5.78 us
    ppermute x1, waiting for transfers between devices, shards(): back = finish(mine, lax.ppermute(send, 'grp', partner), sp_count)  5.71 us
  transfers between devices with their start and end apart: 7, of which 6 were waited for; matrix products, arithmetic and copies ran while one was open for 2% of the time, Pallas kernels for 6%

profile of v3, /device:TPU:65, one launch (start us, length us, event | category | flops | bytes accessed | tf_op | source)
XLA Modules:
  0.0 262.6 jit_solution(17077314170107313892)
XLA Ops:
  6.5 0.0 all-gather.3.cloned.1.call-start
  6.6 2.8 %pack_weights.1 = bf16[3072,128]{1,0:T(8,128)(2,1)} custom-call(s32[1]{0:T(128)} %bitcast.7.part_ref, bf16[1,2048,128]{2,1,0:T(8,128)(2,1)} %gate_ref.1, bf16[1,2048,128]{2,1,0:T(8,128)(2,1)} %up_ref.1, bf16[1,128,2048]{2,1,0:T(8,128)(2,1)} %down_ref.1), custom_call_target="tpu_custom_call" | custom-call | tf_op jit(solution)/shard_map/pack_weights/pallas_call | solution.py:481
  9.3 0.1 all-gather.3.cloned.1.call-update
  9.4 0.7 slice_bitcast_fusion.2
  10.1 0.7 slice_bitcast_fusion
  10.8 0.6 concatenate.3.dec_ref
  11.4 1.3 dynamic-slice_bitcast_fusion.base_ref
  12.7 0.0 copy-start.10
  12.7 0.0 copy-start.9
  12.7 3.6 %retention_local.1 = (bf16[256,256]{1,0:T(8,128)(2,1)}, bf16[256,128]{1,0:T(8,128)(2,1)}, f32[256,640]{1,0:T(8,128)}, bf16[2,288,512]{2,1,0:T(8,128)(2,1)}) custom-call(bf16[256,256]{1,0:T(8,128)(2,1)} %qa_ref.1, bf16[256,256]{1,0:T(8,128)(2,1)} %ka_ref.1, bf16[256,512]{1,0:T(8,128)(2,1)} %va_ref.1, bf16[256,128]{1,0:T(8,128)(2,1)} %qb_ref.1, ...), custom_call_target="tpu_custom_call" | custom-call | tf_op jit(solution)/shard_map/retention_local/pallas_call | solution.py:169
  16.3 43.4 %collective-permute-start = (bf16[2,288,512]{2,1,0:T(8,128)(2,1)}, bf16[2,288,512]{2,1,0:T(8,128)(2,1)S(1)}, u32[]{:S(2)}, u32[]{:S(2)}) collective-permute-start(bf16[2,288,512]{2,1,0:T(8,128)(2,1)} %get-tuple-element.16.own_ref), channel_id=1, source_target_pairs={{0,8},{8,0},{1,9},{9,1},{2,10},{10,2},{3,11},{11,3},{4,12},{12,4},... | collective-permute-start | bytes 1769480 | tf_op jit(solution)/shard_map/ppermute | solution.py:650
  59.6 1.8 collective-permute-done.oth_ref.pay_ref
  61.5 0.0 copy-start.1
  61.5 0.8 copy-done.1
  62.3 2.2 pack_states.1
  64.5 20.6 %all_to_all.25.refs_1_ = bf16[16,80,128]{2,1,0:T(8,128)(2,1)} all-to-all(bf16[16,80,128]{2,1,0:T(8,128)(2,1)} %pack_states.1), channel_id=1, replica_groups=mesh['grp'=2,'sp_0'=16,'sp_1'=2,'tp'=8] {'sp_0'}, dimensions={0} | all-to-all | bytes 655360 | tf_op jit(solution)/shard_map/all_to_all | solution.py:613
  85.1 1.8 scan_states.1
  87.0 26.1 %all_to_all.26.own_ref = bf16[16,80,128]{2,1,0:T(8,128)(2,1)S(1)} all-to-all(bf16[16,80,128]{2,1,0:T(8,128)(2,1)} %scan_states.1), channel_id=1, replica_groups=mesh['grp'=2,'sp_0'=16,'sp_1'=2,'tp'=8] {'sp_0'}, dimensions={0} | all-to-all | bytes 655360 | tf_op jit(solution)/shard_map/all_to_all | solution.py:613
  113.1 8.5 %collective-permute-start.1 = (bf16[16,80,128]{2,1,0:T(8,128)(2,1)S(1)}, bf16[16,80,128]{2,1,0:T(8,128)(2,1)S(1)}, u32[]{:S(2)}, u32[]{:S(2)}) collective-permute-start(bf16[16,80,128]{2,1,0:T(8,128)(2,1)S(1)} %all_to_all.26.own_ref), channel_id=1, source_target_pairs={{0,8},{8,0},{1,9},{9,1},{2,10},{10,2},{3,11},{11,3},{4,12},{12,4},... | collective-permute-start | bytes 983048 | tf_op jit(solution)/shard_map/ppermute | solution.py:654
  121.6 1.2 collective-permute-done.1.oth_ref
  122.9 0.0 copy-done.2
  122.9 0.7 copy-done.5
  123.6 5.4 %mix_project.1 = bf16[256,2048]{1,0:T(8,128)(2,1)} custom-call(s32[1]{0:T(128)} %bitcast.core_ref.refs_0_, bf16[256,256]{1,0:T(8,128)(2,1)} %get-tuple-element.13.qa_ref, bf16[256,128]{1,0:T(8,128)(2,1)} %get-tuple-element.14.qb_ref, f32[256,640]{1,0:T(8,128)} %get-tuple-element.15.loc_ref, bf16[16,80,128]{2,1,0:T(8,128)(2,1)} %copy-done.2, ...), custom_call_target="tpu_custom_call" | custom-call | tf_op jit(solution)/shard_map/mix_project/pallas_call | solution.py:385
  129.0 6.0 %all-to-all-start.2 = ((bf16[8,32,2048]{2,1,0:T(8,128)(2,1)}), bf16[8,32,2048]{2,1,0:T(8,128)(2,1)S(1)}, u32[]{:S(2)}, u32[]{:S(2)}) async-start(bf16[8,32,2048]{2,1,0:T(8,128)(2,1)} %bitcast.15), calls=%async_computation.2 | async-start | bytes 2097152 | tf_op jit(solution)/shard_map/all_to_all | solution.py:613
  135.0 0.0 copy-done.10
  135.0 0.0 copy-done.9
  135.0 0.1 copy.23
  135.1 0.6 reshape.19.ids_ref
  135.8 28.5 %all-to-all-done.2.arr_ref = bf16[8,32,2048]{2,1,0:T(8,128)(2,1)S(1)} async-done(((bf16[8,32,2048]{2,1,0:T(8,128)(2,1)}), bf16[8,32,2048]{2,1,0:T(8,128)(2,1)S(1)}, u32[]{:S(2)}, u32[]{:S(2)}) %all-to-all-start.2) | async-done | bytes 1048608 | tf_op jit(solution)/shard_map/all_to_all | solution.py:613
  164.2 1.0 copy-done
  165.2 2.7 %dispatch.1 = (bf16[32,2048]{1,0:T(8,128)(2,1)}, bf16[32,32,128]{2,1,0:T(8,128)(2,1)}) custom-call(bf16[8,32,2048]{2,1,0:T(8,128)(2,1)} %copy-done, bf16[32,2048]{1,0:T(8,128)(2,1)} %res_ref.1, f32[2,2048]{1,0:T(2,128)} %gain_ref.3, s32[1,64]{1,0:T(1,128)} %reshape.19.ids_ref), custom_call_target="tpu_custom_call" | custom-call | tf_op jit(solution)/shard_map/dispatch/pallas_call | solution.py:447
  167.9 28.9 %all_to_all.27.own_ref = bf16[32,32,128]{2,1,0:T(8,128)(2,1)S(1)} all-to-all(bf16[32,32,128]{2,1,0:T(8,128)(2,1)} %get-tuple-element.17), channel_id=1, replica_groups=mesh['grp'=2,'sp_0'=16,'sp_1'=2,'tp'=8] {'sp_0','sp_1'}, dimensions={0} | all-to-all | bytes 524288 | tf_op jit(solution)/shard_map/all_to_all | solution.py:613
  196.8 4.4 %collective-permute-start.2 = (bf16[32,32,128]{2,1,0:T(8,128)(2,1)S(1)}, bf16[32,32,128]{2,1,0:T(8,128)(2,1)S(1)}, u32[]{:S(2)}, u32[]{:S(2)}) collective-permute-start(bf16[32,32,128]{2,1,0:T(8,128)(2,1)S(1)} %all_to_all.27.own_ref), channel_id=1, source_target_pairs={{0,256},{256,0},{1,257},{257,1},{2,258},{258,2},{3,259},{259,3},{4... | collective-permute-start | bytes 786440 | tf_op jit(solution)/shard_map/ppermute | solution.py:662
  201.3 6.1 %collective-permute-done.2.oth_ref = bf16[32,32,128]{2,1,0:T(8,128)(2,1)S(1)} collective-permute-done((bf16[32,32,128]{2,1,0:T(8,128)(2,1)S(1)}, bf16[32,32,128]{2,1,0:T(8,128)(2,1)S(1)}, u32[]{:S(2)}, u32[]{:S(2)}) %collective-permute-start.2) | collective-permute-done | bytes 262176 | tf_op jit(solution)/shard_map/ppermute | solution.py:662
  207.4 0.0 copy-done.4
  207.4 0.7 copy-done.7
  208.0 5.8 %experts.1 = (f32[64,2048]{1,0:T(8,128)}, bf16[64,2048]{1,0:T(8,128)(2,1)}) custom-call(bf16[32,32,128]{2,1,0:T(8,128)(2,1)} %copy-done.4, bf16[32,32,128]{2,1,0:T(8,128)(2,1)} %copy-done.7, bf16[8,3072,128]{2,1,0:T(8,128)(2,1)} %bitcast.14), custom_call_target="tpu_custom_call" | custom-call | tf_op jit(solution)/shard_map/experts/pallas_call | solution.py:547
  213.8 3.1 %collective-permute-start.3 = (bf16[64,2048]{1,0:T(8,128)(2,1)}, bf16[64,2048]{1,0:T(8,128)(2,1)S(1)}, u32[]{:S(2)}, u32[]{:S(2)}) collective-permute-start(bf16[64,2048]{1,0:T(8,128)(2,1)} %get-tuple-element.19), channel_id=1, source_target_pairs={{0,256},{256,0},{1,257},{257,1},{2,258},{258,2},{3,259},{259,3},{4... | collective-permute-start | bytes 786440 | tf_op jit(solution)/shard_map/ppermute | solution.py:664
  216.9 5.7 %collective-permute-done.3.arrived_ref = bf16[64,2048]{1,0:T(8,128)(2,1)S(1)} collective-permute-done((bf16[64,2048]{1,0:T(8,128)(2,1)}, bf16[64,2048]{1,0:T(8,128)(2,1)S(1)}, u32[]{:S(2)}, u32[]{:S(2)}) %collective-permute-start.3) | collective-permute-done | bytes 262176 | tf_op jit(solution)/shard_map/ppermute | solution.py:664
  222.7 0.7 copy-done.6
  223.4 2.0 finish.1
  225.3 5.8 %all-to-all-start.4 = ((bf16[32,32,128]{2,1,0:T(8,128)(2,1)}), bf16[32,32,128]{2,1,0:T(8,128)(2,1)S(1)}, u32[]{:S(2)}, u32[]{:S(2)}) async-start(bf16[32,32,128]{2,1,0:T(8,128)(2,1)} %finish.1), calls=%async_computation.4 | async-start | bytes 524288 | tf_op jit(solution)/shard_map/all_to_all | solution.py:613
  231.1 0.0 copy-done.8
  231.2 0.1 copy.24
  231.2 0.6 reshape.21.w_ref
  231.9 20.7 %all-to-all-done.4.ret_ref = bf16[32,32,128]{2,1,0:T(8,128)(2,1)S(1)} async-done(((bf16[32,32,128]{2,1,0:T(8,128)(2,1)}), bf16[32,32,128]{2,1,0:T(8,128)(2,1)S(1)}, u32[]{:S(2)}, u32[]{:S(2)}) %all-to-all-start.4) | async-done | bytes 262176 | tf_op jit(solution)/shard_map/all_to_all | solution.py:613
  252.6 0.7 copy-done.3
  253.3 2.5 combine.1
  (12 shorter events, 0.0 us)
Async XLA Ops:
  6.5 200.8 %all-gather.3.cloned.1.call-start = ((), (), s32[]{:S(2)}) async-start(), calls=%async_computation.5 | async-start | bytes 7077888 | tf_op jit(solution)/shard_map/all_gather | solution.py:636
  12.7 122.3 %copy-start.10 = (s32[32]{0:T(128)S(1)}, s32[32]{0:T(128)}, u32[]{:S(2)}) copy-start(s32[32]{0:T(128)} %param.32) | copy-start | bytes 388
  12.7 122.3 %copy-start.9 = (s32[32,2]{0,1:T(2,128)S(1)}, s32[32,2]{0,1:T(2,128)}, u32[]{:S(2)}) copy-start(s32[32,2]{0,1:T(2,128)} %param.33) | copy-start | bytes 772
  16.3 45.2 %collective-permute-start = (bf16[2,288,512]{2,1,0:T(8,128)(2,1)}, bf16[2,288,512]{2,1,0:T(8,128)(2,1)S(1)}, u32[]{:S(2)}, u32[]{:S(2)}) collective-permute-start(bf16[2,288,512]{2,1,0:T(8,128)(2,1)} %get-tuple-element.16.own_ref), channel_id=1, source_target_pairs={{0,8},{8,0},{1,9},{9,1},{2,10},{10,2},{3,11},{11,3},{4,12},{12,4},... | collective-permute-start | bytes 1769480 | tf_op jit(solution)/shard_map/ppermute | solution.py:650
  61.5 0.8 copy-start.1
  113.1 9.8 %copy-start.2 = (bf16[16,80,128]{2,1,0:T(8,128)(2,1)}, bf16[16,80,128]{2,1,0:T(8,128)(2,1)S(1)}, u32[]{:S(2)}) copy-start(bf16[16,80,128]{2,1,0:T(8,128)(2,1)S(1)} %all_to_all.26.own_ref) | copy-start | bytes 983044
  113.1 9.8 %collective-permute-start.1 = (bf16[16,80,128]{2,1,0:T(8,128)(2,1)S(1)}, bf16[16,80,128]{2,1,0:T(8,128)(2,1)S(1)}, u32[]{:S(2)}, u32[]{:S(2)}) collective-permute-start(bf16[16,80,128]{2,1,0:T(8,128)(2,1)S(1)} %all_to_all.26.own_ref), channel_id=1, source_target_pairs={{0,8},{8,0},{1,9},{9,1},{2,10},{10,2},{3,11},{11,3},{4,12},{12,4},... | collective-permute-start | bytes 983048 | tf_op jit(solution)/shard_map/ppermute | solution.py:654
  122.9 0.7 copy-start.5
  129.0 102.1 %copy-start.8 = (f32[32,2]{0,1:T(2,128)S(1)}, f32[32,2]{0,1:T(2,128)}, u32[]{:S(2)}) copy-start(f32[32,2]{0,1:T(2,128)} %param.34) | copy-start | bytes 772
  129.0 35.2 %all-to-all-start.2 = ((bf16[8,32,2048]{2,1,0:T(8,128)(2,1)}), bf16[8,32,2048]{2,1,0:T(8,128)(2,1)S(1)}, u32[]{:S(2)}, u32[]{:S(2)}) async-start(bf16[8,32,2048]{2,1,0:T(8,128)(2,1)} %bitcast.15), calls=%async_computation.2 | async-start | bytes 2097152 | tf_op jit(solution)/shard_map/all_to_all | solution.py:613
  164.2 1.0 copy-start
  196.8 10.5 %copy-start.4 = (bf16[32,32,128]{2,1,0:T(8,128)(2,1)}, bf16[32,32,128]{2,1,0:T(8,128)(2,1)S(1)}, u32[]{:S(2)}) copy-start(bf16[32,32,128]{2,1,0:T(8,128)(2,1)S(1)} %all_to_all.27.own_ref) | copy-start | bytes 786436
  196.8 10.5 %collective-permute-start.2 = (bf16[32,32,128]{2,1,0:T(8,128)(2,1)S(1)}, bf16[32,32,128]{2,1,0:T(8,128)(2,1)S(1)}, u32[]{:S(2)}, u32[]{:S(2)}) collective-permute-start(bf16[32,32,128]{2,1,0:T(8,128)(2,1)S(1)} %all_to_all.27.own_ref), channel_id=1, source_target_pairs={{0,256},{256,0},{1,257},{257,1},{2,258},{258,2},{3,259},{259,3},{4... | collective-permute-start | bytes 786440 | tf_op jit(solution)/shard_map/ppermute | solution.py:662
  207.4 0.7 copy-start.7
  213.8 8.8 %collective-permute-start.3 = (bf16[64,2048]{1,0:T(8,128)(2,1)}, bf16[64,2048]{1,0:T(8,128)(2,1)S(1)}, u32[]{:S(2)}, u32[]{:S(2)}) collective-permute-start(bf16[64,2048]{1,0:T(8,128)(2,1)} %get-tuple-element.19), channel_id=1, source_target_pairs={{0,256},{256,0},{1,257},{257,1},{2,258},{258,2},{3,259},{259,3},{4... | collective-permute-start | bytes 786440 | tf_op jit(solution)/shard_map/ppermute | solution.py:664
  222.7 0.7 copy-start.6
  225.3 27.2 %all-to-all-start.4 = ((bf16[32,32,128]{2,1,0:T(8,128)(2,1)}), bf16[32,32,128]{2,1,0:T(8,128)(2,1)S(1)}, u32[]{:S(2)}, u32[]{:S(2)}) async-start(bf16[32,32,128]{2,1,0:T(8,128)(2,1)} %finish.1), calls=%async_computation.4 | async-start | bytes 524288 | tf_op jit(solution)/shard_map/all_to_all | solution.py:613
  252.6 0.7 copy-start.3
Sparse Core Ops, SparseCore 0:
  9.5 114.8 all-gather.2

commit v4 on v3

--- a/solution.py
+++ b/solution.py
@@ -28,13 +28,27 @@
 
 LANES = 128
 TILE = 16
+SIDE = 8
 
 
 def vmem(count):
     return [pl.BlockSpec(memory_space=pltpu.VMEM)] * count
 
 
+def near(array):
+    return array if INTERPRET else pltpu.with_memory_space_constraint(array, pltpu.VMEM)
+
+
+def far(array):
+    return array if INTERPRET else pltpu.with_memory_space_constraint(array, pltpu.HBM)
+
+
+def near_shape(shape, dtype):
+    return jax.ShapeDtypeStruct(shape, dtype) if INTERPRET else pltpu.VMEM(shape, dtype)
+
+
 SMEM_SPEC = pl.BlockSpec(memory_space=pltpu.SMEM)
+PARAMS = pltpu.CompilerParams(vmem_limit_bytes=20 << 20)
 ANY_SPEC = pl.BlockSpec(memory_space=pl.ANY)
 
 
@@ -78,8 +92,8 @@
 
 
 def retention_body(
-    qa_ref, ka_ref, va_ref, qb_ref, kb_ref, vb_ref, dec_ref, tab_ref, base_ref,
-    qa_out, qb_out, loc_out, pay_out,
+    index_ref, qa_ref, ka_ref, va_ref, qb_ref, kb_ref, vb_ref, da_ref, db_ref, tab_ref, base_ref,
+    qa_out, qb_out, loc_out, pay_out, dec_out,
 ):
     n, dk = qa_ref.shape
     dv = va_ref.shape[1]
@@ -87,7 +101,11 @@
     hb = qb_ref.shape[1] // 2
     hq = hb // 2
     row, col = iota((n, n), 0), iota((n, n), 1)
-    dec = dec_ref[...]
+    for d in range(2):
+        dec_out[3 * d : 3 * d + 1, :] = da_ref[d]
+        dec_out[3 * d + 1 : 3 * d + 3, :] = db_ref[d]
+    dec_out[6:8, :] = jnp.zeros((2, n), F32)
+    dec = dec_out[...]
     cr = jnp.dot(dec, (row <= col).astype(F32), precision=HIGHEST, preferred_element_type=F32)
     cc = mm_nt((col <= row).astype(F32), dec, HIGHEST)
     er = cr - dec
@@ -99,7 +117,7 @@
         backward = er[3 + h : 4 + h, :] - ec[:, 3 + h : 4 + h]
         return jnp.exp(jnp.where(col <= row, forward, backward))
 
-    base = base_ref[...]
+    base = base_ref[index_ref[0]]
     cos_a = tab_ref[0] * base[0:1] - tab_ref[1] * base[1:2]
     sin_a = tab_ref[1] * base[0:1] + tab_ref[0] * base[1:2]
 
@@ -163,22 +181,24 @@
     loc_out[:, dv:] = acc
 
 
-def retention_local(qa, ka, va, qb, kb, vb, dec, tab, base):
+def retention_local(index, qa, ka, va, qb, kb, vb, da, db, tab, base):
     n, dk = qa.shape
     dv, wb = va.shape[1], vb.shape[1]
     return pl.pallas_call(
         retention_body,
         out_shape=(
-            jax.ShapeDtypeStruct((n, dk), BF16),
-            jax.ShapeDtypeStruct((n, wb), BF16),
-            jax.ShapeDtypeStruct((n, dv + wb), F32),
-            jax.ShapeDtypeStruct((2, dk + 2 * TILE, dv), BF16),
+            near_shape((n, dk), BF16),
+            near_shape((n, wb), BF16),
+            near_shape((n, dv + wb), F32),
+            near_shape((2, dk + 2 * TILE, dv), BF16),
+            near_shape((8, n), F32),
         ),
-        in_specs=vmem(9),
-        out_specs=tuple(vmem(4)),
-        interpret=INTERPRET,
+        in_specs=[SMEM_SPEC] + vmem(10),
+        out_specs=tuple(vmem(5)),
+        interpret=INTERPRET,
+        compiler_params=PARAMS,
         name="retention_local",
-    )(qa, ka, va, qb, kb, vb, dec, tab, base)
+    )(index, *map(far, (qa, ka, va, qb, kb, vb, da, db, tab, base)))
 
 
 def log_rows(ref, d, dk):
@@ -231,52 +251,68 @@
         part = jnp.where(first, part[0], part[1])
         for k in range(TILE // per):
             ext_scr[q * (TILE // per) + k, 0:per, :] = part[k * per : (k + 1) * per]
-    rows = iota((TILE - per, LANES), 0)
-    logs = jnp.zeros((TILE - per, LANES), F32)
+    quarter = lane // (LANES // 4)
+
+    def quarters(values):
+        out = values[0]
+        for k in range(1, len(values)):
+            out = jnp.where(quarter == k, values[k], out)
+        return out
+
     sums_f = [x + y for x, y in zip(own_f, oth_f)]
     sums_b = [x + y for x, y in zip(own_b, oth_b)]
-    for k, value in enumerate(
-        [
-            sums_f[0],
-            sums_b[0],
-            jnp.where(left, sums_f[1], sums_f[2]),
-            jnp.where(left, sums_b[1], sums_b[2]),
-        ]
-    ):
-        hi, lo = split2(value)
-        logs = jnp.where(rows == 2 * k, hi, jnp.where(rows == 2 * k + 1, lo, logs))
-    ext_scr[:, per:, :] = jnp.broadcast_to(logs[None], (chips, TILE - per, LANES))
+    lines = [
+        *split2(quarters([sums_f[1], sums_f[2], sums_f[0], sums_b[0]])),
+        *split2(quarters([sums_b[1], sums_b[2]])),
+    ]
+    for k, line in enumerate(lines):
+        ext_scr[:, per + k : per + k + 1, :] = jnp.broadcast_to(line[None], (chips, 1, LANES))
     at = 2 * blocks * step
-    out_ref[:, at : at + TILE, :] = ext_scr[...].astype(BF16)
+    out_ref[:, at : at + SIDE, :] = ext_scr[...].astype(BF16)
 
 
 def pack_states(core, own, other, chips):
     dv = own.shape[2]
     dk = own.shape[1] - 2 * TILE
-    rows = dv // LANES * (dk // chips) + TILE
+    rows = dv // LANES * (dk // chips) + SIDE
     return pl.pallas_call(
         pack_body,
-        out_shape=jax.ShapeDtypeStruct((chips, rows, LANES), BF16),
+        out_shape=near_shape((chips, rows, LANES), BF16),
         in_specs=[SMEM_SPEC] + vmem(2),
         out_specs=vmem(1)[0],
-        scratch_shapes=[pltpu.VMEM((chips, TILE, LANES), F32)],
-        interpret=INTERPRET,
+        scratch_shapes=[pltpu.VMEM((chips, SIDE, LANES), F32)],
+        interpret=INTERPRET,
+        compiler_params=PARAMS,
         name="pack_states",
-    )(core, own, other)
+    )(core, near(own), near(other))
 
 
 def scan_body(per, core_ref, in_ref, out_ref):
     chips, rows, _ = in_ref.shape
-    main = rows - TILE
+    main = rows - SIDE
     side = main // 2
     first = core_ref[0] == 0
+    left = iota((1, LANES), 1) < LANES // 2
     ext = [in_ref[i, main:, :].astype(F32) for i in range(chips)]
-    decays = [
-        [jnp.exp(e[per + 2 * k : per + 2 * k + 1] + e[per + 2 * k + 1 : per + 2 * k + 2]) for k in range(4)]
-        for e in ext
-    ]
+    decays = []
+    for e in ext:
+        one = jnp.exp(e[per : per + 1] + e[per + 1 : per + 2])
+        two = jnp.exp(e[per + 2 : per + 3] + e[per + 3 : per + 4])
+
+        def lane(line, k):
+            at = k * (LANES // 4)
+            return line[:, at : at + 1]
+
+        decays.append(
+            [
+                lane(one, 2),
+                lane(one, 3),
+                jnp.where(left, lane(one, 0), lane(one, 1)),
+                jnp.where(left, lane(two, 0), lane(two, 1)),
+            ]
+        )
     carry = jnp.zeros((side, LANES), F32)
-    group = jnp.zeros((TILE, LANES), F32)
+    group = jnp.zeros((SIDE, LANES), F32)
     into = []
     for i in range(chips):
         out_ref[i, :side, :] = carry.astype(BF16)
@@ -284,7 +320,7 @@
         carry = decays[i][0] * carry + in_ref[i, :side, :].astype(F32)
         group = decays[i][2] * group + ext[i]
     carry = jnp.zeros((side, LANES), F32)
-    group = jnp.zeros((TILE, LANES), F32)
+    group = jnp.zeros((SIDE, LANES), F32)
     for i in reversed(range(chips)):
         out_ref[i, side:main, :] = carry.astype(BF16)
         out_ref[i, main:, :] = jnp.where(first, into[i], group).astype(BF16)
@@ -298,12 +334,13 @@
 
     return pl.pallas_call(
         body,
-        out_shape=jax.ShapeDtypeStruct(pieces.shape, BF16),
+        out_shape=near_shape(pieces.shape, BF16),
         in_specs=[SMEM_SPEC] + vmem(1),
         out_specs=vmem(1)[0],
         interpret=INTERPRET,
+        compiler_params=PARAMS,
         name="scan_states",
-    )(core, pieces)
+    )(core, near(pieces))
 
 
 def mix_body(
@@ -317,7 +354,7 @@
     chips, rows, _ = own_ref.shape
     step = dk // chips
     blocks = dv // LANES // 2
-    main = rows - TILE
+    main = rows - SIDE
     first = core_ref[0] == 0
     row, col = iota((n, n), 0), iota((n, n), 1)
     dec = dec_ref[...]
@@ -384,13 +421,14 @@
     hb = qb.shape[1] // 2
     return pl.pallas_call(
         mix_body,
-        out_shape=jax.ShapeDtypeStruct((qa.shape[0], wa.shape[1]), BF16),
+        out_shape=near_shape((qa.shape[0], wa.shape[1]), BF16),
         in_specs=[SMEM_SPEC] + vmem(9),
         out_specs=vmem(1)[0],
         scratch_shapes=[pltpu.VMEM((hb, qb.shape[1]), F32)],
         interpret=INTERPRET,
+        compiler_params=PARAMS,
         name="mix_project",
-    )(core, qa, qb, loc, own, other, pay, dec, wa, wb)
+    )(core, *map(near, (qa, qb, loc, own, other, pay, dec)), wa, wb)
 
 
 def layer_norm(stream, gain):
@@ -447,15 +485,16 @@
     return pl.pallas_call(
         dispatch_body,
         out_shape=(
-            jax.ShapeDtypeStruct((rows, width), BF16),
-            jax.ShapeDtypeStruct((peers, lines // peers, LANES), BF16),
+            near_shape((rows, width), BF16),
+            near_shape((peers, lines // peers, LANES), BF16),
         ),
         in_specs=vmem(4),
         out_specs=tuple(vmem(2)),
         scratch_shapes=[pltpu.VMEM((lines, LANES), F32)],
         interpret=INTERPRET,
+        compiler_params=PARAMS,
         name="dispatch",
-    )(arrived, residual, gain, ids)
+    )(near(arrived), residual, gain, ids)
 
 
 def pack_weights_body(part_ref, gate_ref, up_ref, down_ref, out_ref):
@@ -484,8 +523,9 @@
         in_specs=[SMEM_SPEC] + vmem(3),
         out_specs=vmem(1)[0],
         interpret=INTERPRET,
+        compiler_params=PARAMS,
         name="pack_weights",
-    )(part, gate, up, down)
+    )(part, far(gate), far(up), far(down))
 
 
 def expert_body(own_ref, oth_ref, w_ref, mine_ref, send_ref, x_scr, w_scr, acc_ref, sems):
@@ -547,8 +587,8 @@
     return pl.pallas_call(
         expert_body,
         out_shape=(
-            jax.ShapeDtypeStruct((rows, width), F32),
-            jax.ShapeDtypeStruct((rows, width), BF16),
+            near_shape((rows, width), F32),
+            near_shape((rows, width), BF16),
         ),
         in_specs=vmem(2) + [ANY_SPEC],
         out_specs=tuple(vmem(2)),
@@ -559,8 +599,9 @@
             pltpu.SemaphoreType.DMA((count,)),
         ],
         interpret=INTERPRET,
+        compiler_params=PARAMS,
         name="experts",
-    )(own, other, weights)
+    )(near(own), near(other), far(weights))
 
 
 def finish_body(mine_ref, arrived_ref, out_ref, scr):
@@ -572,13 +613,14 @@
     lines = rows * width // LANES
     return pl.pallas_call(
         finish_body,
-        out_shape=jax.ShapeDtypeStruct((peers, lines // peers, LANES), BF16),
+        out_shape=near_shape((peers, lines // peers, LANES), BF16),
         in_specs=vmem(2),
         out_specs=vmem(1)[0],
         scratch_shapes=[pltpu.VMEM((lines, LANES), F32)],
         interpret=INTERPRET,
+        compiler_params=PARAMS,
         name="finish",
-    )(mine, arrived)
+    )(near(mine), near(arrived))
 
 
 def combine_body(ret_ref, hid_ref, gain_ref, ids_ref, w_ref, out_ref, scr):
@@ -605,19 +647,13 @@
         out_specs=vmem(1)[0],
         scratch_shapes=[pltpu.VMEM((lines, LANES), F32)],
         interpret=INTERPRET,
+        compiler_params=PARAMS,
         name="combine",
-    )(returned, hidden, gain, ids, weights)
+    )(near(returned), near(hidden), gain, ids, weights)
 
 
 def exchange(array, axis):
     return lax.all_to_all(array, axis, split_axis=0, concat_axis=0, tiled=True)
-
-
-def decay_rows(decay_a, decay_b):
-    length = decay_a.shape[-1]
-    return jnp.concatenate(
-        [decay_a[0], decay_b[0], decay_a[1], decay_b[1], jnp.zeros((2, length), F32)], axis=0
-    )
 
 
 def shards(
@@ -641,10 +677,10 @@
     local, base = angle_tables(
         length, query_a.shape[1] // 2, query_b.shape[1] // 4, sp_count
     )
-    base = lax.dynamic_index_in_dim(jnp.asarray(base), lax.axis_index(SP), 0, keepdims=False)
-    dec = decay_rows(decay_a, decay_b)
-    qa, qb, loc, pay = retention_local(
-        query_a, key_a, value_a, query_b, key_b, value_b, dec, jnp.asarray(local), base
+    index = lax.axis_index(SP).astype(jnp.int32).reshape(1)
+    qa, qb, loc, pay, dec = retention_local(
+        index, query_a, key_a, value_a, query_b, key_b, value_b, decay_a, decay_b,
+        jnp.asarray(local), jnp.asarray(base),
     )
     swap = [(0, 1), (1, 0)]
     pay_other = lax.ppermute(pay, "sp_1", swap)

time: 264 us -> 243 us (0.920)
  Pallas kernels: 28.8 us -> 16.2 us
  local copies, waits for them, and re-layouts: 9.37 us -> 0.42 us
    pallas_call x7, Pallas kernels: 23.6 us -> 11.8 us  [the longest x1 3.85 us: experts(): pl.pallas_call(expert_body, out_shape=(near_shape((rows, width), F32), ne...]
    unnamed x23 -> x15, local copies, waits for them, and re-layouts: 4.71 us -> 0.12 us
    squeeze x3 -> x0, local copies, waits for them, and re-layouts: 2.68 us -> none  [the longest x1 1.28 us: shards(): lax.dynamic_index_in_dim(jnp.asarray(base), lax.axis_index(SP), 0, keepdi...]
  transfers between devices with their start and end apart: 7 -> 7, of which waited for: 6 -> 6; matrix products, arithmetic and copies ran while one was open for 2% -> 0% of each run, Pallas kernels for 6% -> 3%
where the time goes in v4:
time: 243 us; the launch traced here: 241 us
  blocking collectives  78 us (32%)
  starting transfers between devices  71.2 us (29%)
  waiting for transfers between devices  61.8 us (25%)
  Pallas kernels  16.2 us (7%)
  between operations  13.6 us (6%)
    all_to_all x3, blocking collectives, exchange(): return lax.all_to_all(array, axis, split_axis=0, concat_axis=0, tiled=True)  78 us
    all_to_all x2, waiting for transfers between devices, exchange(): return lax.all_to_all(array, axis, split_axis=0, concat_axis=0, tiled=True)  47.9 us
    ppermute x1, starting transfers between devices, shards(): pay_other = lax.ppermute(pay, 'sp_1', swap)  43.4 us
    all_to_all x2, starting transfers between devices, exchange(): return lax.all_to_all(array, axis, split_axis=0, concat_axis=0, tiled=True)  13.2 us
    ppermute x1, starting transfers between devices, shards(): carried_other = lax.ppermute(carried, 'sp_1', swap)  8.12 us
    ppermute x1, waiting for transfers between devices, shards(): received_other = lax.ppermute(received, 'grp', partner)  5.97 us
    ppermute x1, waiting for transfers between devices, shards(): back = finish(mine, lax.ppermute(send, 'grp', partner), sp_count)  5.11 us
  transfers between devices with their start and end apart: 7, of which 6 were waited for; matrix products, arithmetic and copies ran while one was open for 0% of the time, Pallas kernels for 3%

profile of v4, /device:TPU:65, one launch (start us, length us, event | category | flops | bytes accessed | tf_op | source)
XLA Modules:
  0.0 241.1 jit_solution(12711330807369273491)
XLA Ops:
  6.5 0.0 copy-start
  6.5 0.0 copy-start.1
  6.6 0.0 all-gather.3.cloned.1.call-start
  6.6 2.9 %pack_weights.1 = bf16[3072,128]{1,0:T(8,128)(2,1)} custom-call(s32[1]{0:T(128)} %bitcast.3.part_ref, bf16[1,2048,128]{2,1,0:T(8,128)(2,1)} %gate_ref.1, bf16[1,2048,128]{2,1,0:T(8,128)(2,1)} %up_ref.1, bf16[1,128,2048]{2,1,0:T(8,128)(2,1)} %down_ref.1), custom_call_target="tpu_custom_call" | custom-call | tf_op jit(solution)/shard_map/pack_weights/pallas_call | solution.py:520
  9.4 0.1 all-gather.3.cloned.1.call-update
  9.5 0.0 copy-start.6
  9.5 0.0 copy-start.5
  9.5 0.0 copy-start.2
  9.5 0.0 copy-start.3
  9.6 2.8 %retention_local.1 = (bf16[256,256]{1,0:T(8,128)(2,1)S(1)}, bf16[256,128]{1,0:T(8,128)(2,1)S(1)}, f32[256,640]{1,0:T(8,128)S(1)}, bf16[2,288,512]{2,1,0:T(8,128)(2,1)S(1)}, f32[8,256]{1,0:T(8,128)S(1)}) custom-call(s32[1]{0:T(128)} %bitcast.1.index_ref, bf16[256,256]{1,0:T(8,128)(2,1)} %qa_ref.1, bf16[256,256]{1,0:T(8,128)(2,1)} %ka_ref.1, ...), custom_call_target="tpu_custom_call" | custom-call | tf_op jit(solution)/shard_map/retention_local/pallas_call | solution.py:187
  12.4 43.4 %collective-permute-start = (bf16[2,288,512]{2,1,0:T(8,128)(2,1)S(1)}, bf16[2,288,512]{2,1,0:T(8,128)(2,1)S(1)}, u32[]{:S(2)}, u32[]{:S(2)}) collective-permute-start(bf16[2,288,512]{2,1,0:T(8,128)(2,1)S(1)} %get-tuple-element.17.own_ref), channel_id=1, source_target_pairs={{0,8},{8,0},{1,9},{9,1},{2,10},{10,2},{3,11},{11,3},{4,12},{12,4},... | collective-permute-start | bytes 1769480 | tf_op jit(solution)/shard_map/ppermute | solution.py:686
  55.8 1.6 collective-permute-done.oth_ref.pay_ref
  57.4 0.2 pack_states.1
  57.6 17.3 %all_to_all.25.refs_1_ = bf16[16,72,128]{2,1,0:T(8,128)(2,1)S(1)} all-to-all(bf16[16,72,128]{2,1,0:T(8,128)(2,1)S(1)} %pack_states.1), channel_id=1, replica_groups=mesh['grp'=2,'sp_0'=16,'sp_1'=2,'tp'=8] {'sp_0'}, dimensions={0} | all-to-all | bytes 589824 | tf_op jit(solution)/shard_map/all_to_all | solution.py:656
  74.9 0.2 scan_states.1
  75.2 25.6 %all_to_all.26.own_ref = bf16[16,72,128]{2,1,0:T(8,128)(2,1)S(1)} all-to-all(bf16[16,72,128]{2,1,0:T(8,128)(2,1)S(1)} %scan_states.1), channel_id=1, replica_groups=mesh['grp'=2,'sp_0'=16,'sp_1'=2,'tp'=8] {'sp_0'}, dimensions={0} | all-to-all | bytes 589824 | tf_op jit(solution)/shard_map/all_to_all | solution.py:656
  100.7 8.1 %collective-permute-start.1 = (bf16[16,72,128]{2,1,0:T(8,128)(2,1)S(1)}, bf16[16,72,128]{2,1,0:T(8,128)(2,1)S(1)}, u32[]{:S(2)}, u32[]{:S(2)}) collective-permute-start(bf16[16,72,128]{2,1,0:T(8,128)(2,1)S(1)} %all_to_all.26.own_ref), channel_id=1, source_target_pairs={{0,8},{8,0},{1,9},{9,1},{2,10},{10,2},{3,11},{11,3},{4,12},{12,4},... | collective-permute-start | bytes 884744 | tf_op jit(solution)/shard_map/ppermute | solution.py:690
  108.8 1.2 collective-permute-done.1.oth_ref
  110.0 0.0 copy-done
  110.0 0.0 copy-done.1
  110.0 3.1 %mix_project.1 = bf16[256,2048]{1,0:T(8,128)(2,1)} custom-call(s32[1]{0:T(128)} %bitcast.core_ref.refs_0_, bf16[256,256]{1,0:T(8,128)(2,1)S(1)} %get-tuple-element.14.qa_ref, bf16[256,128]{1,0:T(8,128)(2,1)S(1)} %get-tuple-element.15.qb_ref, f32[256,640]{1,0:T(8,128)S(1)} %get-tuple-element.16.loc_ref, bf16[16,72,128]{2,1,0:T(8,128)(2,1)S(1)} %all_to_all.26.own_ref, ...), custom_call_target="tpu_custom_call" | custom-call | tf_op jit(solution)/shard_map/mix_project/pallas_call | solution.py:422
  113.2 0.0 copy-start.4
  113.2 7.2 %all-to-all-start.2 = ((bf16[8,32,2048]{2,1,0:T(8,128)(2,1)}), bf16[8,32,2048]{2,1,0:T(8,128)(2,1)S(1)}, u32[]{:S(2)}, u32[]{:S(2)}) async-start(bf16[8,32,2048]{2,1,0:T(8,128)(2,1)} %bitcast.2), calls=%async_computation.2 | async-start | bytes 2097152 | tf_op jit(solution)/shard_map/all_to_all | solution.py:656
  120.3 0.0 copy-done.6
  120.3 0.0 copy-done.5
  120.4 0.1 copy.23
  120.5 0.1 reshape.23.ids_ref
  120.6 26.7 %all-to-all-done.2.arr_ref = bf16[8,32,2048]{2,1,0:T(8,128)(2,1)S(1)} async-done(((bf16[8,32,2048]{2,1,0:T(8,128)(2,1)}), bf16[8,32,2048]{2,1,0:T(8,128)(2,1)S(1)}, u32[]{:S(2)}, u32[]{:S(2)}) %all-to-all-start.2) | async-done | bytes 1048608 | tf_op jit(solution)/shard_map/all_to_all | solution.py:656
  147.2 0.0 copy-done.2
  147.2 0.0 copy-done.3
  147.2 0.7 dispatch.1
  147.9 35.1 %all_to_all.27.own_ref = bf16[32,32,128]{2,1,0:T(8,128)(2,1)S(1)} all-to-all(bf16[32,32,128]{2,1,0:T(8,128)(2,1)S(1)} %get-tuple-element.19), channel_id=1, replica_groups=mesh['grp'=2,'sp_0'=16,'sp_1'=2,'tp'=8] {'sp_0','sp_1'}, dimensions={0} | all-to-all | bytes 524288 | tf_op jit(solution)/shard_map/all_to_all | solution.py:656
  183.0 3.2 %collective-permute-start.2 = (bf16[32,32,128]{2,1,0:T(8,128)(2,1)S(1)}, bf16[32,32,128]{2,1,0:T(8,128)(2,1)S(1)}, u32[]{:S(2)}, u32[]{:S(2)}) collective-permute-start(bf16[32,32,128]{2,1,0:T(8,128)(2,1)S(1)} %all_to_all.27.own_ref), channel_id=1, source_target_pairs={{0,256},{256,0},{1,257},{257,1},{2,258},{258,2},{3,259},{259,3},{4... | collective-permute-start | bytes 786440 | tf_op jit(solution)/shard_map/ppermute | solution.py:698
  186.2 6.0 %collective-permute-done.2.oth_ref = bf16[32,32,128]{2,1,0:T(8,128)(2,1)S(1)} collective-permute-done((bf16[32,32,128]{2,1,0:T(8,128)(2,1)S(1)}, bf16[32,32,128]{2,1,0:T(8,128)(2,1)S(1)}, u32[]{:S(2)}, u32[]{:S(2)}) %collective-permute-start.2) | collective-permute-done | bytes 262176 | tf_op jit(solution)/shard_map/ppermute | solution.py:698
  192.2 0.0 all-gather.3.cloned.1.call-done
  192.2 3.9 %experts.1 = (f32[64,2048]{1,0:T(8,128)S(1)}, bf16[64,2048]{1,0:T(8,128)(2,1)S(1)}) custom-call(bf16[32,32,128]{2,1,0:T(8,128)(2,1)S(1)} %all_to_all.27.own_ref, bf16[32,32,128]{2,1,0:T(8,128)(2,1)S(1)} %collective-permute-done.2.oth_ref, bf16[8,3072,128]{2,1,0:T(8,128)(2,1)} %bitcast.5), custom_call_target="tpu_custom_call" | custom-call | tf_op jit(solution)/shard_map/experts/pallas_call | solution.py:587
  196.1 3.2 %collective-permute-start.3 = (bf16[64,2048]{1,0:T(8,128)(2,1)S(1)}, bf16[64,2048]{1,0:T(8,128)(2,1)S(1)}, u32[]{:S(2)}, u32[]{:S(2)}) collective-permute-start(bf16[64,2048]{1,0:T(8,128)(2,1)S(1)} %get-tuple-element.21), channel_id=1, source_target_pairs={{0,256},{256,0},{1,257},{257,1},{2,258},{258,2},{3,259},{259,3},{4... | collective-permute-start | bytes 786440 | tf_op jit(solution)/shard_map/ppermute | solution.py:700
  199.3 5.1 %collective-permute-done.3.arrived_ref = bf16[64,2048]{1,0:T(8,128)(2,1)S(1)} collective-permute-done((bf16[64,2048]{1,0:T(8,128)(2,1)S(1)}, bf16[64,2048]{1,0:T(8,128)(2,1)S(1)}, u32[]{:S(2)}, u32[]{:S(2)}) %collective-permute-start.3) | collective-permute-done | bytes 262176 | tf_op jit(solution)/shard_map/ppermute | solution.py:700
  204.4 0.9 finish.1
  205.3 6.1 %all-to-all-start.4 = ((bf16[32,32,128]{2,1,0:T(8,128)(2,1)}), bf16[32,32,128]{2,1,0:T(8,128)(2,1)S(1)}, u32[]{:S(2)}, u32[]{:S(2)}) async-start(bf16[32,32,128]{2,1,0:T(8,128)(2,1)} %finish.1), calls=%async_computation.4 | async-start | bytes 524288 | tf_op jit(solution)/shard_map/all_to_all | solution.py:656
  211.4 0.0 copy-done.4
  211.4 0.1 copy.24
  211.5 0.1 reshape.25.w_ref
  211.6 21.2 %all-to-all-done.4.ret_ref = bf16[32,32,128]{2,1,0:T(8,128)(2,1)S(1)} async-done(((bf16[32,32,128]{2,1,0:T(8,128)(2,1)}), bf16[32,32,128]{2,1,0:T(8,128)(2,1)S(1)}, u32[]{:S(2)}, u32[]{:S(2)}) %all-to-all-start.4) | async-done | bytes 262176 | tf_op jit(solution)/shard_map/all_to_all | solution.py:656
  232.8 1.5 combine.1
  (2 shorter events, 0.0 us)
Async XLA Ops:
  6.5 103.5 %copy-start = (bf16[512,2048]{1,0:T(8,128)(2,1)S(1)}, bf16[512,2048]{1,0:T(8,128)(2,1)}, u32[]{:S(2)}) copy-start(bf16[512,2048]{1,0:T(8,128)(2,1)} %wa_ref.1) | copy-start | bytes 6291460
  6.5 103.5 %copy-start.1 = (bf16[128,2048]{1,0:T(8,128)(2,1)S(1)}, bf16[128,2048]{1,0:T(8,128)(2,1)}, u32[]{:S(2)}) copy-start(bf16[128,2048]{1,0:T(8,128)(2,1)} %wb_ref.1) | copy-start | bytes 1572868
  6.6 185.7 %all-gather.3.cloned.1.call-start = ((), (), s32[]{:S(2)}) async-start(), calls=%async_computation.5 | async-start | bytes 7077888 | tf_op jit(solution)/shard_map/all_gather | solution.py:672
  9.5 110.8 %copy-start.6 = (s32[32]{0:T(128)S(1)}, s32[32]{0:T(128)}, u32[]{:S(2)}) copy-start(s32[32]{0:T(128)} %param.32) | copy-start | bytes 388
  9.5 110.8 %copy-start.5 = (s32[32,2]{0,1:T(2,128)S(1)}, s32[32,2]{0,1:T(2,128)}, u32[]{:S(2)}) copy-start(s32[32,2]{0,1:T(2,128)} %param.33) | copy-start | bytes 772
  9.5 137.7 %copy-start.2 = (bf16[32,2048]{1,0:T(8,128)(2,1)S(1)}, bf16[32,2048]{1,0:T(8,128)(2,1)}, u32[]{:S(2)}) copy-start(bf16[32,2048]{1,0:T(8,128)(2,1)} %res_ref.1) | copy-start | bytes 393220
  9.5 137.7 %copy-start.3 = (f32[2,2048]{1,0:T(2,128)S(1)}, f32[2,2048]{1,0:T(2,128)}, u32[]{:S(2)}) copy-start(f32[2,2048]{1,0:T(2,128)} %gain_ref.3) | copy-start | bytes 49156
  12.4 45.0 %collective-permute-start = (bf16[2,288,512]{2,1,0:T(8,128)(2,1)S(1)}, bf16[2,288,512]{2,1,0:T(8,128)(2,1)S(1)}, u32[]{:S(2)}, u32[]{:S(2)}) collective-permute-start(bf16[2,288,512]{2,1,0:T(8,128)(2,1)S(1)} %get-tuple-element.17.own_ref), channel_id=1, source_target_pairs={{0,8},{8,0},{1,9},{9,1},{2,10},{10,2},{3,11},{11,3},{4,12},{12,4},... | collective-permute-start | bytes 1769480 | tf_op jit(solution)/shard_map/ppermute | solution.py:686
  100.7 9.3 %collective-permute-start.1 = (bf16[16,72,128]{2,1,0:T(8,128)(2,1)S(1)}, bf16[16,72,128]{2,1,0:T(8,128)(2,1)S(1)}, u32[]{:S(2)}, u32[]{:S(2)}) collective-permute-start(bf16[16,72,128]{2,1,0:T(8,128)(2,1)S(1)} %all_to_all.26.own_ref), channel_id=1, source_target_pairs={{0,8},{8,0},{1,9},{9,1},{2,10},{10,2},{3,11},{11,3},{4,12},{12,4},... | collective-permute-start | bytes 884744 | tf_op jit(solution)/shard_map/ppermute | solution.py:690
  113.2 98.2 %copy-start.4 = (f32[32,2]{0,1:T(2,128)S(1)}, f32[32,2]{0,1:T(2,128)}, u32[]{:S(2)}) copy-start(f32[32,2]{0,1:T(2,128)} %param.34) | copy-start | bytes 772
  113.2 34.1 %all-to-all-start.2 = ((bf16[8,32,2048]{2,1,0:T(8,128)(2,1)}), bf16[8,32,2048]{2,1,0:T(8,128)(2,1)S(1)}, u32[]{:S(2)}, u32[]{:S(2)}) async-start(bf16[8,32,2048]{2,1,0:T(8,128)(2,1)} %bitcast.2), calls=%async_computation.2 | async-start | bytes 2097152 | tf_op jit(solution)/shard_map/all_to_all | solution.py:656
  183.0 9.2 %collective-permute-start.2 = (bf16[32,32,128]{2,1,0:T(8,128)(2,1)S(1)}, bf16[32,32,128]{2,1,0:T(8,128)(2,1)S(1)}, u32[]{:S(2)}, u32[]{:S(2)}) collective-permute-start(bf16[32,32,128]{2,1,0:T(8,128)(2,1)S(1)} %all_to_all.27.own_ref), channel_id=1, source_target_pairs={{0,256},{256,0},{1,257},{257,1},{2,258},{258,2},{3,259},{259,3},{4... | collective-permute-start | bytes 786440 | tf_op jit(solution)/shard_map/ppermute | solution.py:698
  196.1 8.3 %collective-permute-start.3 = (bf16[64,2048]{1,0:T(8,128)(2,1)S(1)}, bf16[64,2048]{1,0:T(8,128)(2,1)S(1)}, u32[]{:S(2)}, u32[]{:S(2)}) collective-permute-start(bf16[64,2048]{1,0:T(8,128)(2,1)S(1)} %get-tuple-element.21), channel_id=1, source_target_pairs={{0,256},{256,0},{1,257},{257,1},{2,258},{258,2},{3,259},{259,3},{4... | collective-permute-start | bytes 786440 | tf_op jit(solution)/shard_map/ppermute | solution.py:700
  205.3 27.5 %all-to-all-start.4 = ((bf16[32,32,128]{2,1,0:T(8,128)(2,1)}), bf16[32,32,128]{2,1,0:T(8,128)(2,1)S(1)}, u32[]{:S(2)}, u32[]{:S(2)}) async-start(bf16[32,32,128]{2,1,0:T(8,128)(2,1)} %finish.1), calls=%async_computation.4 | async-start | bytes 524288 | tf_op jit(solution)/shard_map/all_to_all | solution.py:656
Sparse Core Ops, SparseCore 0:
  9.6 114.8 all-gather.2

commit v5 on v4

--- a/solution.py
+++ b/solution.py
@@ -8,6 +8,7 @@
 from jax.experimental.pallas import tpu as pltpu
 from jax.sharding import Mesh
 from jax.sharding import PartitionSpec as P
+
 
 CAP = 2
 TOP = 2
@@ -345,8 +346,14 @@
 
 def mix_body(
     core_ref, qa_ref, qb_ref, loc_ref, own_ref, oth_ref, pay_ref, dec_ref, wa_ref, wb_ref,
-    out_ref, grp_scr,
+    out_ref, grp_scr, wa_scr, wb_scr, sems,
 ):
+    copies = [
+        pltpu.make_async_copy(wa_ref, wa_scr, sems.at[0]),
+        pltpu.make_async_copy(wb_ref, wb_scr, sems.at[1]),
+    ]
+    for copy in copies:
+        copy.start()
     n, dk = qa_ref.shape
     width = qb_ref.shape[1]
     hb = width // 2
@@ -414,7 +421,9 @@
     s0 = jnp.sum(jnp.where(left, sq, 0.0), axis=1, keepdims=True) / hb
     s1 = jnp.sum(jnp.where(left, 0.0, sq), axis=1, keepdims=True) / hb
     mixed_b = (total_b * lax.rsqrt(jnp.where(left, s0, s1) + GROUP_EPS)).astype(BF16)
-    out_ref[...] = (mm(mixed_a, wa_ref[...]) + mm(mixed_b, wb_ref[...])).astype(BF16)
+    for copy in copies:
+        copy.wait()
+    out_ref[...] = (mm(mixed_a, wa_scr[...]) + mm(mixed_b, wb_scr[...])).astype(BF16)
 
 
 def mix_project(core, qa, qb, loc, own, other, pay, dec, wa, wb):
@@ -422,13 +431,18 @@
     return pl.pallas_call(
         mix_body,
         out_shape=near_shape((qa.shape[0], wa.shape[1]), BF16),
-        in_specs=[SMEM_SPEC] + vmem(9),
+        in_specs=[SMEM_SPEC] + vmem(7) + [ANY_SPEC] * 2,
         out_specs=vmem(1)[0],
-        scratch_shapes=[pltpu.VMEM((hb, qb.shape[1]), F32)],
+        scratch_shapes=[
+            pltpu.VMEM((hb, qb.shape[1]), F32),
+            pltpu.VMEM(wa.shape, BF16),
+            pltpu.VMEM(wb.shape, BF16),
+            pltpu.SemaphoreType.DMA((2,)),
+        ],
         interpret=INTERPRET,
         compiler_params=PARAMS,
         name="mix_project",
-    )(core, *map(near, (qa, qb, loc, own, other, pay, dec)), wa, wb)
+    )(core, *map(near, (qa, qb, loc, own, other, pay, dec)), far(wa), far(wb))
 
 
 def layer_norm(stream, gain):
@@ -495,6 +509,24 @@
         compiler_params=PARAMS,
         name="dispatch",
     )(near(arrived), residual, gain, ids)
+
+
+def hand_on(*arrays):
+    count = len(arrays)
+
+    def body(*refs):
+        del refs
+
+    return pl.pallas_call(
+        body,
+        out_shape=tuple(jax.ShapeDtypeStruct(x.shape, x.dtype) for x in arrays),
+        in_specs=[ANY_SPEC] * count,
+        out_specs=tuple([ANY_SPEC] * count),
+        input_output_aliases={k: k for k in range(count)},
+        interpret=INTERPRET,
+        compiler_params=PARAMS,
+        name="hand_on",
+    )(*map(far, arrays))
 
 
 def pack_weights_body(part_ref, gate_ref, up_ref, down_ref, out_ref):
@@ -528,14 +560,13 @@
     )(part, far(gate), far(up), far(down))
 
 
-def expert_body(own_ref, oth_ref, w_ref, mine_ref, send_ref, x_scr, w_scr, acc_ref, sems):
-    count, depth, units = w_scr.shape
+def expert_body(own_ref, oth_ref, *refs):
+    *held, mine_ref, send_ref, x_scr, blocks, acc_ref, sems = refs
+    count, _, units = blocks.shape
     rows = mine_ref.shape[0]
     width = mine_ref.shape[1]
     half = units // 2
-    copies = [
-        pltpu.make_async_copy(w_ref.at[k], w_scr.at[k], sems.at[k]) for k in range(count)
-    ]
+    copies = [pltpu.make_async_copy(held[k], blocks.at[k], sems.at[k]) for k in range(count)]
     for copy in copies:
         copy.start()
     x = jnp.concatenate(
@@ -552,7 +583,7 @@
         for k in range(first, first + group, 2):
             copies[k].wait()
             copies[k + 1].wait()
-            both = mm(x, jnp.concatenate([w_scr[k, :width, :], w_scr[k + 1, :width, :]], axis=1))
+            both = mm(x, jnp.concatenate([blocks[k, :width, :], blocks[k + 1, :width, :]], axis=1))
             one, two = both[:, :units], both[:, units:]
             one = silu(one) * pltpu.roll(one, half, 1)
             two = silu(pltpu.roll(two, half, 1)) * two
@@ -564,7 +595,7 @@
                 at = width + j * half
                 cols.append(
                     jnp.concatenate(
-                        [w_scr[k, at : at + half, :] for k in range(first, first + group)], axis=0
+                        [blocks[k, at : at + half, :] for k in range(first, first + group)], axis=0
                     )
                 )
             part = mm(hidden, jnp.concatenate(cols, axis=1))
@@ -579,8 +610,8 @@
                 send_ref[:, cut] = part[rows:].astype(BF16)
 
 
-def experts(own, other, weights):
-    count, depth, units = weights.shape
+def experts(own, other, blocks):
+    depth, units = blocks[0].shape
     width = depth * 2 // 3
     lines = own.shape[0] * own.shape[1]
     rows = lines * LANES // width
@@ -590,18 +621,18 @@
             near_shape((rows, width), F32),
             near_shape((rows, width), BF16),
         ),
-        in_specs=vmem(2) + [ANY_SPEC],
+        in_specs=vmem(2) + [ANY_SPEC] * len(blocks),
         out_specs=tuple(vmem(2)),
         scratch_shapes=[
             pltpu.VMEM((lines, LANES), F32),
-            pltpu.VMEM((count, depth, units), BF16),
+            pltpu.VMEM((len(blocks), depth, units), BF16),
             pltpu.VMEM((2 * rows, width), F32),
-            pltpu.SemaphoreType.DMA((count,)),
+            pltpu.SemaphoreType.DMA((len(blocks),)),
         ],
         interpret=INTERPRET,
         compiler_params=PARAMS,
         name="experts",
-    )(near(own), near(other), far(weights))
+    )(near(own), near(other), *map(far, blocks))
 
 
 def finish_body(mine_ref, arrived_ref, out_ref, scr):
@@ -669,9 +700,8 @@
     routes = rows_dev * TOP
     part = (lax.axis_index("grp") % 2).astype(jnp.int32).reshape(1)
     partner = [(k, k ^ 1) for k in range(lax.axis_size("grp"))]
-    weights_all = lax.all_gather(
-        pack_weights(part, expert_gate, expert_up, expert_down), "tp"
-    )
+    up_ring = [(k, (k + 1) % tp) for k in range(tp)]
+    down_ring = [(k, (k - 1) % tp) for k in range(tp)]
 
     core = lax.axis_index("sp_1").astype(jnp.int32).reshape(1)
     local, base = angle_tables(
@@ -684,9 +714,20 @@
     )
     swap = [(0, 1), (1, 0)]
     pay_other = lax.ppermute(pay, "sp_1", swap)
-    pieces = exchange(pack_states(core, pay, pay_other, chips), "sp_0")
+    packed = pack_weights(part, expert_gate, expert_up, expert_down)
+    blocks = [packed]
+    held = (lax.ppermute(packed, "tp", up_ring), lax.ppermute(packed, "tp", down_ring))
+    outgoing_states = pack_states(core, pay, pay_other, chips)
+    pieces = exchange(outgoing_states, "sp_0")
+    held = hand_on(*held)
+    blocks += held
+    held = (lax.ppermute(held[0], "tp", up_ring), lax.ppermute(held[1], "tp", down_ring))
     per = value_a.shape[1] // LANES * TILE // chips
-    carried = exchange(scan_states(core, pieces, per), "sp_0")
+    scanned = scan_states(core, pieces, per)
+    carried = exchange(scanned, "sp_0")
+    held = hand_on(*held)
+    blocks += held
+    held = (lax.ppermute(held[0], "tp", up_ring), lax.ppermute(held[1], "tp", down_ring))
     carried_other = lax.ppermute(carried, "sp_1", swap)
     partial = mix_project(
         core, qa, qb, loc, carried, carried_other, pay_other, dec, out_weight_a, out_weight_b
@@ -695,9 +736,13 @@
     ids = (route_group[:, None] * EXP_GROUP + route_expert).reshape(1, routes)
     hidden, outgoing = dispatch(arrived, residual, norm_gain, ids, sp_count)
     received = exchange(outgoing, SP)
+    held = hand_on(*held)
+    blocks += held
+    blocks.append(lax.ppermute(held[0], "tp", up_ring))
     received_other = lax.ppermute(received, "grp", partner)
-    mine, send = experts(received, received_other, weights_all)
-    back = finish(mine, lax.ppermute(send, "grp", partner), sp_count)
+    mine, send = experts(received, received_other, blocks)
+    arrived_sums = lax.ppermute(send, "grp", partner)
+    back = finish(mine, arrived_sums, sp_count)
     returned = exchange(back, SP)
     return combine(returned, hidden, norm_gain, ids, route_weight.reshape(1, routes))
 
@@ -729,6 +774,7 @@
         P(SP, "tp", None),
     )
     out_specs = P(GRP_SP_TP, None)
+
     return jax.shard_map(
         shards, mesh=finer, in_specs=in_specs, out_specs=out_specs, check_vma=False
     )

time: 243 us -> 260 us (1.070)
  blocking collectives: 78 us -> 42.7 us
  starting transfers between devices: 71.2 us -> 106 us
  waiting for transfers between devices: 61.8 us -> 90.1 us
  between operations: 13.6 us -> 0.28 us
    ppermute x1 -> x8, waiting for transfers between devices: 5.11 us -> 54.7 us  [the longest x2 37.1 us: shards(): lax.ppermute(held[0], 'tp', up_ring)]
    all_to_all x3 -> x2, blocking collectives: 78 us -> 42.7 us  [exchange(): return lax.all_to_all(array, axis, split_axis=0, concat_axis=0, tiled=True)]
    ppermute x1 -> x8, starting transfers between devices: 3.22 us -> 29.2 us  [the longest x2 8.6 us: shards(): lax.ppermute(held[1], 'tp', down_ring)]
    all_to_all x2 -> x3, waiting for transfers between devices: 47.9 us -> 30.9 us  [exchange(): return lax.all_to_all(array, axis, split_axis=0, concat_axis=0, tiled=True)]
    all_to_all x2 -> x3, starting transfers between devices: 13.2 us -> 21.4 us  [exchange(): return lax.all_to_all(array, axis, split_axis=0, concat_axis=0, tiled=True)]
    ppermute x1, waiting for transfers between devices: 5.97 us -> 2.85 us  [shards(): received_other = lax.ppermute(received, 'grp', partner)]
  transfers between devices with their start and end apart: 7 -> 14, of which waited for: 6 -> 12; matrix products, arithmetic and copies ran while one was open for 0% -> 0% of each run, Pallas kernels for 3% -> 3%
where the time goes in v5:
time: 260 us; the launch traced here: 259 us
  starting transfers between devices  106 us (41%)
  waiting for transfers between devices  90.1 us (35%)
  blocking collectives  42.7 us (16%)
  Pallas kernels  17.2 us (7%)
    ppermute x1, starting transfers between devices, shards(): pay_other = lax.ppermute(pay, 'sp_1', swap)  43.4 us
    all_to_all x2, blocking collectives, exchange(): return lax.all_to_all(array, axis, split_axis=0, concat_axis=0, tiled=True)  42.7 us
    ppermute x2, waiting for transfers between devices, shards(): lax.ppermute(held[0], 'tp', up_ring)  37.1 us
    all_to_all x3, waiting for transfers between devices, exchange(): return lax.all_to_all(array, axis, split_axis=0, concat_axis=0, tiled=True)  30.9 us
    all_to_all x3, starting transfers between devices, exchange(): return lax.all_to_all(array, axis, split_axis=0, concat_axis=0, tiled=True)  21.4 us
    ppermute x2, starting transfers between devices, shards(): lax.ppermute(held[1], 'tp', down_ring)  8.6 us
    ppermute x1, starting transfers between devices, shards(): carried_other = lax.ppermute(carried, 'sp_1', swap)  8.1 us
    ppermute x2, starting transfers between devices, shards(): lax.ppermute(held[0], 'tp', up_ring)  5.98 us
  transfers between devices with their start and end apart: 14, of which 12 were waited for; matrix products, arithmetic and copies ran while one was open for 0% of the time, Pallas kernels for 3%

profile of v5, /device:TPU:65, one launch (start us, length us, event | category | flops | bytes accessed | tf_op | source)
XLA Modules:
  0.0 259.0 jit_solution(9203443199597677469)
XLA Ops:
  0.0 2.8 %retention_local.1 = (bf16[256,256]{1,0:T(8,128)(2,1)S(1)}, bf16[256,128]{1,0:T(8,128)(2,1)S(1)}, f32[256,640]{1,0:T(8,128)S(1)}, bf16[2,288,512]{2,1,0:T(8,128)(2,1)S(1)}, f32[8,256]{1,0:T(8,128)S(1)}) custom-call(s32[1]{0:T(128)} %bitcast.1.index_ref, bf16[256,256]{1,0:T(8,128)(2,1)} %qa_ref.1, bf16[256,256]{1,0:T(8,128)(2,1)} %ka_ref.1, ...), custom_call_target="tpu_custom_call" | custom-call | tf_op jit(solution)/shard_map/retention_local/pallas_call | solution.py:188
  2.8 43.4 %collective-permute-start = (bf16[2,288,512]{2,1,0:T(8,128)(2,1)S(1)}, bf16[2,288,512]{2,1,0:T(8,128)(2,1)S(1)}, u32[]{:S(2)}, u32[]{:S(2)}) collective-permute-start(bf16[2,288,512]{2,1,0:T(8,128)(2,1)S(1)} %get-tuple-element.23.own_ref), channel_id=1, source_target_pairs={{0,8},{8,0},{1,9},{9,1},{2,10},{10,2},{3,11},{11,3},{4,12},{12,4},... | collective-permute-start | bytes 1769480 | tf_op jit(solution)/shard_map/ppermute | solution.py:716
  46.2 1.6 collective-permute-done.oth_ref.pay_ref
  47.8 0.2 pack_states.1
  48.0 17.3 %all_to_all.25.refs_1_ = bf16[16,72,128]{2,1,0:T(8,128)(2,1)S(1)} all-to-all(bf16[16,72,128]{2,1,0:T(8,128)(2,1)S(1)} %pack_states.1), channel_id=1, replica_groups=mesh['grp'=2,'sp_0'=16,'sp_1'=2,'tp'=8] {'sp_0'}, dimensions={0} | all-to-all | bytes 589824 | tf_op jit(solution)/shard_map/all_to_all | solution.py:687
  65.3 0.2 scan_states.1
  65.5 25.4 %all_to_all.26.own_ref = bf16[16,72,128]{2,1,0:T(8,128)(2,1)S(1)} all-to-all(bf16[16,72,128]{2,1,0:T(8,128)(2,1)S(1)} %scan_states.1), channel_id=1, replica_groups=mesh['grp'=2,'sp_0'=16,'sp_1'=2,'tp'=8] {'sp_0'}, dimensions={0} | all-to-all | bytes 589824 | tf_op jit(solution)/shard_map/all_to_all | solution.py:687
  90.9 8.1 %collective-permute-start.1 = (bf16[16,72,128]{2,1,0:T(8,128)(2,1)S(1)}, bf16[16,72,128]{2,1,0:T(8,128)(2,1)S(1)}, u32[]{:S(2)}, u32[]{:S(2)}) collective-permute-start(bf16[16,72,128]{2,1,0:T(8,128)(2,1)S(1)} %all_to_all.26.own_ref), channel_id=1, source_target_pairs={{0,8},{8,0},{1,9},{9,1},{2,10},{10,2},{3,11},{11,3},{4,12},{12,4},... | collective-permute-start | bytes 884744 | tf_op jit(solution)/shard_map/ppermute | solution.py:731
  99.0 1.9 pack_weights.1.refs_0_
  100.9 3.3 %collective-permute-start.3 = (bf16[3072,128]{1,0:T(8,128)(2,1)S(1)}, bf16[3072,128]{1,0:T(8,128)(2,1)}, u32[]{:S(2)}, u32[]{:S(2)}) collective-permute-start(bf16[3072,128]{1,0:T(8,128)(2,1)S(1)} %pack_weights.1.refs_0_), channel_id=1, source_target_pairs={{0,1},{1,2},{2,3},{3,4},{4,5},{5,6},{6,7},{7,0},{8,9},{9,10},{10,1... | collective-permute-start | bytes 2359304 | tf_op jit(solution)/shard_map/ppermute | solution.py:719
  104.2 4.2 %collective-permute-start.4 = (bf16[3072,128]{1,0:T(8,128)(2,1)S(1)}, bf16[3072,128]{1,0:T(8,128)(2,1)}, u32[]{:S(2)}, u32[]{:S(2)}) collective-permute-start(bf16[3072,128]{1,0:T(8,128)(2,1)S(1)} %pack_weights.1.refs_0_), channel_id=1, source_target_pairs={{0,7},{1,0},{2,1},{3,2},{4,3},{5,4},{6,5},{7,6},{8,15},{9,8},{10,9... | collective-permute-start | bytes 2359304 | tf_op jit(solution)/shard_map/ppermute | solution.py:719
  108.3 0.0 collective-permute-done.1.oth_ref
  108.4 4.5 %mix_project.1 = bf16[256,2048]{1,0:T(8,128)(2,1)} custom-call(s32[1]{0:T(128)} %bitcast.core_ref.refs_0_, bf16[256,256]{1,0:T(8,128)(2,1)S(1)} %get-tuple-element.20.qa_ref, bf16[256,128]{1,0:T(8,128)(2,1)S(1)} %get-tuple-element.21.qb_ref, f32[256,640]{1,0:T(8,128)S(1)} %get-tuple-element.22.loc_ref, bf16[16,72,128]{2,1,0:T(8,128)(2,1)S(1)} %all_to_all.26.own_ref, ...), custom_call_target="tpu_custom_call" | custom-call | tf_op jit(solution)/shard_map/mix_project/pallas_call | solution.py:431
  112.9 6.2 %all-to-all-start.2 = ((bf16[8,32,2048]{2,1,0:T(8,128)(2,1)}), bf16[8,32,2048]{2,1,0:T(8,128)(2,1)S(1)}, u32[]{:S(2)}, u32[]{:S(2)}) async-start(bf16[8,32,2048]{2,1,0:T(8,128)(2,1)} %bitcast.2), calls=%async_computation.2 | async-start | bytes 2097152 | tf_op jit(solution)/shard_map/all_to_all | solution.py:687
  119.1 0.0 copy-start.9
  119.1 0.0 copy-start.1
  119.1 0.0 copy-start.2
  119.1 5.3 %collective-permute-done.3.refs_0_ = bf16[3072,128]{1,0:T(8,128)(2,1)} collective-permute-done((bf16[3072,128]{1,0:T(8,128)(2,1)S(1)}, bf16[3072,128]{1,0:T(8,128)(2,1)}, u32[]{:S(2)}, u32[]{:S(2)}) %collective-permute-start.3) | collective-permute-done | bytes 786464 | tf_op jit(solution)/shard_map/ppermute | solution.py:719
  124.4 0.8 collective-permute-done.4.refs_1_
  125.2 3.1 %collective-permute-start.5 = (bf16[3072,128]{1,0:T(8,128)(2,1)}, bf16[3072,128]{1,0:T(8,128)(2,1)S(1)}, u32[]{:S(2)}, u32[]{:S(2)}) collective-permute-start(bf16[3072,128]{1,0:T(8,128)(2,1)} %get-tuple-element.26.refs_1_), channel_id=1, source_target_pairs={{0,1},{1,2},{2,3},{3,4},{4,5},{5,6},{6,7},{7,0},{8,9},{9,10},{10,1... | collective-permute-start | bytes 2359304 | tf_op jit(solution)/shard_map/ppermute | solution.py:724
  128.3 4.3 %collective-permute-start.6 = (bf16[3072,128]{1,0:T(8,128)(2,1)}, bf16[3072,128]{1,0:T(8,128)(2,1)S(1)}, u32[]{:S(2)}, u32[]{:S(2)}) collective-permute-start(bf16[3072,128]{1,0:T(8,128)(2,1)} %get-tuple-element.27.refs_2_), channel_id=1, source_target_pairs={{0,7},{1,0},{2,1},{3,2},{4,3},{5,4},{6,5},{7,6},{8,15},{9,8},{10,9... | collective-permute-start | bytes 2359304 | tf_op jit(solution)/shard_map/ppermute | solution.py:724
  132.6 31.0 %collective-permute-done.5.refs_0_ = bf16[3072,128]{1,0:T(8,128)(2,1)S(1)} collective-permute-done((bf16[3072,128]{1,0:T(8,128)(2,1)}, bf16[3072,128]{1,0:T(8,128)(2,1)S(1)}, u32[]{:S(2)}, u32[]{:S(2)}) %collective-permute-start.5) | collective-permute-done | bytes 786464 | tf_op jit(solution)/shard_map/ppermute | solution.py:724
  163.6 1.0 collective-permute-done.6.refs_1_
  164.6 0.9 copy-done.6
  165.5 2.9 %collective-permute-start.7 = (bf16[3072,128]{1,0:T(8,128)(2,1)}, bf16[3072,128]{1,0:T(8,128)(2,1)S(1)}, u32[]{:S(2)}, u32[]{:S(2)}) collective-permute-start(bf16[3072,128]{1,0:T(8,128)(2,1)} %get-tuple-element.28.refs_3_), channel_id=1, source_target_pairs={{0,1},{1,2},{2,3},{3,4},{4,5},{5,6},{6,7},{7,0},{8,9},{9,10},{10,1... | collective-permute-start | bytes 2359304 | tf_op jit(solution)/shard_map/ppermute | solution.py:730
  168.4 4.3 %collective-permute-start.8 = (bf16[3072,128]{1,0:T(8,128)(2,1)}, bf16[3072,128]{1,0:T(8,128)(2,1)S(1)}, u32[]{:S(2)}, u32[]{:S(2)}) collective-permute-start(bf16[3072,128]{1,0:T(8,128)(2,1)} %get-tuple-element.29.refs_4_), channel_id=1, source_target_pairs={{0,7},{1,0},{2,1},{3,2},{4,3},{5,4},{6,5},{7,6},{8,15},{9,8},{10,9... | collective-permute-start | bytes 2359304 | tf_op jit(solution)/shard_map/ppermute | solution.py:730
  172.8 0.1 copy.29
  172.9 0.1 reshape.23.ids_ref
  173.0 0.0 all-to-all-done.2.arr_ref
  173.0 1.4 dispatch.1
  174.4 7.5 %all-to-all-start.3 = ((bf16[32,32,128]{2,1,0:T(8,128)(2,1)}), bf16[32,32,128]{2,1,0:T(8,128)(2,1)S(1)}, u32[]{:S(2)}, u32[]{:S(2)}) async-start(bf16[32,32,128]{2,1,0:T(8,128)(2,1)} %get-tuple-element.25), calls=%async_computation.3 | async-start | bytes 524288 | tf_op jit(solution)/shard_map/all_to_all | solution.py:687
  181.9 6.1 %collective-permute-done.7.refs_0_ = bf16[3072,128]{1,0:T(8,128)(2,1)S(1)} collective-permute-done((bf16[3072,128]{1,0:T(8,128)(2,1)}, bf16[3072,128]{1,0:T(8,128)(2,1)S(1)}, u32[]{:S(2)}, u32[]{:S(2)}) %collective-permute-start.7) | collective-permute-done | bytes 786464 | tf_op jit(solution)/shard_map/ppermute | solution.py:730
  188.0 2.0 collective-permute-done.8.refs_1_
  190.1 0.9 copy-done.4
  191.0 4.0 %collective-permute-start.9 = (bf16[3072,128]{1,0:T(8,128)(2,1)}, bf16[3072,128]{1,0:T(8,128)(2,1)S(1)}, u32[]{:S(2)}, u32[]{:S(2)}) collective-permute-start(bf16[3072,128]{1,0:T(8,128)(2,1)} %get-tuple-element.30.refs_5_), channel_id=1, source_target_pairs={{0,1},{1,2},{2,3},{3,4},{4,5},{5,6},{6,7},{7,0},{8,9},{9,10},{10,1... | collective-permute-start | bytes 2359304 | tf_op jit(solution)/shard_map/ppermute | solution.py:741
  195.0 9.0 %all-to-all-done.3.own_ref = bf16[32,32,128]{2,1,0:T(8,128)(2,1)S(1)} async-done(((bf16[32,32,128]{2,1,0:T(8,128)(2,1)}), bf16[32,32,128]{2,1,0:T(8,128)(2,1)S(1)}, u32[]{:S(2)}, u32[]{:S(2)}) %all-to-all-start.3) | async-done | bytes 262176 | tf_op jit(solution)/shard_map/all_to_all | solution.py:687
  204.0 4.4 %collective-permute-start.2 = (bf16[32,32,128]{2,1,0:T(8,128)(2,1)S(1)}, bf16[32,32,128]{2,1,0:T(8,128)(2,1)S(1)}, u32[]{:S(2)}, u32[]{:S(2)}) collective-permute-start(bf16[32,32,128]{2,1,0:T(8,128)(2,1)S(1)} %all-to-all-done.3.own_ref), channel_id=1, source_target_pairs={{0,256},{256,0},{1,257},{257,1},{2,258},{258,2},{3,259},{259,3},{4... | collective-permute-start | bytes 786440 | tf_op jit(solution)/shard_map/ppermute | solution.py:742
  208.5 3.2 %collective-permute-done.9.refs_7_ = bf16[3072,128]{1,0:T(8,128)(2,1)S(1)} collective-permute-done((bf16[3072,128]{1,0:T(8,128)(2,1)}, bf16[3072,128]{1,0:T(8,128)(2,1)S(1)}, u32[]{:S(2)}, u32[]{:S(2)}) %collective-permute-start.9) | collective-permute-done | bytes 786464 | tf_op jit(solution)/shard_map/ppermute | solution.py:741
  211.7 2.9 %collective-permute-done.2.oth_ref = bf16[32,32,128]{2,1,0:T(8,128)(2,1)S(1)} collective-permute-done((bf16[32,32,128]{2,1,0:T(8,128)(2,1)S(1)}, bf16[32,32,128]{2,1,0:T(8,128)(2,1)S(1)}, u32[]{:S(2)}, u32[]{:S(2)}) %collective-permute-start.2) | collective-permute-done | bytes 262176 | tf_op jit(solution)/shard_map/ppermute | solution.py:742
  214.5 3.9 %experts.1 = (f32[64,2048]{1,0:T(8,128)S(1)}, bf16[64,2048]{1,0:T(8,128)(2,1)S(1)}) custom-call(bf16[32,32,128]{2,1,0:T(8,128)(2,1)S(1)} %all-to-all-done.3.own_ref, bf16[32,32,128]{2,1,0:T(8,128)(2,1)S(1)} %collective-permute-done.2.oth_ref, bf16[3072,128]{1,0:T(8,128)(2,1)} %copy-done, bf16[3072,128]{1,0:T(8,128)(2,1)} %get-tuple-element.26.refs_1_, ...), custom_call_target="tpu_custom_call" | custom-call | tf_op jit(solution)/shard_map/experts/pallas_call | solution.py:618
  218.4 3.1 %collective-permute-start.10 = (bf16[64,2048]{1,0:T(8,128)(2,1)S(1)}, bf16[64,2048]{1,0:T(8,128)(2,1)S(1)}, u32[]{:S(2)}, u32[]{:S(2)}) collective-permute-start(bf16[64,2048]{1,0:T(8,128)(2,1)S(1)} %get-tuple-element.33), channel_id=1, source_target_pairs={{0,256},{256,0},{1,257},{257,1},{2,258},{258,2},{3,259},{259,3},{4... | collective-permute-start | bytes 786440 | tf_op jit(solution)/shard_map/ppermute | solution.py:744
  221.5 5.3 %collective-permute-done.10.arrived_ref = bf16[64,2048]{1,0:T(8,128)(2,1)S(1)} collective-permute-done((bf16[64,2048]{1,0:T(8,128)(2,1)S(1)}, bf16[64,2048]{1,0:T(8,128)(2,1)S(1)}, u32[]{:S(2)}, u32[]{:S(2)}) %collective-permute-start.10) | collective-permute-done | bytes 262176 | tf_op jit(solution)/shard_map/ppermute | solution.py:744
  226.8 0.9 finish.1
  227.7 7.7 %all-to-all-start.4 = ((bf16[32,32,128]{2,1,0:T(8,128)(2,1)}), bf16[32,32,128]{2,1,0:T(8,128)(2,1)S(1)}, u32[]{:S(2)}, u32[]{:S(2)}) async-start(bf16[32,32,128]{2,1,0:T(8,128)(2,1)} %finish.1), calls=%async_computation.4 | async-start | bytes 524288 | tf_op jit(solution)/shard_map/all_to_all | solution.py:687
  235.4 0.1 copy.30
  235.5 0.1 reshape.25.w_ref
  235.6 21.9 %all-to-all-done.4.ret_ref = bf16[32,32,128]{2,1,0:T(8,128)(2,1)S(1)} async-done(((bf16[32,32,128]{2,1,0:T(8,128)(2,1)}), bf16[32,32,128]{2,1,0:T(8,128)(2,1)S(1)}, u32[]{:S(2)}, u32[]{:S(2)}) %all-to-all-start.4) | async-done | bytes 262176 | tf_op jit(solution)/shard_map/all_to_all | solution.py:687
  257.5 1.5 combine.1
  (22 shorter events, 0.0 us)
Async XLA Ops:
  2.8 45.0 %collective-permute-start = (bf16[2,288,512]{2,1,0:T(8,128)(2,1)S(1)}, bf16[2,288,512]{2,1,0:T(8,128)(2,1)S(1)}, u32[]{:S(2)}, u32[]{:S(2)}) collective-permute-start(bf16[2,288,512]{2,1,0:T(8,128)(2,1)S(1)} %get-tuple-element.23.own_ref), channel_id=1, source_target_pairs={{0,8},{8,0},{1,9},{9,1},{2,10},{10,2},{3,11},{11,3},{4,12},{12,4},... | collective-permute-start | bytes 1769480 | tf_op jit(solution)/shard_map/ppermute | solution.py:716
  90.9 17.4 %collective-permute-start.1 = (bf16[16,72,128]{2,1,0:T(8,128)(2,1)S(1)}, bf16[16,72,128]{2,1,0:T(8,128)(2,1)S(1)}, u32[]{:S(2)}, u32[]{:S(2)}) collective-permute-start(bf16[16,72,128]{2,1,0:T(8,128)(2,1)S(1)} %all_to_all.26.own_ref), channel_id=1, source_target_pairs={{0,8},{8,0},{1,9},{9,1},{2,10},{10,2},{3,11},{11,3},{4,12},{12,4},... | collective-permute-start | bytes 884744 | tf_op jit(solution)/shard_map/ppermute | solution.py:731
  100.9 12.0 %copy-start = (bf16[3072,128]{1,0:T(8,128)(2,1)}, bf16[3072,128]{1,0:T(8,128)(2,1)S(1)}, u32[]{:S(2)}) copy-start(bf16[3072,128]{1,0:T(8,128)(2,1)S(1)} %pack_weights.1.refs_0_) | copy-start | bytes 2359300
  100.9 23.5 %collective-permute-start.3 = (bf16[3072,128]{1,0:T(8,128)(2,1)S(1)}, bf16[3072,128]{1,0:T(8,128)(2,1)}, u32[]{:S(2)}, u32[]{:S(2)}) collective-permute-start(bf16[3072,128]{1,0:T(8,128)(2,1)S(1)} %pack_weights.1.refs_0_), channel_id=1, source_target_pairs={{0,1},{1,2},{2,3},{3,4},{4,5},{5,6},{6,7},{7,0},{8,9},{9,10},{10,1... | collective-permute-start | bytes 2359304 | tf_op jit(solution)/shard_map/ppermute | solution.py:719
  104.2 21.0 %collective-permute-start.4 = (bf16[3072,128]{1,0:T(8,128)(2,1)S(1)}, bf16[3072,128]{1,0:T(8,128)(2,1)}, u32[]{:S(2)}, u32[]{:S(2)}) collective-permute-start(bf16[3072,128]{1,0:T(8,128)(2,1)S(1)} %pack_weights.1.refs_0_), channel_id=1, source_target_pairs={{0,7},{1,0},{2,1},{3,2},{4,3},{5,4},{6,5},{7,6},{8,15},{9,8},{10,9... | collective-permute-start | bytes 2359304 | tf_op jit(solution)/shard_map/ppermute | solution.py:719
  112.9 60.1 %all-to-all-start.2 = ((bf16[8,32,2048]{2,1,0:T(8,128)(2,1)}), bf16[8,32,2048]{2,1,0:T(8,128)(2,1)S(1)}, u32[]{:S(2)}, u32[]{:S(2)}) async-start(bf16[8,32,2048]{2,1,0:T(8,128)(2,1)} %bitcast.2), calls=%async_computation.2 | async-start | bytes 2097152 | tf_op jit(solution)/shard_map/all_to_all | solution.py:687
  119.1 53.7 %copy-start.10 = (s32[32]{0:T(128)S(1)}, s32[32]{0:T(128)}, u32[]{:S(2)}) copy-start(s32[32]{0:T(128)} %param.32) | copy-start | bytes 388
  119.1 53.7 %copy-start.9 = (s32[32,2]{0,1:T(2,128)S(1)}, s32[32,2]{0,1:T(2,128)}, u32[]{:S(2)}) copy-start(s32[32,2]{0,1:T(2,128)} %param.33) | copy-start | bytes 772
  119.1 53.9 %copy-start.1 = (bf16[32,2048]{1,0:T(8,128)(2,1)S(1)}, bf16[32,2048]{1,0:T(8,128)(2,1)}, u32[]{:S(2)}) copy-start(bf16[32,2048]{1,0:T(8,128)(2,1)} %res_ref.1) | copy-start | bytes 393220
  119.1 53.9 %copy-start.2 = (f32[2,2048]{1,0:T(2,128)S(1)}, f32[2,2048]{1,0:T(2,128)}, u32[]{:S(2)}) copy-start(f32[2,2048]{1,0:T(2,128)} %gain_ref.3) | copy-start | bytes 49156
  125.2 38.4 %collective-permute-start.5 = (bf16[3072,128]{1,0:T(8,128)(2,1)}, bf16[3072,128]{1,0:T(8,128)(2,1)S(1)}, u32[]{:S(2)}, u32[]{:S(2)}) collective-permute-start(bf16[3072,128]{1,0:T(8,128)(2,1)} %get-tuple-element.26.refs_1_), channel_id=1, source_target_pairs={{0,1},{1,2},{2,3},{3,4},{4,5},{5,6},{6,7},{7,0},{8,9},{9,10},{10,1... | collective-permute-start | bytes 2359304 | tf_op jit(solution)/shard_map/ppermute | solution.py:724
  128.3 36.3 %collective-permute-start.6 = (bf16[3072,128]{1,0:T(8,128)(2,1)}, bf16[3072,128]{1,0:T(8,128)(2,1)S(1)}, u32[]{:S(2)}, u32[]{:S(2)}) collective-permute-start(bf16[3072,128]{1,0:T(8,128)(2,1)} %get-tuple-element.27.refs_2_), channel_id=1, source_target_pairs={{0,7},{1,0},{2,1},{3,2},{4,3},{5,4},{6,5},{7,6},{8,15},{9,8},{10,9... | collective-permute-start | bytes 2359304 | tf_op jit(solution)/shard_map/ppermute | solution.py:724
  163.6 1.0 copy-start.5
  164.6 0.9 copy-start.6
  165.5 22.5 %collective-permute-start.7 = (bf16[3072,128]{1,0:T(8,128)(2,1)}, bf16[3072,128]{1,0:T(8,128)(2,1)S(1)}, u32[]{:S(2)}, u32[]{:S(2)}) collective-permute-start(bf16[3072,128]{1,0:T(8,128)(2,1)} %get-tuple-element.28.refs_3_), channel_id=1, source_target_pairs={{0,1},{1,2},{2,3},{3,4},{4,5},{5,6},{6,7},{7,0},{8,9},{9,10},{10,1... | collective-permute-start | bytes 2359304 | tf_op jit(solution)/shard_map/ppermute | solution.py:730
  168.4 21.6 %collective-permute-start.8 = (bf16[3072,128]{1,0:T(8,128)(2,1)}, bf16[3072,128]{1,0:T(8,128)(2,1)S(1)}, u32[]{:S(2)}, u32[]{:S(2)}) collective-permute-start(bf16[3072,128]{1,0:T(8,128)(2,1)} %get-tuple-element.29.refs_4_), channel_id=1, source_target_pairs={{0,7},{1,0},{2,1},{3,2},{4,3},{5,4},{6,5},{7,6},{8,15},{9,8},{10,9... | collective-permute-start | bytes 2359304 | tf_op jit(solution)/shard_map/ppermute | solution.py:730
  174.4 29.6 %all-to-all-start.3 = ((bf16[32,32,128]{2,1,0:T(8,128)(2,1)}), bf16[32,32,128]{2,1,0:T(8,128)(2,1)S(1)}, u32[]{:S(2)}, u32[]{:S(2)}) async-start(bf16[32,32,128]{2,1,0:T(8,128)(2,1)} %get-tuple-element.25), calls=%async_computation.3 | async-start | bytes 524288 | tf_op jit(solution)/shard_map/all_to_all | solution.py:687
  188.0 2.0 copy-start.3
  190.1 0.9 copy-start.4
  191.0 20.7 %collective-permute-start.9 = (bf16[3072,128]{1,0:T(8,128)(2,1)}, bf16[3072,128]{1,0:T(8,128)(2,1)S(1)}, u32[]{:S(2)}, u32[]{:S(2)}) collective-permute-start(bf16[3072,128]{1,0:T(8,128)(2,1)} %get-tuple-element.30.refs_5_), channel_id=1, source_target_pairs={{0,1},{1,2},{2,3},{3,4},{4,5},{5,6},{6,7},{7,0},{8,9},{9,10},{10,1... | collective-permute-start | bytes 2359304 | tf_op jit(solution)/shard_map/ppermute | solution.py:741
  204.0 10.5 %collective-permute-start.2 = (bf16[32,32,128]{2,1,0:T(8,128)(2,1)S(1)}, bf16[32,32,128]{2,1,0:T(8,128)(2,1)S(1)}, u32[]{:S(2)}, u32[]{:S(2)}) collective-permute-start(bf16[32,32,128]{2,1,0:T(8,128)(2,1)S(1)} %all-to-all-done.3.own_ref), channel_id=1, source_target_pairs={{0,256},{256,0},{1,257},{257,1},{2,258},{258,2},{3,259},{259,3},{4... | collective-permute-start | bytes 786440 | tf_op jit(solution)/shard_map/ppermute | solution.py:742
  211.7 2.9 %copy-start.7 = (bf16[3072,128]{1,0:T(8,128)(2,1)}, bf16[3072,128]{1,0:T(8,128)(2,1)S(1)}, u32[]{:S(2)}) copy-start(bf16[3072,128]{1,0:T(8,128)(2,1)S(1)} %collective-permute-done.9.refs_7_) | copy-start | bytes 2359300
  214.5 20.9 %copy-start.8 = (f32[32,2]{0,1:T(2,128)S(1)}, f32[32,2]{0,1:T(2,128)}, u32[]{:S(2)}) copy-start(f32[32,2]{0,1:T(2,128)} %param.34) | copy-start | bytes 772
  218.4 8.4 %collective-permute-start.10 = (bf16[64,2048]{1,0:T(8,128)(2,1)S(1)}, bf16[64,2048]{1,0:T(8,128)(2,1)S(1)}, u32[]{:S(2)}, u32[]{:S(2)}) collective-permute-start(bf16[64,2048]{1,0:T(8,128)(2,1)S(1)} %get-tuple-element.33), channel_id=1, source_target_pairs={{0,256},{256,0},{1,257},{257,1},{2,258},{258,2},{3,259},{259,3},{4... | collective-permute-start | bytes 786440 | tf_op jit(solution)/shard_map/ppermute | solution.py:744
  227.7 29.8 %all-to-all-start.4 = ((bf16[32,32,128]{2,1,0:T(8,128)(2,1)}), bf16[32,32,128]{2,1,0:T(8,128)(2,1)S(1)}, u32[]{:S(2)}, u32[]{:S(2)}) async-start(bf16[32,32,128]{2,1,0:T(8,128)(2,1)} %finish.1), calls=%async_computation.4 | async-start | bytes 524288 | tf_op jit(solution)/shard_map/all_to_all | solution.py:687

commit v6 on v5

--- a/solution.py
+++ b/solution.py
@@ -46,6 +46,10 @@
 
 def near_shape(shape, dtype):
     return jax.ShapeDtypeStruct(shape, dtype) if INTERPRET else pltpu.VMEM(shape, dtype)
+
+
+def far_shape(shape, dtype):
+    return jax.ShapeDtypeStruct(shape, dtype) if INTERPRET else pltpu.HBM(shape, dtype)
 
 
 SMEM_SPEC = pl.BlockSpec(memory_space=pltpu.SMEM)
@@ -188,9 +192,9 @@
     return pl.pallas_call(
         retention_body,
         out_shape=(
-            near_shape((n, dk), BF16),
-            near_shape((n, wb), BF16),
-            near_shape((n, dv + wb), F32),
+            far_shape((n, dk), BF16),
+            far_shape((n, wb), BF16),
+            far_shape((n, dv + wb), F32),
             near_shape((2, dk + 2 * TILE, dv), BF16),
             near_shape((8, n), F32),
         ),
@@ -346,14 +350,8 @@
 
 def mix_body(
     core_ref, qa_ref, qb_ref, loc_ref, own_ref, oth_ref, pay_ref, dec_ref, wa_ref, wb_ref,
-    out_ref, grp_scr, wa_scr, wb_scr, sems,
+    out_ref, grp_scr,
 ):
-    copies = [
-        pltpu.make_async_copy(wa_ref, wa_scr, sems.at[0]),
-        pltpu.make_async_copy(wb_ref, wb_scr, sems.at[1]),
-    ]
-    for copy in copies:
-        copy.start()
     n, dk = qa_ref.shape
     width = qb_ref.shape[1]
     hb = width // 2
@@ -421,9 +419,7 @@
     s0 = jnp.sum(jnp.where(left, sq, 0.0), axis=1, keepdims=True) / hb
     s1 = jnp.sum(jnp.where(left, 0.0, sq), axis=1, keepdims=True) / hb
     mixed_b = (total_b * lax.rsqrt(jnp.where(left, s0, s1) + GROUP_EPS)).astype(BF16)
-    for copy in copies:
-        copy.wait()
-    out_ref[...] = (mm(mixed_a, wa_scr[...]) + mm(mixed_b, wb_scr[...])).astype(BF16)
+    out_ref[...] = (mm(mixed_a, wa_ref[...]) + mm(mixed_b, wb_ref[...])).astype(BF16)
 
 
 def mix_project(core, qa, qb, loc, own, other, pay, dec, wa, wb):
@@ -431,18 +427,13 @@
     return pl.pallas_call(
         mix_body,
         out_shape=near_shape((qa.shape[0], wa.shape[1]), BF16),
-        in_specs=[SMEM_SPEC] + vmem(7) + [ANY_SPEC] * 2,
+        in_specs=[SMEM_SPEC] + vmem(9),
         out_specs=vmem(1)[0],
-        scratch_shapes=[
-            pltpu.VMEM((hb, qb.shape[1]), F32),
-            pltpu.VMEM(wa.shape, BF16),
-            pltpu.VMEM(wb.shape, BF16),
-            pltpu.SemaphoreType.DMA((2,)),
-        ],
+        scratch_shapes=[pltpu.VMEM((hb, qb.shape[1]), F32)],
         interpret=INTERPRET,
         compiler_params=PARAMS,
         name="mix_project",
-    )(core, *map(near, (qa, qb, loc, own, other, pay, dec)), far(wa), far(wb))
+    )(core, *map(far, (qa, qb, loc)), *map(near, (own, other, pay, dec, wa, wb)))
 
 
 def layer_norm(stream, gain):
@@ -526,6 +517,31 @@
         interpret=INTERPRET,
         compiler_params=PARAMS,
         name="hand_on",
+    )(*map(far, arrays))
+
+
+def fetch(*arrays):
+    count = len(arrays)
+
+    def body(*refs):
+        sems = refs[-1]
+        copies = [
+            pltpu.make_async_copy(refs[k], refs[count + k], sems.at[k]) for k in range(count)
+        ]
+        for copy in copies:
+            copy.start()
+        for copy in copies:
+            copy.wait()
+
+    return pl.pallas_call(
+        body,
+        out_shape=tuple(near_shape(x.shape, x.dtype) for x in arrays),
+        in_specs=[ANY_SPEC] * count,
+        out_specs=tuple(vmem(count)),
+        scratch_shapes=[pltpu.SemaphoreType.DMA((count,))],
+        interpret=INTERPRET,
+        compiler_params=PARAMS,
+        name="fetch",
     )(*map(far, arrays))
 
 
@@ -551,7 +567,7 @@
     _, width, units = gate.shape
     return pl.pallas_call(
         pack_weights_body,
-        out_shape=jax.ShapeDtypeStruct((width + width // 2, units), BF16),
+        out_shape=far_shape((width + width // 2, units), BF16),
         in_specs=[SMEM_SPEC] + vmem(3),
         out_specs=vmem(1)[0],
         interpret=INTERPRET,
@@ -562,13 +578,20 @@
 
 def expert_body(own_ref, oth_ref, *refs):
     *held, mine_ref, send_ref, x_scr, blocks, acc_ref, sems = refs
-    count, _, units = blocks.shape
+    fetched, _, units = blocks.shape
+    count = len(held)
     rows = mine_ref.shape[0]
     width = mine_ref.shape[1]
     half = units // 2
-    copies = [pltpu.make_async_copy(held[k], blocks.at[k], sems.at[k]) for k in range(count)]
+    copies = [pltpu.make_async_copy(held[k], blocks.at[k], sems.at[k]) for k in range(fetched)]
     for copy in copies:
         copy.start()
+
+    def weights(k, at, size):
+        if k < fetched:
+            return blocks[k, at : at + size, :]
+        return held[k][at : at + size, :]
+
     x = jnp.concatenate(
         [load_chunks(own_ref, rows, x_scr), load_chunks(oth_ref, rows, x_scr)], axis=0
     )
@@ -581,9 +604,12 @@
     for first in range(0, count, group):
         hidden = []
         for k in range(first, first + group, 2):
-            copies[k].wait()
-            copies[k + 1].wait()
-            both = mm(x, jnp.concatenate([blocks[k, :width, :], blocks[k + 1, :width, :]], axis=1))
+            for j in (k, k + 1):
+                if j < fetched:
+                    copies[j].wait()
+            both = mm(
+                x, jnp.concatenate([weights(k, 0, width), weights(k + 1, 0, width)], axis=1)
+            )
             one, two = both[:, :units], both[:, units:]
             one = silu(one) * pltpu.roll(one, half, 1)
             two = silu(pltpu.roll(two, half, 1)) * two
@@ -595,7 +621,7 @@
                 at = width + j * half
                 cols.append(
                     jnp.concatenate(
-                        [blocks[k, at : at + half, :] for k in range(first, first + group)], axis=0
+                        [weights(k, at, half) for k in range(first, first + group)], axis=0
                     )
                 )
             part = mm(hidden, jnp.concatenate(cols, axis=1))
@@ -610,7 +636,7 @@
                 send_ref[:, cut] = part[rows:].astype(BF16)
 
 
-def experts(own, other, blocks):
+def experts(own, other, blocks, late):
     depth, units = blocks[0].shape
     width = depth * 2 // 3
     lines = own.shape[0] * own.shape[1]
@@ -621,7 +647,7 @@
             near_shape((rows, width), F32),
             near_shape((rows, width), BF16),
         ),
-        in_specs=vmem(2) + [ANY_SPEC] * len(blocks),
+        in_specs=vmem(2) + [ANY_SPEC] * len(blocks) + vmem(len(late)),
         out_specs=tuple(vmem(2)),
         scratch_shapes=[
             pltpu.VMEM((lines, LANES), F32),
@@ -632,7 +658,7 @@
         interpret=INTERPRET,
         compiler_params=PARAMS,
         name="experts",
-    )(near(own), near(other), *map(far, blocks))
+    )(near(own), near(other), *map(far, blocks), *map(near, late))
 
 
 def finish_body(mine_ref, arrived_ref, out_ref, scr):
@@ -716,31 +742,38 @@
     pay_other = lax.ppermute(pay, "sp_1", swap)
     packed = pack_weights(part, expert_gate, expert_up, expert_down)
     blocks = [packed]
-    held = (lax.ppermute(packed, "tp", up_ring), lax.ppermute(packed, "tp", down_ring))
+
+    def start(array, ring):
+        return lax.ppermute(array, "tp", ring)
+
+    def arrive(array):
+        held = hand_on(array)[0]
+        blocks.append(held)
+        return held
+
+    above = start(packed, up_ring)
     outgoing_states = pack_states(core, pay, pay_other, chips)
     pieces = exchange(outgoing_states, "sp_0")
-    held = hand_on(*held)
-    blocks += held
-    held = (lax.ppermute(held[0], "tp", up_ring), lax.ppermute(held[1], "tp", down_ring))
+    below = start(packed, down_ring)
+    above = start(arrive(above), up_ring)
     per = value_a.shape[1] // LANES * TILE // chips
     scanned = scan_states(core, pieces, per)
     carried = exchange(scanned, "sp_0")
-    held = hand_on(*held)
-    blocks += held
-    held = (lax.ppermute(held[0], "tp", up_ring), lax.ppermute(held[1], "tp", down_ring))
+    below = start(arrive(below), down_ring)
+    above = start(arrive(above), up_ring)
+    out_a, out_b = fetch(out_weight_a, out_weight_b)
     carried_other = lax.ppermute(carried, "sp_1", swap)
     partial = mix_project(
-        core, qa, qb, loc, carried, carried_other, pay_other, dec, out_weight_a, out_weight_b
+        core, qa, qb, loc, carried, carried_other, pay_other, dec, out_a, out_b
     )
     arrived = exchange(partial.reshape(tp, rows_dev, width), "tp")
     ids = (route_group[:, None] * EXP_GROUP + route_expert).reshape(1, routes)
     hidden, outgoing = dispatch(arrived, residual, norm_gain, ids, sp_count)
     received = exchange(outgoing, SP)
-    held = hand_on(*held)
-    blocks += held
-    blocks.append(lax.ppermute(held[0], "tp", up_ring))
+    above = start(arrive(above), up_ring)
+    below = start(arrive(below), down_ring)
     received_other = lax.ppermute(received, "grp", partner)
-    mine, send = experts(received, received_other, blocks)
+    mine, send = experts(received, received_other, blocks, [above, below])
     arrived_sums = lax.ppermute(send, "grp", partner)
     back = finish(mine, arrived_sums, sp_count)
     returned = exchange(back, SP)

time: 260 us -> 256 us (0.985)
  waiting for transfers between devices: 90.1 us -> 83.6 us
  Pallas kernels: 17.2 us -> 20 us
    ppermute x7, starting transfers between devices: 26 us -> 22.2 us  [start(): return lax.ppermute(array, 'tp', ring)]
    pallas_call x2 -> x3, Pallas kernels: 4.63 us -> 8.02 us  [the longest x1 3.62 us: retention_local(): pl.pallas_call(retention_body, out_shape=(far_shape((n, dk), BF16), far_s...]
    ppermute x1, waiting for transfers between devices: 2.85 us -> 0.14 us  [shards(): received_other = lax.ppermute(received, 'grp', partner)]
  transfers between devices with their start and end apart: 14 -> 14, of which waited for: 12 -> 11; matrix products, arithmetic and copies ran while one was open for 0% -> 0% of each run, Pallas kernels for 3% -> 4%
where the time goes in v6:
time: 256 us; the launch traced here: 255 us
  starting transfers between devices  105 us (41%)
  waiting for transfers between devices  83.6 us (33%)
  blocking collectives  42.7 us (17%)
  Pallas kernels  20 us (8%)
  local copies, waits for them, and re-layouts  3.98 us (2%)
    ppermute x7, waiting for transfers between devices, start(): return lax.ppermute(array, 'tp', ring)  46.9 us
    ppermute x1, starting transfers between devices, shards(): pay_other = lax.ppermute(pay, 'sp_1', swap)  43.4 us
    all_to_all x2, blocking collectives, exchange(): return lax.all_to_all(array, axis, split_axis=0, concat_axis=0, tiled=True)  42.7 us
    all_to_all x3, waiting for transfers between devices, exchange(): return lax.all_to_all(array, axis, split_axis=0, concat_axis=0, tiled=True)  30.6 us
    all_to_all x3, starting transfers between devices, exchange(): return lax.all_to_all(array, axis, split_axis=0, concat_axis=0, tiled=True)  22.5 us
    ppermute x7, starting transfers between devices, start(): return lax.ppermute(array, 'tp', ring)  22.2 us
    ppermute x1, starting transfers between devices, shards(): carried_other = lax.ppermute(carried, 'sp_1', swap)  8.1 us
  transfers between devices with their start and end apart: 14, of which 11 were waited for; matrix products, arithmetic and copies ran while one was open for 0% of the time, Pallas kernels for 4%

profile of v6, /device:TPU:65, one launch (start us, length us, event | category | flops | bytes accessed | tf_op | source)
XLA Modules:
  0.0 255.4 jit_solution(10610117658130765990)
XLA Ops:
  0.0 3.6 %retention_local.1 = (bf16[256,256]{1,0:T(8,128)(2,1)}, bf16[256,128]{1,0:T(8,128)(2,1)}, f32[256,640]{1,0:T(8,128)}, bf16[2,288,512]{2,1,0:T(8,128)(2,1)S(1)}, f32[8,256]{1,0:T(8,128)S(1)}) custom-call(s32[1]{0:T(128)} %bitcast.1.index_ref, bf16[256,256]{1,0:T(8,128)(2,1)} %qa_ref.1, bf16[256,256]{1,0:T(8,128)(2,1)} %ka_ref.1, bf16[256,512]{1,0:T(8,128)(2,1)} %va_ref.1, ...), custom_call_target="tpu_custom_call" | custom-call | tf_op jit(solution)/shard_map/retention_local/pallas_call | solution.py:192
  3.6 43.4 %collective-permute-start = (bf16[2,288,512]{2,1,0:T(8,128)(2,1)S(1)}, bf16[2,288,512]{2,1,0:T(8,128)(2,1)S(1)}, u32[]{:S(2)}, u32[]{:S(2)}) collective-permute-start(bf16[2,288,512]{2,1,0:T(8,128)(2,1)S(1)} %get-tuple-element.19.own_ref), channel_id=1, source_target_pairs={{0,8},{8,0},{1,9},{9,1},{2,10},{10,2},{3,11},{11,3},{4,12},{12,4},... | collective-permute-start | bytes 1769480 | tf_op jit(solution)/shard_map/ppermute | solution.py:742
  47.0 1.6 collective-permute-done.oth_ref.pay_ref
  48.6 0.2 pack_states.1
  48.8 17.3 %all_to_all.25.refs_1_ = bf16[16,72,128]{2,1,0:T(8,128)(2,1)S(1)} all-to-all(bf16[16,72,128]{2,1,0:T(8,128)(2,1)S(1)} %pack_states.1), channel_id=1, replica_groups=mesh['grp'=2,'sp_0'=16,'sp_1'=2,'tp'=8] {'sp_0'}, dimensions={0} | all-to-all | bytes 589824 | tf_op jit(solution)/shard_map/all_to_all | solution.py:713
  66.2 0.2 scan_states.1
  66.4 25.4 %all_to_all.26.own_ref = bf16[16,72,128]{2,1,0:T(8,128)(2,1)S(1)} all-to-all(bf16[16,72,128]{2,1,0:T(8,128)(2,1)S(1)} %scan_states.1), channel_id=1, replica_groups=mesh['grp'=2,'sp_0'=16,'sp_1'=2,'tp'=8] {'sp_0'}, dimensions={0} | all-to-all | bytes 589824 | tf_op jit(solution)/shard_map/all_to_all | solution.py:713
  91.7 8.1 %collective-permute-start.1 = (bf16[16,72,128]{2,1,0:T(8,128)(2,1)S(1)}, bf16[16,72,128]{2,1,0:T(8,128)(2,1)S(1)}, u32[]{:S(2)}, u32[]{:S(2)}) collective-permute-start(bf16[16,72,128]{2,1,0:T(8,128)(2,1)S(1)} %all_to_all.26.own_ref), channel_id=1, source_target_pairs={{0,8},{8,0},{1,9},{9,1},{2,10},{10,2},{3,11},{11,3},{4,12},{12,4},... | collective-permute-start | bytes 884744 | tf_op jit(solution)/shard_map/ppermute | solution.py:765
  99.8 2.7 %pack_weights.1.refs_0_ = bf16[3072,128]{1,0:T(8,128)(2,1)} custom-call(s32[1]{0:T(128)} %bitcast.3.part_ref, bf16[1,2048,128]{2,1,0:T(8,128)(2,1)} %gate_ref.1, bf16[1,2048,128]{2,1,0:T(8,128)(2,1)} %up_ref.1, bf16[1,128,2048]{2,1,0:T(8,128)(2,1)} %down_ref.1), custom_call_target="tpu_custom_call" | custom-call | tf_op jit(solution)/shard_map/pack_weights/pallas_call | solution.py:568
  102.6 3.3 %collective-permute-start.3 = (bf16[3072,128]{1,0:T(8,128)(2,1)}, bf16[3072,128]{1,0:T(8,128)(2,1)S(1)}, u32[]{:S(2)}, u32[]{:S(2)}) collective-permute-start(bf16[3072,128]{1,0:T(8,128)(2,1)} %pack_weights.1.refs_0_), channel_id=1, source_target_pairs={{0,1},{1,2},{2,3},{3,4},{4,5},{5,6},{6,7},{7,0},{8,9},{9,10},{10,1... | collective-permute-start | bytes 2359304 | tf_op jit(solution)/shard_map/ppermute | solution.py:747
  105.8 1.7 fetch.1
  107.5 4.3 %mix_project.1 = bf16[256,2048]{1,0:T(8,128)(2,1)} custom-call(s32[1]{0:T(128)} %bitcast.core_ref.refs_0_, bf16[256,256]{1,0:T(8,128)(2,1)} %get-tuple-element.16.qa_ref, bf16[256,128]{1,0:T(8,128)(2,1)} %get-tuple-element.17.qb_ref, f32[256,640]{1,0:T(8,128)} %get-tuple-element.18.loc_ref, bf16[16,72,128]{2,1,0:T(8,128)(2,1)S(1)} %all_to_all.26.own_ref, ...), custom_call_target="tpu_custom_call" | custom-call | tf_op jit(solution)/shard_map/mix_project/pallas_call | solution.py:427
  111.9 6.3 %all-to-all-start.2 = ((bf16[8,32,2048]{2,1,0:T(8,128)(2,1)}), bf16[8,32,2048]{2,1,0:T(8,128)(2,1)S(1)}, u32[]{:S(2)}, u32[]{:S(2)}) async-start(bf16[8,32,2048]{2,1,0:T(8,128)(2,1)} %bitcast.2), calls=%async_computation.2 | async-start | bytes 2097152 | tf_op jit(solution)/shard_map/all_to_all | solution.py:713
  118.2 0.0 copy-start.9
  118.2 0.0 copy-start.8
  118.2 0.0 copy-start
  118.2 4.7 %collective-permute-start.4 = (bf16[3072,128]{1,0:T(8,128)(2,1)S(1)}, bf16[3072,128]{1,0:T(8,128)(2,1)S(1)}, u32[]{:S(2)}, u32[]{:S(2)}) collective-permute-start(bf16[3072,128]{1,0:T(8,128)(2,1)S(1)} %copy-done.2), channel_id=1, source_target_pairs={{0,7},{1,0},{2,1},{3,2},{4,3},{5,4},{6,5},{7,6},{8,15},{9,8},{10,9... | collective-permute-start | bytes 2359304 | tf_op jit(solution)/shard_map/ppermute | solution.py:747
  122.9 3.2 %collective-permute-done.3.refs_0_ = bf16[3072,128]{1,0:T(8,128)(2,1)S(1)} collective-permute-done((bf16[3072,128]{1,0:T(8,128)(2,1)}, bf16[3072,128]{1,0:T(8,128)(2,1)S(1)}, u32[]{:S(2)}, u32[]{:S(2)}) %collective-permute-start.3) | collective-permute-done | bytes 786464 | tf_op jit(solution)/shard_map/ppermute | solution.py:747
  126.1 0.9 copy-done.4
  127.0 1.9 collective-permute-start.5
  129.0 30.4 %collective-permute-done.4.refs_0_ = bf16[3072,128]{1,0:T(8,128)(2,1)S(1)} collective-permute-done((bf16[3072,128]{1,0:T(8,128)(2,1)S(1)}, bf16[3072,128]{1,0:T(8,128)(2,1)S(1)}, u32[]{:S(2)}, u32[]{:S(2)}) %collective-permute-start.4) | collective-permute-done | bytes 786464 | tf_op jit(solution)/shard_map/ppermute | solution.py:747
  159.4 0.9 copy-done.5
  160.2 3.4 %collective-permute-start.7 = (bf16[3072,128]{1,0:T(8,128)(2,1)}, bf16[3072,128]{1,0:T(8,128)(2,1)S(1)}, u32[]{:S(2)}, u32[]{:S(2)}) collective-permute-start(bf16[3072,128]{1,0:T(8,128)(2,1)} %hand_on.6.refs_2_), channel_id=1, source_target_pairs={{0,7},{1,0},{2,1},{3,2},{4,3},{5,4},{6,5},{7,6},{8,15},{9,8},{10,9... | collective-permute-start | bytes 2359304 | tf_op jit(solution)/shard_map/ppermute | solution.py:747
  163.7 1.8 collective-permute-done.5.refs_0_
  165.5 0.9 copy-done.6
  166.3 1.9 collective-permute-start.6
  168.3 0.1 copy.28
  168.4 0.1 reshape.23.ids_ref
  168.6 1.4 dispatch.1
  170.0 7.0 %all-to-all-start.3 = ((bf16[32,32,128]{2,1,0:T(8,128)(2,1)}), bf16[32,32,128]{2,1,0:T(8,128)(2,1)S(1)}, u32[]{:S(2)}, u32[]{:S(2)}) async-start(bf16[32,32,128]{2,1,0:T(8,128)(2,1)} %get-tuple-element.23), calls=%async_computation.3 | async-start | bytes 524288 | tf_op jit(solution)/shard_map/all_to_all | solution.py:713
  176.9 3.2 %collective-permute-done.7.refs_0_ = bf16[3072,128]{1,0:T(8,128)(2,1)S(1)} collective-permute-done((bf16[3072,128]{1,0:T(8,128)(2,1)}, bf16[3072,128]{1,0:T(8,128)(2,1)S(1)}, u32[]{:S(2)}, u32[]{:S(2)}) %collective-permute-start.7) | collective-permute-done | bytes 786464 | tf_op jit(solution)/shard_map/ppermute | solution.py:747
  180.1 0.9 copy-done.3
  181.0 4.8 %collective-permute-start.9 = (bf16[3072,128]{1,0:T(8,128)(2,1)}, bf16[3072,128]{1,0:T(8,128)(2,1)S(1)}, u32[]{:S(2)}, u32[]{:S(2)}) collective-permute-start(bf16[3072,128]{1,0:T(8,128)(2,1)} %hand_on.9.refs_5_), channel_id=1, source_target_pairs={{0,7},{1,0},{2,1},{3,2},{4,3},{5,4},{6,5},{7,6},{8,15},{9,8},{10,9... | collective-permute-start | bytes 2359304 | tf_op jit(solution)/shard_map/ppermute | solution.py:747
  185.9 2.4 collective-permute-done.6.refs_0_
  188.3 2.1 collective-permute-start.8
  190.4 8.7 %all-to-all-done.3.own_ref = bf16[32,32,128]{2,1,0:T(8,128)(2,1)S(1)} async-done(((bf16[32,32,128]{2,1,0:T(8,128)(2,1)}), bf16[32,32,128]{2,1,0:T(8,128)(2,1)S(1)}, u32[]{:S(2)}, u32[]{:S(2)}) %all-to-all-start.3) | async-done | bytes 262176 | tf_op jit(solution)/shard_map/all_to_all | solution.py:713
  199.0 4.4 %collective-permute-start.2 = (bf16[32,32,128]{2,1,0:T(8,128)(2,1)S(1)}, bf16[32,32,128]{2,1,0:T(8,128)(2,1)S(1)}, u32[]{:S(2)}, u32[]{:S(2)}) collective-permute-start(bf16[32,32,128]{2,1,0:T(8,128)(2,1)S(1)} %all-to-all-done.3.own_ref), channel_id=1, source_target_pairs={{0,256},{256,0},{1,257},{257,1},{2,258},{258,2},{3,259},{259,3},{4... | collective-permute-start | bytes 786440 | tf_op jit(solution)/shard_map/ppermute | solution.py:775
  203.5 5.9 %collective-permute-done.8.refs_6_ = bf16[3072,128]{1,0:T(8,128)(2,1)S(1)} collective-permute-done((bf16[3072,128]{1,0:T(8,128)(2,1)}, bf16[3072,128]{1,0:T(8,128)(2,1)S(1)}, u32[]{:S(2)}, u32[]{:S(2)}) %collective-permute-start.8) | collective-permute-done | bytes 786464 | tf_op jit(solution)/shard_map/ppermute | solution.py:747
  209.4 0.1 collective-permute-done.2.oth_ref
  209.6 3.4 %experts.1 = (f32[64,2048]{1,0:T(8,128)S(1)}, bf16[64,2048]{1,0:T(8,128)(2,1)S(1)}) custom-call(bf16[32,32,128]{2,1,0:T(8,128)(2,1)S(1)} %all-to-all-done.3.own_ref, bf16[32,32,128]{2,1,0:T(8,128)(2,1)S(1)} %collective-permute-done.2.oth_ref, bf16[3072,128]{1,0:T(8,128)(2,1)} %pack_weights.1.refs_0_, bf16[3072,128]{1,0:T(8,128)(2,1)} %hand_on.5.refs_1_, ...), custom_call_target="tpu_custom_call" | custom-call | tf_op jit(solution)/shard_map/experts/pallas_call | solution.py:644
  213.0 4.3 %collective-permute-start.10 = (bf16[64,2048]{1,0:T(8,128)(2,1)S(1)}, bf16[64,2048]{1,0:T(8,128)(2,1)S(1)}, u32[]{:S(2)}, u32[]{:S(2)}) collective-permute-start(bf16[64,2048]{1,0:T(8,128)(2,1)S(1)} %get-tuple-element.25), channel_id=1, source_target_pairs={{0,256},{256,0},{1,257},{257,1},{2,258},{258,2},{3,259},{259,3},{4... | collective-permute-start | bytes 786440 | tf_op jit(solution)/shard_map/ppermute | solution.py:777
  217.3 4.4 %collective-permute-done.10.arrived_ref = bf16[64,2048]{1,0:T(8,128)(2,1)S(1)} collective-permute-done((bf16[64,2048]{1,0:T(8,128)(2,1)S(1)}, bf16[64,2048]{1,0:T(8,128)(2,1)S(1)}, u32[]{:S(2)}, u32[]{:S(2)}) %collective-permute-start.10) | collective-permute-done | bytes 262176 | tf_op jit(solution)/shard_map/ppermute | solution.py:777
  221.6 0.9 finish.1
  222.5 9.3 %all-to-all-start.4 = ((bf16[32,32,128]{2,1,0:T(8,128)(2,1)}), bf16[32,32,128]{2,1,0:T(8,128)(2,1)S(1)}, u32[]{:S(2)}, u32[]{:S(2)}) async-start(bf16[32,32,128]{2,1,0:T(8,128)(2,1)} %finish.1), calls=%async_computation.4 | async-start | bytes 524288 | tf_op jit(solution)/shard_map/all_to_all | solution.py:713
  231.8 0.1 copy.29
  231.9 0.1 reshape.25.w_ref
  232.0 21.9 %all-to-all-done.4.ret_ref = bf16[32,32,128]{2,1,0:T(8,128)(2,1)S(1)} async-done(((bf16[32,32,128]{2,1,0:T(8,128)(2,1)}), bf16[32,32,128]{2,1,0:T(8,128)(2,1)S(1)}, u32[]{:S(2)}, u32[]{:S(2)}) %all-to-all-start.4) | async-done | bytes 262176 | tf_op jit(solution)/shard_map/all_to_all | solution.py:713
  253.9 1.5 combine.1
  (23 shorter events, 0.0 us)
Async XLA Ops:
  3.6 45.0 %collective-permute-start = (bf16[2,288,512]{2,1,0:T(8,128)(2,1)S(1)}, bf16[2,288,512]{2,1,0:T(8,128)(2,1)S(1)}, u32[]{:S(2)}, u32[]{:S(2)}) collective-permute-start(bf16[2,288,512]{2,1,0:T(8,128)(2,1)S(1)} %get-tuple-element.19.own_ref), channel_id=1, source_target_pairs={{0,8},{8,0},{1,9},{9,1},{2,10},{10,2},{3,11},{11,3},{4,12},{12,4},... | collective-permute-start | bytes 1769480 | tf_op jit(solution)/shard_map/ppermute | solution.py:742
  91.7 15.8 %collective-permute-start.1 = (bf16[16,72,128]{2,1,0:T(8,128)(2,1)S(1)}, bf16[16,72,128]{2,1,0:T(8,128)(2,1)S(1)}, u32[]{:S(2)}, u32[]{:S(2)}) collective-permute-start(bf16[16,72,128]{2,1,0:T(8,128)(2,1)S(1)} %all_to_all.26.own_ref), channel_id=1, source_target_pairs={{0,8},{8,0},{1,9},{9,1},{2,10},{10,2},{3,11},{11,3},{4,12},{12,4},... | collective-permute-start | bytes 884744 | tf_op jit(solution)/shard_map/ppermute | solution.py:765
  102.6 23.6 %collective-permute-start.3 = (bf16[3072,128]{1,0:T(8,128)(2,1)}, bf16[3072,128]{1,0:T(8,128)(2,1)S(1)}, u32[]{:S(2)}, u32[]{:S(2)}) collective-permute-start(bf16[3072,128]{1,0:T(8,128)(2,1)} %pack_weights.1.refs_0_), channel_id=1, source_target_pairs={{0,1},{1,2},{2,3},{3,4},{4,5},{5,6},{6,7},{7,0},{8,9},{9,10},{10,1... | collective-permute-start | bytes 2359304 | tf_op jit(solution)/shard_map/ppermute | solution.py:747
  111.9 6.3 %copy-start.2 = (bf16[3072,128]{1,0:T(8,128)(2,1)S(1)}, bf16[3072,128]{1,0:T(8,128)(2,1)}, u32[]{:S(2)}) copy-start(bf16[3072,128]{1,0:T(8,128)(2,1)} %pack_weights.1.refs_0_) | copy-start | bytes 2359300
  111.9 56.6 %all-to-all-start.2 = ((bf16[8,32,2048]{2,1,0:T(8,128)(2,1)}), bf16[8,32,2048]{2,1,0:T(8,128)(2,1)S(1)}, u32[]{:S(2)}, u32[]{:S(2)}) async-start(bf16[8,32,2048]{2,1,0:T(8,128)(2,1)} %bitcast.2), calls=%async_computation.2 | async-start | bytes 2097152 | tf_op jit(solution)/shard_map/all_to_all | solution.py:713
  118.2 50.1 %copy-start.9 = (s32[32]{0:T(128)S(1)}, s32[32]{0:T(128)}, u32[]{:S(2)}) copy-start(s32[32]{0:T(128)} %param.32) | copy-start | bytes 388
  118.2 50.1 %copy-start.8 = (s32[32,2]{0,1:T(2,128)S(1)}, s32[32,2]{0,1:T(2,128)}, u32[]{:S(2)}) copy-start(s32[32,2]{0,1:T(2,128)} %param.33) | copy-start | bytes 772
  118.2 50.4 %copy-start = (bf16[32,2048]{1,0:T(8,128)(2,1)S(1)}, bf16[32,2048]{1,0:T(8,128)(2,1)}, u32[]{:S(2)}) copy-start(bf16[32,2048]{1,0:T(8,128)(2,1)} %res_ref.1) | copy-start | bytes 393220
  118.2 50.4 %copy-start.1 = (f32[2,2048]{1,0:T(2,128)S(1)}, f32[2,2048]{1,0:T(2,128)}, u32[]{:S(2)}) copy-start(f32[2,2048]{1,0:T(2,128)} %gain_ref.3) | copy-start | bytes 49156
  118.2 41.1 %collective-permute-start.4 = (bf16[3072,128]{1,0:T(8,128)(2,1)S(1)}, bf16[3072,128]{1,0:T(8,128)(2,1)S(1)}, u32[]{:S(2)}, u32[]{:S(2)}) collective-permute-start(bf16[3072,128]{1,0:T(8,128)(2,1)S(1)} %copy-done.2), channel_id=1, source_target_pairs={{0,7},{1,0},{2,1},{3,2},{4,3},{5,4},{6,5},{7,6},{8,15},{9,8},{10,9... | collective-permute-start | bytes 2359304 | tf_op jit(solution)/shard_map/ppermute | solution.py:747
  126.1 0.9 copy-start.4
  127.0 38.4 %collective-permute-start.5 = (bf16[3072,128]{1,0:T(8,128)(2,1)}, bf16[3072,128]{1,0:T(8,128)(2,1)S(1)}, u32[]{:S(2)}, u32[]{:S(2)}) collective-permute-start(bf16[3072,128]{1,0:T(8,128)(2,1)} %hand_on.5.refs_1_), channel_id=1, source_target_pairs={{0,1},{1,2},{2,3},{3,4},{4,5},{5,6},{6,7},{7,0},{8,9},{9,10},{10,1... | collective-permute-start | bytes 2359304 | tf_op jit(solution)/shard_map/ppermute | solution.py:747
  159.4 0.9 copy-start.5
  160.2 19.9 %collective-permute-start.7 = (bf16[3072,128]{1,0:T(8,128)(2,1)}, bf16[3072,128]{1,0:T(8,128)(2,1)S(1)}, u32[]{:S(2)}, u32[]{:S(2)}) collective-permute-start(bf16[3072,128]{1,0:T(8,128)(2,1)} %hand_on.6.refs_2_), channel_id=1, source_target_pairs={{0,7},{1,0},{2,1},{3,2},{4,3},{5,4},{6,5},{7,6},{8,15},{9,8},{10,9... | collective-permute-start | bytes 2359304 | tf_op jit(solution)/shard_map/ppermute | solution.py:747
  165.5 0.9 copy-start.6
  166.3 21.9 %collective-permute-start.6 = (bf16[3072,128]{1,0:T(8,128)(2,1)}, bf16[3072,128]{1,0:T(8,128)(2,1)}, u32[]{:S(2)}, u32[]{:S(2)}) collective-permute-start(bf16[3072,128]{1,0:T(8,128)(2,1)} %hand_on.7.refs_3_), channel_id=1, source_target_pairs={{0,1},{1,2},{2,3},{3,4},{4,5},{5,6},{6,7},{7,0},{8,9},{9,10},{10,1... | collective-permute-start | bytes 2359304 | tf_op jit(solution)/shard_map/ppermute | solution.py:747
  170.0 29.1 %all-to-all-start.3 = ((bf16[32,32,128]{2,1,0:T(8,128)(2,1)}), bf16[32,32,128]{2,1,0:T(8,128)(2,1)S(1)}, u32[]{:S(2)}, u32[]{:S(2)}) async-start(bf16[32,32,128]{2,1,0:T(8,128)(2,1)} %get-tuple-element.23), calls=%async_computation.3 | async-start | bytes 524288 | tf_op jit(solution)/shard_map/all_to_all | solution.py:713
  180.1 0.9 copy-start.3
  181.0 22.4 %collective-permute-start.9 = (bf16[3072,128]{1,0:T(8,128)(2,1)}, bf16[3072,128]{1,0:T(8,128)(2,1)S(1)}, u32[]{:S(2)}, u32[]{:S(2)}) collective-permute-start(bf16[3072,128]{1,0:T(8,128)(2,1)} %hand_on.9.refs_5_), channel_id=1, source_target_pairs={{0,7},{1,0},{2,1},{3,2},{4,3},{5,4},{6,5},{7,6},{8,15},{9,8},{10,9... | collective-permute-start | bytes 2359304 | tf_op jit(solution)/shard_map/ppermute | solution.py:747
  188.3 43.5 %copy-start.7 = (f32[32,2]{0,1:T(2,128)S(1)}, f32[32,2]{0,1:T(2,128)}, u32[]{:S(2)}) copy-start(f32[32,2]{0,1:T(2,128)} %param.34) | copy-start | bytes 772
  188.3 21.1 %collective-permute-start.8 = (bf16[3072,128]{1,0:T(8,128)(2,1)}, bf16[3072,128]{1,0:T(8,128)(2,1)S(1)}, u32[]{:S(2)}, u32[]{:S(2)}) collective-permute-start(bf16[3072,128]{1,0:T(8,128)(2,1)} %hand_on.8.refs_4_), channel_id=1, source_target_pairs={{0,1},{1,2},{2,3},{3,4},{4,5},{5,6},{6,7},{7,0},{8,9},{9,10},{10,1... | collective-permute-start | bytes 2359304 | tf_op jit(solution)/shard_map/ppermute | solution.py:747
  199.0 10.5 %collective-permute-start.2 = (bf16[32,32,128]{2,1,0:T(8,128)(2,1)S(1)}, bf16[32,32,128]{2,1,0:T(8,128)(2,1)S(1)}, u32[]{:S(2)}, u32[]{:S(2)}) collective-permute-start(bf16[32,32,128]{2,1,0:T(8,128)(2,1)S(1)} %all-to-all-done.3.own_ref), channel_id=1, source_target_pairs={{0,256},{256,0},{1,257},{257,1},{2,258},{258,2},{3,259},{259,3},{4... | collective-permute-start | bytes 786440 | tf_op jit(solution)/shard_map/ppermute | solution.py:775
  213.0 8.7 %collective-permute-start.10 = (bf16[64,2048]{1,0:T(8,128)(2,1)S(1)}, bf16[64,2048]{1,0:T(8,128)(2,1)S(1)}, u32[]{:S(2)}, u32[]{:S(2)}) collective-permute-start(bf16[64,2048]{1,0:T(8,128)(2,1)S(1)} %get-tuple-element.25), channel_id=1, source_target_pairs={{0,256},{256,0},{1,257},{257,1},{2,258},{258,2},{3,259},{259,3},{4... | collective-permute-start | bytes 786440 | tf_op jit(solution)/shard_map/ppermute | solution.py:777
  222.5 31.4 %all-to-all-start.4 = ((bf16[32,32,128]{2,1,0:T(8,128)(2,1)}), bf16[32,32,128]{2,1,0:T(8,128)(2,1)S(1)}, u32[]{:S(2)}, u32[]{:S(2)}) async-start(bf16[32,32,128]{2,1,0:T(8,128)(2,1)} %finish.1), calls=%async_computation.4 | async-start | bytes 524288 | tf_op jit(solution)/shard_map/all_to_all | solution.py:713

commit v7 on v6

--- a/solution.py
+++ b/solution.py
@@ -46,10 +46,6 @@
 
 def near_shape(shape, dtype):
     return jax.ShapeDtypeStruct(shape, dtype) if INTERPRET else pltpu.VMEM(shape, dtype)
-
-
-def far_shape(shape, dtype):
-    return jax.ShapeDtypeStruct(shape, dtype) if INTERPRET else pltpu.HBM(shape, dtype)
 
 
 SMEM_SPEC = pl.BlockSpec(memory_space=pltpu.SMEM)
@@ -192,9 +188,9 @@
     return pl.pallas_call(
         retention_body,
         out_shape=(
-            far_shape((n, dk), BF16),
-            far_shape((n, wb), BF16),
-            far_shape((n, dv + wb), F32),
+            near_shape((n, dk), BF16),
+            near_shape((n, wb), BF16),
+            near_shape((n, dv + wb), F32),
             near_shape((2, dk + 2 * TILE, dv), BF16),
             near_shape((8, n), F32),
         ),
@@ -433,7 +429,7 @@
         interpret=INTERPRET,
         compiler_params=PARAMS,
         name="mix_project",
-    )(core, *map(far, (qa, qb, loc)), *map(near, (own, other, pay, dec, wa, wb)))
+    )(core, *map(near, (qa, qb, loc, own, other, pay, dec, wa, wb)))
 
 
 def layer_norm(stream, gain):
@@ -567,7 +563,7 @@
     _, width, units = gate.shape
     return pl.pallas_call(
         pack_weights_body,
-        out_shape=far_shape((width + width // 2, units), BF16),
+        out_shape=jax.ShapeDtypeStruct((width + width // 2, units), BF16),
         in_specs=[SMEM_SPEC] + vmem(3),
         out_specs=vmem(1)[0],
         interpret=INTERPRET,

time: 256 us -> 254 us (level)
  Pallas kernels: 20 us -> 17.1 us
  transfers between devices with their start and end apart: 14 -> 14, of which waited for: 11 -> 11; matrix products, arithmetic and copies ran while one was open for 0% -> 0% of each run, Pallas kernels for 4% -> 3%
where the time goes in v7:
time: 254 us
  starting transfers between devices  105 us (41%)
  waiting for transfers between devices  85.6 us (34%)
  blocking collectives  42.7 us (17%)
  Pallas kernels  17.1 us (7%)
  local copies, waits for them, and re-layouts  3.06 us (1%)
    ppermute x7, waiting for transfers between devices, start(): return lax.ppermute(array, 'tp', ring)  49 us
    ppermute x1, starting transfers between devices, shards(): pay_other = lax.ppermute(pay, 'sp_1', swap)  43.4 us
    all_to_all x2, blocking collectives, exchange(): return lax.all_to_all(array, axis, split_axis=0, concat_axis=0, tiled=True)  42.7 us
    all_to_all x3, waiting for transfers between devices, exchange(): return lax.all_to_all(array, axis, split_axis=0, concat_axis=0, tiled=True)  30.6 us
    all_to_all x3, starting transfers between devices, exchange(): return lax.all_to_all(array, axis, split_axis=0, concat_axis=0, tiled=True)  22.4 us
    ppermute x7, starting transfers between devices, start(): return lax.ppermute(array, 'tp', ring)  22.2 us
    ppermute x1, starting transfers between devices, shards(): carried_other = lax.ppermute(carried, 'sp_1', swap)  8.1 us
  transfers between devices with their start and end apart: 14, of which 11 were waited for; matrix products, arithmetic and copies ran while one was open for 0% of the time, Pallas kernels for 3%

profile of v7, /device:TPU:65, one launch (start us, length us, event | category | flops | bytes accessed | tf_op | source)
XLA Modules:
  0.0 253.5 jit_solution(16718721742196186404)
XLA Ops:
  0.0 2.8 %retention_local.1 = (bf16[256,256]{1,0:T(8,128)(2,1)S(1)}, bf16[256,128]{1,0:T(8,128)(2,1)S(1)}, f32[256,640]{1,0:T(8,128)S(1)}, bf16[2,288,512]{2,1,0:T(8,128)(2,1)S(1)}, f32[8,256]{1,0:T(8,128)S(1)}) custom-call(s32[1]{0:T(128)} %bitcast.1.index_ref, bf16[256,256]{1,0:T(8,128)(2,1)} %qa_ref.1, bf16[256,256]{1,0:T(8,128)(2,1)} %ka_ref.1, ...), custom_call_target="tpu_custom_call" | custom-call | tf_op jit(solution)/shard_map/retention_local/pallas_call | solution.py:188
  2.8 43.4 %collective-permute-start = (bf16[2,288,512]{2,1,0:T(8,128)(2,1)S(1)}, bf16[2,288,512]{2,1,0:T(8,128)(2,1)S(1)}, u32[]{:S(2)}, u32[]{:S(2)}) collective-permute-start(bf16[2,288,512]{2,1,0:T(8,128)(2,1)S(1)} %get-tuple-element.19.own_ref), channel_id=1, source_target_pairs={{0,8},{8,0},{1,9},{9,1},{2,10},{10,2},{3,11},{11,3},{4,12},{12,4},... | collective-permute-start | bytes 1769480 | tf_op jit(solution)/shard_map/ppermute | solution.py:738
  46.2 1.6 collective-permute-done.oth_ref.pay_ref
  47.8 0.2 pack_states.1
  48.0 17.3 %all_to_all.25.refs_1_ = bf16[16,72,128]{2,1,0:T(8,128)(2,1)S(1)} all-to-all(bf16[16,72,128]{2,1,0:T(8,128)(2,1)S(1)} %pack_states.1), channel_id=1, replica_groups=mesh['grp'=2,'sp_0'=16,'sp_1'=2,'tp'=8] {'sp_0'}, dimensions={0} | all-to-all | bytes 589824 | tf_op jit(solution)/shard_map/all_to_all | solution.py:709
  65.3 0.2 scan_states.1
  65.5 25.4 %all_to_all.26.own_ref = bf16[16,72,128]{2,1,0:T(8,128)(2,1)S(1)} all-to-all(bf16[16,72,128]{2,1,0:T(8,128)(2,1)S(1)} %scan_states.1), channel_id=1, replica_groups=mesh['grp'=2,'sp_0'=16,'sp_1'=2,'tp'=8] {'sp_0'}, dimensions={0} | all-to-all | bytes 589824 | tf_op jit(solution)/shard_map/all_to_all | solution.py:709
  90.9 8.1 %collective-permute-start.1 = (bf16[16,72,128]{2,1,0:T(8,128)(2,1)S(1)}, bf16[16,72,128]{2,1,0:T(8,128)(2,1)S(1)}, u32[]{:S(2)}, u32[]{:S(2)}) collective-permute-start(bf16[16,72,128]{2,1,0:T(8,128)(2,1)S(1)} %all_to_all.26.own_ref), channel_id=1, source_target_pairs={{0,8},{8,0},{1,9},{9,1},{2,10},{10,2},{3,11},{11,3},{4,12},{12,4},... | collective-permute-start | bytes 884744 | tf_op jit(solution)/shard_map/ppermute | solution.py:761
  99.0 1.9 pack_weights.1.refs_0_
  100.9 3.3 %collective-permute-start.3 = (bf16[3072,128]{1,0:T(8,128)(2,1)S(1)}, bf16[3072,128]{1,0:T(8,128)(2,1)}, u32[]{:S(2)}, u32[]{:S(2)}) collective-permute-start(bf16[3072,128]{1,0:T(8,128)(2,1)S(1)} %pack_weights.1.refs_0_), channel_id=1, source_target_pairs={{0,1},{1,2},{2,3},{3,4},{4,5},{5,6},{6,7},{7,0},{8,9},{9,10},{10,1... | collective-permute-start | bytes 2359304 | tf_op jit(solution)/shard_map/ppermute | solution.py:743
  104.2 1.7 fetch.1
  105.9 3.1 %mix_project.1 = bf16[256,2048]{1,0:T(8,128)(2,1)} custom-call(s32[1]{0:T(128)} %bitcast.core_ref.refs_0_, bf16[256,256]{1,0:T(8,128)(2,1)S(1)} %get-tuple-element.16.qa_ref, bf16[256,128]{1,0:T(8,128)(2,1)S(1)} %get-tuple-element.17.qb_ref, f32[256,640]{1,0:T(8,128)S(1)} %get-tuple-element.18.loc_ref, bf16[16,72,128]{2,1,0:T(8,128)(2,1)S(1)} %all_to_all.26.own_ref, ...), custom_call_target="tpu_custom_call" | custom-call | tf_op jit(solution)/shard_map/mix_project/pallas_call | solution.py:423
  109.0 6.1 %all-to-all-start.2 = ((bf16[8,32,2048]{2,1,0:T(8,128)(2,1)}), bf16[8,32,2048]{2,1,0:T(8,128)(2,1)S(1)}, u32[]{:S(2)}, u32[]{:S(2)}) async-start(bf16[8,32,2048]{2,1,0:T(8,128)(2,1)} %bitcast.2), calls=%async_computation.2 | async-start | bytes 2097152 | tf_op jit(solution)/shard_map/all_to_all | solution.py:709
  115.2 0.0 copy-start.8
  115.2 0.0 copy-start.7
  115.2 0.0 copy-start.1
  115.2 0.0 copy-start.2
  115.2 4.7 %collective-permute-start.4 = (bf16[3072,128]{1,0:T(8,128)(2,1)S(1)}, bf16[3072,128]{1,0:T(8,128)(2,1)S(1)}, u32[]{:S(2)}, u32[]{:S(2)}) collective-permute-start(bf16[3072,128]{1,0:T(8,128)(2,1)S(1)} %pack_weights.1.refs_0_), channel_id=1, source_target_pairs={{0,7},{1,0},{2,1},{3,2},{4,3},{5,4},{6,5},{7,6},{8,15},{9,8},{10,9... | collective-permute-start | bytes 2359304 | tf_op jit(solution)/shard_map/ppermute | solution.py:743
  119.9 4.4 %collective-permute-done.3.refs_0_ = bf16[3072,128]{1,0:T(8,128)(2,1)} collective-permute-done((bf16[3072,128]{1,0:T(8,128)(2,1)S(1)}, bf16[3072,128]{1,0:T(8,128)(2,1)}, u32[]{:S(2)}, u32[]{:S(2)}) %collective-permute-start.3) | collective-permute-done | bytes 786464 | tf_op jit(solution)/shard_map/ppermute | solution.py:743
  124.4 1.9 collective-permute-start.5
  126.3 30.0 %collective-permute-done.4.refs_0_ = bf16[3072,128]{1,0:T(8,128)(2,1)S(1)} collective-permute-done((bf16[3072,128]{1,0:T(8,128)(2,1)S(1)}, bf16[3072,128]{1,0:T(8,128)(2,1)S(1)}, u32[]{:S(2)}, u32[]{:S(2)}) %collective-permute-start.4) | collective-permute-done | bytes 786464 | tf_op jit(solution)/shard_map/ppermute | solution.py:743
  156.4 0.9 copy-done.4
  157.2 3.4 %collective-permute-start.7 = (bf16[3072,128]{1,0:T(8,128)(2,1)}, bf16[3072,128]{1,0:T(8,128)(2,1)S(1)}, u32[]{:S(2)}, u32[]{:S(2)}) collective-permute-start(bf16[3072,128]{1,0:T(8,128)(2,1)} %hand_on.6.refs_2_), channel_id=1, source_target_pairs={{0,7},{1,0},{2,1},{3,2},{4,3},{5,4},{6,5},{7,6},{8,15},{9,8},{10,9... | collective-permute-start | bytes 2359304 | tf_op jit(solution)/shard_map/ppermute | solution.py:743
  160.7 2.9 %collective-permute-done.5.refs_0_ = bf16[3072,128]{1,0:T(8,128)(2,1)S(1)} collective-permute-done((bf16[3072,128]{1,0:T(8,128)(2,1)}, bf16[3072,128]{1,0:T(8,128)(2,1)S(1)}, u32[]{:S(2)}, u32[]{:S(2)}) %collective-permute-start.5) | collective-permute-done | bytes 786464 | tf_op jit(solution)/shard_map/ppermute | solution.py:743
  163.6 0.9 copy-done.5
  164.5 1.9 collective-permute-start.6
  166.5 0.1 copy.28
  166.6 0.1 reshape.23.ids_ref
  166.7 1.4 dispatch.1
  168.1 7.0 %all-to-all-start.3 = ((bf16[32,32,128]{2,1,0:T(8,128)(2,1)}), bf16[32,32,128]{2,1,0:T(8,128)(2,1)S(1)}, u32[]{:S(2)}, u32[]{:S(2)}) async-start(bf16[32,32,128]{2,1,0:T(8,128)(2,1)} %get-tuple-element.23), calls=%async_computation.3 | async-start | bytes 524288 | tf_op jit(solution)/shard_map/all_to_all | solution.py:709
  175.1 2.1 collective-permute-done.7.refs_0_
  177.1 0.9 copy-done.3
  178.0 4.8 %collective-permute-start.9 = (bf16[3072,128]{1,0:T(8,128)(2,1)}, bf16[3072,128]{1,0:T(8,128)(2,1)S(1)}, u32[]{:S(2)}, u32[]{:S(2)}) collective-permute-start(bf16[3072,128]{1,0:T(8,128)(2,1)} %hand_on.9.refs_5_), channel_id=1, source_target_pairs={{0,7},{1,0},{2,1},{3,2},{4,3},{5,4},{6,5},{7,6},{8,15},{9,8},{10,9... | collective-permute-start | bytes 2359304 | tf_op jit(solution)/shard_map/ppermute | solution.py:743
  182.8 3.6 %collective-permute-done.6.refs_0_ = bf16[3072,128]{1,0:T(8,128)(2,1)} collective-permute-done((bf16[3072,128]{1,0:T(8,128)(2,1)}, bf16[3072,128]{1,0:T(8,128)(2,1)}, u32[]{:S(2)}, u32[]{:S(2)}) %collective-permute-start.6) | collective-permute-done | bytes 786464 | tf_op jit(solution)/shard_map/ppermute | solution.py:743
  186.4 2.1 collective-permute-start.8
  188.5 8.7 %all-to-all-done.3.own_ref = bf16[32,32,128]{2,1,0:T(8,128)(2,1)S(1)} async-done(((bf16[32,32,128]{2,1,0:T(8,128)(2,1)}), bf16[32,32,128]{2,1,0:T(8,128)(2,1)S(1)}, u32[]{:S(2)}, u32[]{:S(2)}) %all-to-all-start.3) | async-done | bytes 262176 | tf_op jit(solution)/shard_map/all_to_all | solution.py:709
  197.2 4.4 %collective-permute-start.2 = (bf16[32,32,128]{2,1,0:T(8,128)(2,1)S(1)}, bf16[32,32,128]{2,1,0:T(8,128)(2,1)S(1)}, u32[]{:S(2)}, u32[]{:S(2)}) collective-permute-start(bf16[32,32,128]{2,1,0:T(8,128)(2,1)S(1)} %all-to-all-done.3.own_ref), channel_id=1, source_target_pairs={{0,256},{256,0},{1,257},{257,1},{2,258},{258,2},{3,259},{259,3},{4... | collective-permute-start | bytes 786440 | tf_op jit(solution)/shard_map/ppermute | solution.py:771
  201.6 5.9 %collective-permute-done.8.refs_6_ = bf16[3072,128]{1,0:T(8,128)(2,1)S(1)} collective-permute-done((bf16[3072,128]{1,0:T(8,128)(2,1)}, bf16[3072,128]{1,0:T(8,128)(2,1)S(1)}, u32[]{:S(2)}, u32[]{:S(2)}) %collective-permute-start.8) | collective-permute-done | bytes 786464 | tf_op jit(solution)/shard_map/ppermute | solution.py:743
  207.6 0.1 collective-permute-done.2.oth_ref
  207.7 3.4 %experts.1 = (f32[64,2048]{1,0:T(8,128)S(1)}, bf16[64,2048]{1,0:T(8,128)(2,1)S(1)}) custom-call(bf16[32,32,128]{2,1,0:T(8,128)(2,1)S(1)} %all-to-all-done.3.own_ref, bf16[32,32,128]{2,1,0:T(8,128)(2,1)S(1)} %collective-permute-done.2.oth_ref, bf16[3072,128]{1,0:T(8,128)(2,1)} %copy-done, bf16[3072,128]{1,0:T(8,128)(2,1)} %hand_on.5.refs_1_, ...), custom_call_target="tpu_custom_call" | custom-call | tf_op jit(solution)/shard_map/experts/pallas_call | solution.py:640
  211.1 4.3 %collective-permute-start.10 = (bf16[64,2048]{1,0:T(8,128)(2,1)S(1)}, bf16[64,2048]{1,0:T(8,128)(2,1)S(1)}, u32[]{:S(2)}, u32[]{:S(2)}) collective-permute-start(bf16[64,2048]{1,0:T(8,128)(2,1)S(1)} %get-tuple-element.25), channel_id=1, source_target_pairs={{0,256},{256,0},{1,257},{257,1},{2,258},{258,2},{3,259},{259,3},{4... | collective-permute-start | bytes 786440 | tf_op jit(solution)/shard_map/ppermute | solution.py:773
  215.4 4.3 %collective-permute-done.10.arrived_ref = bf16[64,2048]{1,0:T(8,128)(2,1)S(1)} collective-permute-done((bf16[64,2048]{1,0:T(8,128)(2,1)S(1)}, bf16[64,2048]{1,0:T(8,128)(2,1)S(1)}, u32[]{:S(2)}, u32[]{:S(2)}) %collective-permute-start.10) | collective-permute-done | bytes 262176 | tf_op jit(solution)/shard_map/ppermute | solution.py:773
  219.8 0.9 finish.1
  220.6 9.3 %all-to-all-start.4 = ((bf16[32,32,128]{2,1,0:T(8,128)(2,1)}), bf16[32,32,128]{2,1,0:T(8,128)(2,1)S(1)}, u32[]{:S(2)}, u32[]{:S(2)}) async-start(bf16[32,32,128]{2,1,0:T(8,128)(2,1)} %finish.1), calls=%async_computation.4 | async-start | bytes 524288 | tf_op jit(solution)/shard_map/all_to_all | solution.py:709
  229.9 0.1 copy.29
  230.0 0.1 reshape.25.w_ref
  230.1 21.9 %all-to-all-done.4.ret_ref = bf16[32,32,128]{2,1,0:T(8,128)(2,1)S(1)} async-done(((bf16[32,32,128]{2,1,0:T(8,128)(2,1)}), bf16[32,32,128]{2,1,0:T(8,128)(2,1)S(1)}, u32[]{:S(2)}, u32[]{:S(2)}) %all-to-all-start.4) | async-done | bytes 262176 | tf_op jit(solution)/shard_map/all_to_all | solution.py:709
  252.0 1.5 combine.1
  (21 shorter events, 0.0 us)
Async XLA Ops:
  2.8 45.0 %collective-permute-start = (bf16[2,288,512]{2,1,0:T(8,128)(2,1)S(1)}, bf16[2,288,512]{2,1,0:T(8,128)(2,1)S(1)}, u32[]{:S(2)}, u32[]{:S(2)}) collective-permute-start(bf16[2,288,512]{2,1,0:T(8,128)(2,1)S(1)} %get-tuple-element.19.own_ref), channel_id=1, source_target_pairs={{0,8},{8,0},{1,9},{9,1},{2,10},{10,2},{3,11},{11,3},{4,12},{12,4},... | collective-permute-start | bytes 1769480 | tf_op jit(solution)/shard_map/ppermute | solution.py:738
  90.9 15.0 %collective-permute-start.1 = (bf16[16,72,128]{2,1,0:T(8,128)(2,1)S(1)}, bf16[16,72,128]{2,1,0:T(8,128)(2,1)S(1)}, u32[]{:S(2)}, u32[]{:S(2)}) collective-permute-start(bf16[16,72,128]{2,1,0:T(8,128)(2,1)S(1)} %all_to_all.26.own_ref), channel_id=1, source_target_pairs={{0,8},{8,0},{1,9},{9,1},{2,10},{10,2},{3,11},{11,3},{4,12},{12,4},... | collective-permute-start | bytes 884744 | tf_op jit(solution)/shard_map/ppermute | solution.py:761
  100.9 14.3 %copy-start = (bf16[3072,128]{1,0:T(8,128)(2,1)}, bf16[3072,128]{1,0:T(8,128)(2,1)S(1)}, u32[]{:S(2)}) copy-start(bf16[3072,128]{1,0:T(8,128)(2,1)S(1)} %pack_weights.1.refs_0_) | copy-start | bytes 2359300
  100.9 23.5 %collective-permute-start.3 = (bf16[3072,128]{1,0:T(8,128)(2,1)S(1)}, bf16[3072,128]{1,0:T(8,128)(2,1)}, u32[]{:S(2)}, u32[]{:S(2)}) collective-permute-start(bf16[3072,128]{1,0:T(8,128)(2,1)S(1)} %pack_weights.1.refs_0_), channel_id=1, source_target_pairs={{0,1},{1,2},{2,3},{3,4},{4,5},{5,6},{6,7},{7,0},{8,9},{9,10},{10,1... | collective-permute-start | bytes 2359304 | tf_op jit(solution)/shard_map/ppermute | solution.py:743
  109.0 57.6 %all-to-all-start.2 = ((bf16[8,32,2048]{2,1,0:T(8,128)(2,1)}), bf16[8,32,2048]{2,1,0:T(8,128)(2,1)S(1)}, u32[]{:S(2)}, u32[]{:S(2)}) async-start(bf16[8,32,2048]{2,1,0:T(8,128)(2,1)} %bitcast.2), calls=%async_computation.2 | async-start | bytes 2097152 | tf_op jit(solution)/shard_map/all_to_all | solution.py:709
  115.2 51.3 %copy-start.8 = (s32[32]{0:T(128)S(1)}, s32[32]{0:T(128)}, u32[]{:S(2)}) copy-start(s32[32]{0:T(128)} %param.32) | copy-start | bytes 388
  115.2 51.3 %copy-start.7 = (s32[32,2]{0,1:T(2,128)S(1)}, s32[32,2]{0,1:T(2,128)}, u32[]{:S(2)}) copy-start(s32[32,2]{0,1:T(2,128)} %param.33) | copy-start | bytes 772
  115.2 51.5 %copy-start.1 = (bf16[32,2048]{1,0:T(8,128)(2,1)S(1)}, bf16[32,2048]{1,0:T(8,128)(2,1)}, u32[]{:S(2)}) copy-start(bf16[32,2048]{1,0:T(8,128)(2,1)} %res_ref.1) | copy-start | bytes 393220
  115.2 51.5 %copy-start.2 = (f32[2,2048]{1,0:T(2,128)S(1)}, f32[2,2048]{1,0:T(2,128)}, u32[]{:S(2)}) copy-start(f32[2,2048]{1,0:T(2,128)} %gain_ref.3) | copy-start | bytes 49156
  115.2 41.1 %collective-permute-start.4 = (bf16[3072,128]{1,0:T(8,128)(2,1)S(1)}, bf16[3072,128]{1,0:T(8,128)(2,1)S(1)}, u32[]{:S(2)}, u32[]{:S(2)}) collective-permute-start(bf16[3072,128]{1,0:T(8,128)(2,1)S(1)} %pack_weights.1.refs_0_), channel_id=1, source_target_pairs={{0,7},{1,0},{2,1},{3,2},{4,3},{5,4},{6,5},{7,6},{8,15},{9,8},{10,9... | collective-permute-start | bytes 2359304 | tf_op jit(solution)/shard_map/ppermute | solution.py:743
  124.4 39.2 %collective-permute-start.5 = (bf16[3072,128]{1,0:T(8,128)(2,1)}, bf16[3072,128]{1,0:T(8,128)(2,1)S(1)}, u32[]{:S(2)}, u32[]{:S(2)}) collective-permute-start(bf16[3072,128]{1,0:T(8,128)(2,1)} %hand_on.5.refs_1_), channel_id=1, source_target_pairs={{0,1},{1,2},{2,3},{3,4},{4,5},{5,6},{6,7},{7,0},{8,9},{9,10},{10,1... | collective-permute-start | bytes 2359304 | tf_op jit(solution)/shard_map/ppermute | solution.py:743
  156.4 0.9 copy-start.4
  157.2 19.9 %collective-permute-start.7 = (bf16[3072,128]{1,0:T(8,128)(2,1)}, bf16[3072,128]{1,0:T(8,128)(2,1)S(1)}, u32[]{:S(2)}, u32[]{:S(2)}) collective-permute-start(bf16[3072,128]{1,0:T(8,128)(2,1)} %hand_on.6.refs_2_), channel_id=1, source_target_pairs={{0,7},{1,0},{2,1},{3,2},{4,3},{5,4},{6,5},{7,6},{8,15},{9,8},{10,9... | collective-permute-start | bytes 2359304 | tf_op jit(solution)/shard_map/ppermute | solution.py:743
  163.6 0.9 copy-start.5
  164.5 21.9 %collective-permute-start.6 = (bf16[3072,128]{1,0:T(8,128)(2,1)}, bf16[3072,128]{1,0:T(8,128)(2,1)}, u32[]{:S(2)}, u32[]{:S(2)}) collective-permute-start(bf16[3072,128]{1,0:T(8,128)(2,1)} %hand_on.7.refs_3_), channel_id=1, source_target_pairs={{0,1},{1,2},{2,3},{3,4},{4,5},{5,6},{6,7},{7,0},{8,9},{9,10},{10,1... | collective-permute-start | bytes 2359304 | tf_op jit(solution)/shard_map/ppermute | solution.py:743
  168.1 29.1 %all-to-all-start.3 = ((bf16[32,32,128]{2,1,0:T(8,128)(2,1)}), bf16[32,32,128]{2,1,0:T(8,128)(2,1)S(1)}, u32[]{:S(2)}, u32[]{:S(2)}) async-start(bf16[32,32,128]{2,1,0:T(8,128)(2,1)} %get-tuple-element.23), calls=%async_computation.3 | async-start | bytes 524288 | tf_op jit(solution)/shard_map/all_to_all | solution.py:709
  177.1 0.9 copy-start.3
  178.0 23.6 %collective-permute-start.9 = (bf16[3072,128]{1,0:T(8,128)(2,1)}, bf16[3072,128]{1,0:T(8,128)(2,1)S(1)}, u32[]{:S(2)}, u32[]{:S(2)}) collective-permute-start(bf16[3072,128]{1,0:T(8,128)(2,1)} %hand_on.9.refs_5_), channel_id=1, source_target_pairs={{0,7},{1,0},{2,1},{3,2},{4,3},{5,4},{6,5},{7,6},{8,15},{9,8},{10,9... | collective-permute-start | bytes 2359304 | tf_op jit(solution)/shard_map/ppermute | solution.py:743
  186.4 43.5 %copy-start.6 = (f32[32,2]{0,1:T(2,128)S(1)}, f32[32,2]{0,1:T(2,128)}, u32[]{:S(2)}) copy-start(f32[32,2]{0,1:T(2,128)} %param.34) | copy-start | bytes 772
  186.4 21.1 %collective-permute-start.8 = (bf16[3072,128]{1,0:T(8,128)(2,1)}, bf16[3072,128]{1,0:T(8,128)(2,1)S(1)}, u32[]{:S(2)}, u32[]{:S(2)}) collective-permute-start(bf16[3072,128]{1,0:T(8,128)(2,1)} %hand_on.8.refs_4_), channel_id=1, source_target_pairs={{0,1},{1,2},{2,3},{3,4},{4,5},{5,6},{6,7},{7,0},{8,9},{9,10},{10,1... | collective-permute-start | bytes 2359304 | tf_op jit(solution)/shard_map/ppermute | solution.py:743
  197.2 10.5 %collective-permute-start.2 = (bf16[32,32,128]{2,1,0:T(8,128)(2,1)S(1)}, bf16[32,32,128]{2,1,0:T(8,128)(2,1)S(1)}, u32[]{:S(2)}, u32[]{:S(2)}) collective-permute-start(bf16[32,32,128]{2,1,0:T(8,128)(2,1)S(1)} %all-to-all-done.3.own_ref), channel_id=1, source_target_pairs={{0,256},{256,0},{1,257},{257,1},{2,258},{258,2},{3,259},{259,3},{4... | collective-permute-start | bytes 786440 | tf_op jit(solution)/shard_map/ppermute | solution.py:771
  211.1 8.7 %collective-permute-start.10 = (bf16[64,2048]{1,0:T(8,128)(2,1)S(1)}, bf16[64,2048]{1,0:T(8,128)(2,1)S(1)}, u32[]{:S(2)}, u32[]{:S(2)}) collective-permute-start(bf16[64,2048]{1,0:T(8,128)(2,1)S(1)} %get-tuple-element.25), channel_id=1, source_target_pairs={{0,256},{256,0},{1,257},{257,1},{2,258},{258,2},{3,259},{259,3},{4... | collective-permute-start | bytes 786440 | tf_op jit(solution)/shard_map/ppermute | solution.py:773
  220.6 31.4 %all-to-all-start.4 = ((bf16[32,32,128]{2,1,0:T(8,128)(2,1)}), bf16[32,32,128]{2,1,0:T(8,128)(2,1)S(1)}, u32[]{:S(2)}, u32[]{:S(2)}) async-start(bf16[32,32,128]{2,1,0:T(8,128)(2,1)} %finish.1), calls=%async_computation.4 | async-start | bytes 524288 | tf_op jit(solution)/shard_map/all_to_all | solution.py:709

commit v8 on v7

--- a/solution.py
+++ b/solution.py
@@ -94,7 +94,7 @@
 
 def retention_body(
     index_ref, qa_ref, ka_ref, va_ref, qb_ref, kb_ref, vb_ref, da_ref, db_ref, tab_ref, base_ref,
-    qa_out, qb_out, loc_out, pay_out, dec_out,
+    qa_out, ka_out, qb_out, kb_out, pay_out, dec_out,
 ):
     n, dk = qa_ref.shape
     dv = va_ref.shape[1]
@@ -108,15 +108,8 @@
     dec_out[6:8, :] = jnp.zeros((2, n), F32)
     dec = dec_out[...]
     cr = jnp.dot(dec, (row <= col).astype(F32), precision=HIGHEST, preferred_element_type=F32)
-    cc = mm_nt((col <= row).astype(F32), dec, HIGHEST)
     er = cr - dec
-    ec = mm_nt((col < row).astype(F32), dec, HIGHEST)
     tot = cr[:, n - 1 : n]
-
-    def pair_weights(h):
-        forward = cc[:, h : h + 1] - cr[h : h + 1, :]
-        backward = er[3 + h : 4 + h, :] - ec[:, 3 + h : 4 + h]
-        return jnp.exp(jnp.where(col <= row, forward, backward))
 
     base = base_ref[index_ref[0]]
     cos_a = tab_ref[0] * base[0:1] - tab_ref[1] * base[1:2]
@@ -130,6 +123,7 @@
     qa = rotate_a(qa_ref[...], 1.0)
     ka = rotate_a(ka_ref[...], 1.0 / math.sqrt(dk))
     qa_out[...] = qa
+    ka_out[...] = ka
 
     width = 2 * hb
     lane = iota((n, width), 1)
@@ -147,6 +141,7 @@
     qb = rotate_b(qb_ref[...], 1.0)
     kb = rotate_b(kb_ref[...], 1.0 / math.sqrt(hb))
     qb_out[...] = qb
+    kb_out[...] = kb
 
     va, vb = va_ref[...], vb_ref[...]
     kat = ka.astype(F32).T
@@ -171,8 +166,29 @@
             hi, lo = split2(tot[3 * d + h : 3 * d + h + 1])
             logs = jnp.where(rows == 2 * h, hi, jnp.where(rows == 2 * h + 1, lo, logs))
         pay_out[d, dk + TILE : dk + 2 * TILE, :] = logs.astype(BF16)
-    weighted = (mm_nt(qa, ka) * pair_weights(0)).astype(BF16)
-    loc_out[:, :dv] = mm(weighted, va)
+
+
+def pairs_body(qa_ref, ka_ref, va_ref, qb_ref, kb_ref, vb_ref, dec_ref, loc_out):
+    n = qa_ref.shape[0]
+    dv = va_ref.shape[1]
+    width = qb_ref.shape[1]
+    hb = width // 2
+    row, col = iota((n, n), 0), iota((n, n), 1)
+    dec = dec_ref[...]
+    cr = jnp.dot(dec, (row <= col).astype(F32), precision=HIGHEST, preferred_element_type=F32)
+    cc = mm_nt((col <= row).astype(F32), dec, HIGHEST)
+    er = cr - dec
+    ec = mm_nt((col < row).astype(F32), dec, HIGHEST)
+
+    def pair_weights(h):
+        forward = cc[:, h : h + 1] - cr[h : h + 1, :]
+        backward = er[3 + h : 4 + h, :] - ec[:, 3 + h : 4 + h]
+        return jnp.exp(jnp.where(col <= row, forward, backward))
+
+    weighted = (mm_nt(qa_ref[...], ka_ref[...]) * pair_weights(0)).astype(BF16)
+    loc_out[:, :dv] = mm(weighted, va_ref[...])
+    qb, kb, vb = qb_ref[...], kb_ref[...], vb_ref[...]
+    lane = iota((n, width), 1)
     acc = jnp.zeros((n, width), F32)
     for h in range(2):
         mine = (lane < hb) if h == 0 else (lane >= hb)
@@ -182,23 +198,36 @@
     loc_out[:, dv:] = acc
 
 
-def retention_local(index, qa, ka, va, qb, kb, vb, da, db, tab, base):
+def retention_pairs(qa, ka, va, qb, kb, vb, dec):
+    return pl.pallas_call(
+        pairs_body,
+        out_shape=near_shape((qa.shape[0], va.shape[1] + vb.shape[1]), F32),
+        in_specs=vmem(7),
+        out_specs=vmem(1)[0],
+        interpret=INTERPRET,
+        compiler_params=PARAMS,
+        name="retention_pairs",
+    )(near(qa), near(ka), far(va), near(qb), near(kb), far(vb), near(dec))
+
+
+def retention_state(index, qa, ka, va, qb, kb, vb, da, db, tab, base):
     n, dk = qa.shape
     dv, wb = va.shape[1], vb.shape[1]
     return pl.pallas_call(
         retention_body,
         out_shape=(
             near_shape((n, dk), BF16),
+            near_shape((n, dk), BF16),
             near_shape((n, wb), BF16),
-            near_shape((n, dv + wb), F32),
+            near_shape((n, wb), BF16),
             near_shape((2, dk + 2 * TILE, dv), BF16),
             near_shape((8, n), F32),
         ),
         in_specs=[SMEM_SPEC] + vmem(10),
-        out_specs=tuple(vmem(5)),
-        interpret=INTERPRET,
-        compiler_params=PARAMS,
-        name="retention_local",
+        out_specs=tuple(vmem(6)),
+        interpret=INTERPRET,
+        compiler_params=PARAMS,
+        name="retention_state",
     )(index, *map(far, (qa, ka, va, qb, kb, vb, da, db, tab, base)))
 
 
@@ -469,20 +498,38 @@
     ).astype(BF16)
 
 
-def dispatch_body(arr_ref, res_ref, gain_ref, ids_ref, hid_ref, out_ref, scr):
+def route_body(ids_ref, w_ref, choose_ref, weights_ref):
+    hot = slots_by_route(ids_ref[...])
+    belongs = route_rows(weights_ref.shape[0], hot.shape[1])
+    choose = mm_nt(hot.astype(BF16), jnp.where(belongs, 1.0, 0.0).astype(BF16))
+    choose_ref[...] = choose.astype(BF16)
+    weights_ref[...] = mm_nt(jnp.where(belongs, w_ref[...], 0.0), hot, HIGHEST)
+
+
+def route(ids, weights, rows):
+    routes = ids.shape[1]
+    return pl.pallas_call(
+        route_body,
+        out_shape=(near_shape((routes, rows), BF16), near_shape((rows, routes), F32)),
+        in_specs=vmem(2),
+        out_specs=tuple(vmem(2)),
+        interpret=INTERPRET,
+        compiler_params=PARAMS,
+        name="route",
+    )(ids, weights)
+
+
+def dispatch_body(arr_ref, res_ref, gain_ref, choose_ref, hid_ref, out_ref, scr):
     mix = jnp.sum(arr_ref[...].astype(F32), axis=0)
     stream = RESIDUAL_SCALE * res_ref[...].astype(F32) + mix
     hidden = layer_norm(stream, gain_ref[0:1, :]).astype(BF16)
     hid_ref[...] = hidden
-    hot = slots_by_route(ids_ref[...])
-    belongs = jnp.where(route_rows(hidden.shape[0], hot.shape[1]), 1.0, 0.0)
-    choose = mm_nt(hot.astype(BF16), belongs.astype(BF16)).astype(BF16)
-    store_chunks(mm(choose, hidden), out_ref, scr)
-
-
-def dispatch(arrived, residual, gain, ids, peers):
+    store_chunks(mm(choose_ref[...], hidden), out_ref, scr)
+
+
+def dispatch(arrived, residual, gain, choose, peers):
     rows, width = residual.shape
-    lines = ids.shape[1] * width // LANES
+    lines = choose.shape[0] * width // LANES
     return pl.pallas_call(
         dispatch_body,
         out_shape=(
@@ -495,7 +542,7 @@
         interpret=INTERPRET,
         compiler_params=PARAMS,
         name="dispatch",
-    )(near(arrived), residual, gain, ids)
+    )(near(arrived), residual, gain, near(choose))
 
 
 def hand_on(*arrays):
@@ -676,12 +723,10 @@
     )(near(mine), near(arrived))
 
 
-def combine_body(ret_ref, hid_ref, gain_ref, ids_ref, w_ref, out_ref, scr):
+def combine_body(ret_ref, hid_ref, gain_ref, w_ref, out_ref, scr):
     hidden = hid_ref[...]
-    hot = slots_by_route(ids_ref[...])
-    factor = jnp.where(route_rows(hidden.shape[0], hot.shape[1]), w_ref[...], 0.0)
-    weights = mm_nt(factor, hot, HIGHEST)
-    returned = load_chunks(ret_ref, hot.shape[0], scr)
+    weights = w_ref[...]
+    returned = load_chunks(ret_ref, weights.shape[1], scr)
     hi = weights.astype(BF16)
     rest = weights - hi.astype(F32)
     mid = rest.astype(BF16)
@@ -691,18 +736,18 @@
     out_ref[...] = layer_norm(stream, gain_ref[1:2, :]).astype(BF16)
 
 
-def combine(returned, hidden, gain, ids, weights):
+def combine(returned, hidden, gain, weights):
     lines = returned.shape[0] * returned.shape[1]
     return pl.pallas_call(
         combine_body,
         out_shape=jax.ShapeDtypeStruct(hidden.shape, BF16),
-        in_specs=vmem(5),
+        in_specs=vmem(4),
         out_specs=vmem(1)[0],
         scratch_shapes=[pltpu.VMEM((lines, LANES), F32)],
         interpret=INTERPRET,
         compiler_params=PARAMS,
         name="combine",
-    )(near(returned), near(hidden), gain, ids, weights)
+    )(near(returned), near(hidden), gain, near(weights))
 
 
 def exchange(array, axis):
@@ -730,7 +775,7 @@
         length, query_a.shape[1] // 2, query_b.shape[1] // 4, sp_count
     )
     index = lax.axis_index(SP).astype(jnp.int32).reshape(1)
-    qa, qb, loc, pay, dec = retention_local(
+    qa, ka, qb, kb, pay, dec = retention_state(
         index, query_a, key_a, value_a, query_b, key_b, value_b, decay_a, decay_b,
         jnp.asarray(local), jnp.asarray(base),
     )
@@ -752,6 +797,7 @@
     pieces = exchange(outgoing_states, "sp_0")
     below = start(packed, down_ring)
     above = start(arrive(above), up_ring)
+    loc = retention_pairs(qa, ka, value_a, qb, kb, value_b, dec)
     per = value_a.shape[1] // LANES * TILE // chips
     scanned = scan_states(core, pieces, per)
     carried = exchange(scanned, "sp_0")
@@ -764,7 +810,8 @@
     )
     arrived = exchange(partial.reshape(tp, rows_dev, width), "tp")
     ids = (route_group[:, None] * EXP_GROUP + route_expert).reshape(1, routes)
-    hidden, outgoing = dispatch(arrived, residual, norm_gain, ids, sp_count)
+    choose, weights = route(ids, route_weight.reshape(1, routes), rows_dev)
+    hidden, outgoing = dispatch(arrived, residual, norm_gain, choose, sp_count)
     received = exchange(outgoing, SP)
     above = start(arrive(above), up_ring)
     below = start(arrive(below), down_ring)
@@ -773,7 +820,7 @@
     arrived_sums = lax.ppermute(send, "grp", partner)
     back = finish(mine, arrived_sums, sp_count)
     returned = exchange(back, SP)
-    return combine(returned, hidden, norm_gain, ids, route_weight.reshape(1, routes))
+    return combine(returned, hidden, norm_gain, weights)
 
 
 def solution(mesh):

time: 254 us -> 254 us (level)
  blocking collectives: 42.7 us -> 74.5 us
  waiting for transfers between devices: 85.6 us -> 61.5 us
  starting transfers between devices: 105 us -> 94.8 us
    all_to_all x2 -> x3, blocking collectives: 42.7 us -> 74.5 us  [exchange(): return lax.all_to_all(array, axis, split_axis=0, concat_axis=0, tiled=True)]
    all_to_all x3 -> x2, waiting for transfers between devices: 30.6 us -> 9.99 us  [exchange(): return lax.all_to_all(array, axis, split_axis=0, concat_axis=0, tiled=True)]
    all_to_all x3 -> x2, starting transfers between devices: 22.4 us -> 13.7 us  [exchange(): return lax.all_to_all(array, axis, split_axis=0, concat_axis=0, tiled=True)]
    ppermute x7, waiting for transfers between devices: 49 us -> 43.3 us  [start(): return lax.ppermute(array, 'tp', ring)]
  transfers between devices with their start and end apart: 14 -> 13, of which waited for: 11 -> 10; matrix products, arithmetic and copies ran while one was open for 0% -> 0% of each run, Pallas kernels for 3% -> 4%
where the time goes in v8:
time: 254 us; the launch traced here: 253 us
  starting transfers between devices  94.8 us (37%)
  blocking collectives  74.5 us (29%)
  waiting for transfers between devices  61.5 us (24%)
  Pallas kernels  17.9 us (7%)
  local copies, waits for them, and re-layouts  3.97 us (2%)
    all_to_all x3, blocking collectives, exchange(): return lax.all_to_all(array, axis, split_axis=0, concat_axis=0, tiled=True)  74.5 us
    ppermute x1, starting transfers between devices, shards(): pay_other = lax.ppermute(pay, 'sp_1', swap)  43.4 us
    ppermute x7, waiting for transfers between devices, start(): return lax.ppermute(array, 'tp', ring)  43.3 us
    ppermute x7, starting transfers between devices, start(): return lax.ppermute(array, 'tp', ring)  22.1 us
    all_to_all x2, starting transfers between devices, exchange(): return lax.all_to_all(array, axis, split_axis=0, concat_axis=0, tiled=True)  13.7 us
    all_to_all x2, waiting for transfers between devices, exchange(): return lax.all_to_all(array, axis, split_axis=0, concat_axis=0, tiled=True)  9.99 us
    ppermute x1, starting transfers between devices, shards(): carried_other = lax.ppermute(carried, 'sp_1', swap)  8.1 us
  transfers between devices with their start and end apart: 13, of which 10 were waited for; matrix products, arithmetic and copies ran while one was open for 0% of the time, Pallas kernels for 4%

profile of v8, /device:TPU:65, one launch (start us, length us, event | category | flops | bytes accessed | tf_op | source)
XLA Modules:
  0.0 252.9 jit_solution(985512231443456394)
XLA Ops:
  0.0 2.2 retention_state.1
  2.2 43.4 %collective-permute-start = (bf16[2,288,512]{2,1,0:T(8,128)(2,1)S(1)}, bf16[2,288,512]{2,1,0:T(8,128)(2,1)S(1)}, u32[]{:S(2)}, u32[]{:S(2)}) collective-permute-start(bf16[2,288,512]{2,1,0:T(8,128)(2,1)S(1)} %get-tuple-element.24.own_ref), channel_id=1, source_target_pairs={{0,8},{8,0},{1,9},{9,1},{2,10},{10,2},{3,11},{11,3},{4,12},{12,4},... | collective-permute-start | bytes 1769480 | tf_op jit(solution)/shard_map/ppermute | solution.py:783
  45.6 1.6 collective-permute-done.oth_ref.pay_ref
  47.2 0.2 pack_states.1
  47.4 17.3 %all_to_all.25.refs_1_ = bf16[16,72,128]{2,1,0:T(8,128)(2,1)S(1)} all-to-all(bf16[16,72,128]{2,1,0:T(8,128)(2,1)S(1)} %pack_states.1), channel_id=1, replica_groups=mesh['grp'=2,'sp_0'=16,'sp_1'=2,'tp'=8] {'sp_0'}, dimensions={0} | all-to-all | bytes 589824 | tf_op jit(solution)/shard_map/all_to_all | solution.py:754
  64.7 0.2 scan_states.1
  65.0 25.4 %all_to_all.26.own_ref = bf16[16,72,128]{2,1,0:T(8,128)(2,1)S(1)} all-to-all(bf16[16,72,128]{2,1,0:T(8,128)(2,1)S(1)} %scan_states.1), channel_id=1, replica_groups=mesh['grp'=2,'sp_0'=16,'sp_1'=2,'tp'=8] {'sp_0'}, dimensions={0} | all-to-all | bytes 589824 | tf_op jit(solution)/shard_map/all_to_all | solution.py:754
  90.3 8.1 %collective-permute-start.1 = (bf16[16,72,128]{2,1,0:T(8,128)(2,1)S(1)}, bf16[16,72,128]{2,1,0:T(8,128)(2,1)S(1)}, u32[]{:S(2)}, u32[]{:S(2)}) collective-permute-start(bf16[16,72,128]{2,1,0:T(8,128)(2,1)S(1)} %all_to_all.26.own_ref), channel_id=1, source_target_pairs={{0,8},{8,0},{1,9},{9,1},{2,10},{10,2},{3,11},{11,3},{4,12},{12,4},... | collective-permute-start | bytes 884744 | tf_op jit(solution)/shard_map/ppermute | solution.py:807
  98.4 1.9 pack_weights.1.refs_0_
  100.3 3.3 %collective-permute-start.3 = (bf16[3072,128]{1,0:T(8,128)(2,1)S(1)}, bf16[3072,128]{1,0:T(8,128)(2,1)S(1)}, u32[]{:S(2)}, u32[]{:S(2)}) collective-permute-start(bf16[3072,128]{1,0:T(8,128)(2,1)S(1)} %pack_weights.1.refs_0_), channel_id=1, source_target_pairs={{0,1},{1,2},{2,3},{3,4},{4,5},{5,6},{6,7},{7,0},{8,9},{9,10},{10,1... | collective-permute-start | bytes 2359304 | tf_op jit(solution)/shard_map/ppermute | solution.py:788
  103.6 1.7 fetch.1
  105.3 2.2 retention_pairs.1.loc_ref
  107.5 3.1 %mix_project.1 = bf16[256,2048]{1,0:T(8,128)(2,1)} custom-call(s32[1]{0:T(128)} %bitcast.core_ref.refs_0_, bf16[256,256]{1,0:T(8,128)(2,1)S(1)} %get-tuple-element.19.qa_ref, bf16[256,128]{1,0:T(8,128)(2,1)S(1)} %get-tuple-element.20.qb_ref, f32[256,640]{1,0:T(8,128)S(1)} %retention_pairs.1.loc_ref, bf16[16,72,128]{2,1,0:T(8,128)(2,1)S(1)} %all_to_all.26.own_ref, ...), custom_call_target="tpu_custom_call" | custom-call | tf_op jit(solution)/shard_map/mix_project/pallas_call | solution.py:452
  110.6 6.1 %all-to-all-start.2 = ((bf16[8,32,2048]{2,1,0:T(8,128)(2,1)}), bf16[8,32,2048]{2,1,0:T(8,128)(2,1)S(1)}, u32[]{:S(2)}, u32[]{:S(2)}) async-start(bf16[8,32,2048]{2,1,0:T(8,128)(2,1)} %bitcast.2), calls=%async_computation.2 | async-start | bytes 2097152 | tf_op jit(solution)/shard_map/all_to_all | solution.py:754
  116.8 0.0 copy-start.7
  116.8 4.7 %collective-permute-start.4 = (bf16[3072,128]{1,0:T(8,128)(2,1)S(1)}, bf16[3072,128]{1,0:T(8,128)(2,1)S(1)}, u32[]{:S(2)}, u32[]{:S(2)}) collective-permute-start(bf16[3072,128]{1,0:T(8,128)(2,1)S(1)} %pack_weights.1.refs_0_), channel_id=1, source_target_pairs={{0,7},{1,0},{2,1},{3,2},{4,3},{5,4},{6,5},{7,6},{8,15},{9,8},{10,9... | collective-permute-start | bytes 2359304 | tf_op jit(solution)/shard_map/ppermute | solution.py:788
  121.6 2.1 collective-permute-done.3.refs_0_
  123.7 0.9 copy-done.4
  124.6 1.9 collective-permute-start.5
  126.5 31.5 %collective-permute-done.4.refs_0_ = bf16[3072,128]{1,0:T(8,128)(2,1)S(1)} collective-permute-done((bf16[3072,128]{1,0:T(8,128)(2,1)S(1)}, bf16[3072,128]{1,0:T(8,128)(2,1)S(1)}, u32[]{:S(2)}, u32[]{:S(2)}) %collective-permute-start.4) | collective-permute-done | bytes 786464 | tf_op jit(solution)/shard_map/ppermute | solution.py:788
  158.0 0.9 copy-done.5
  158.8 3.4 %collective-permute-start.7 = (bf16[3072,128]{1,0:T(8,128)(2,1)}, bf16[3072,128]{1,0:T(8,128)(2,1)S(1)}, u32[]{:S(2)}, u32[]{:S(2)}) collective-permute-start(bf16[3072,128]{1,0:T(8,128)(2,1)} %hand_on.6.refs_2_), channel_id=1, source_target_pairs={{0,7},{1,0},{2,1},{3,2},{4,3},{5,4},{6,5},{7,6},{8,15},{9,8},{10,9... | collective-permute-start | bytes 2359304 | tf_op jit(solution)/shard_map/ppermute | solution.py:788
  162.3 0.7 collective-permute-done.5.refs_0_
  163.0 0.9 copy-done.6
  163.9 1.9 collective-permute-start.6
  165.9 0.1 copy.28
  166.0 0.1 reshape.23.ids_ref
  166.1 0.1 copy.29
  166.2 0.1 reshape.24.w_ref
  166.3 0.3 route.1
  166.5 0.0 copy-done.1
  166.6 1.4 dispatch.1
  167.9 7.6 %all-to-all-start.3 = ((bf16[32,32,128]{2,1,0:T(8,128)(2,1)}), bf16[32,32,128]{2,1,0:T(8,128)(2,1)S(1)}, u32[]{:S(2)}, u32[]{:S(2)}) async-start(bf16[32,32,128]{2,1,0:T(8,128)(2,1)} %get-tuple-element.28), calls=%async_computation.3 | async-start | bytes 524288 | tf_op jit(solution)/shard_map/all_to_all | solution.py:754
  175.6 3.2 %collective-permute-done.7.refs_0_ = bf16[3072,128]{1,0:T(8,128)(2,1)S(1)} collective-permute-done((bf16[3072,128]{1,0:T(8,128)(2,1)}, bf16[3072,128]{1,0:T(8,128)(2,1)S(1)}, u32[]{:S(2)}, u32[]{:S(2)}) %collective-permute-start.7) | collective-permute-done | bytes 786464 | tf_op jit(solution)/shard_map/ppermute | solution.py:788
  178.8 0.9 copy-done.3
  179.6 4.8 %collective-permute-start.9 = (bf16[3072,128]{1,0:T(8,128)(2,1)}, bf16[3072,128]{1,0:T(8,128)(2,1)S(1)}, u32[]{:S(2)}, u32[]{:S(2)}) collective-permute-start(bf16[3072,128]{1,0:T(8,128)(2,1)} %hand_on.9.refs_5_), channel_id=1, source_target_pairs={{0,7},{1,0},{2,1},{3,2},{4,3},{5,4},{6,5},{7,6},{8,15},{9,8},{10,9... | collective-permute-start | bytes 2359304 | tf_op jit(solution)/shard_map/ppermute | solution.py:788
  184.5 1.3 collective-permute-done.6.refs_0_
  185.7 1.9 collective-permute-start.8
  187.7 10.0 %all-to-all-done.3.own_ref = bf16[32,32,128]{2,1,0:T(8,128)(2,1)S(1)} async-done(((bf16[32,32,128]{2,1,0:T(8,128)(2,1)}), bf16[32,32,128]{2,1,0:T(8,128)(2,1)S(1)}, u32[]{:S(2)}, u32[]{:S(2)}) %all-to-all-start.3) | async-done | bytes 262176 | tf_op jit(solution)/shard_map/all_to_all | solution.py:754
  197.7 4.4 %collective-permute-start.2 = (bf16[32,32,128]{2,1,0:T(8,128)(2,1)S(1)}, bf16[32,32,128]{2,1,0:T(8,128)(2,1)S(1)}, u32[]{:S(2)}, u32[]{:S(2)}) collective-permute-start(bf16[32,32,128]{2,1,0:T(8,128)(2,1)S(1)} %all-to-all-done.3.own_ref), channel_id=1, source_target_pairs={{0,256},{256,0},{1,257},{257,1},{2,258},{258,2},{3,259},{259,3},{4... | collective-permute-start | bytes 786440 | tf_op jit(solution)/shard_map/ppermute | solution.py:818
  202.1 4.5 %collective-permute-done.8.refs_6_ = bf16[3072,128]{1,0:T(8,128)(2,1)S(1)} collective-permute-done((bf16[3072,128]{1,0:T(8,128)(2,1)}, bf16[3072,128]{1,0:T(8,128)(2,1)S(1)}, u32[]{:S(2)}, u32[]{:S(2)}) %collective-permute-start.8) | collective-permute-done | bytes 786464 | tf_op jit(solution)/shard_map/ppermute | solution.py:788
  206.6 1.6 collective-permute-done.2.oth_ref
  208.2 3.4 %experts.1 = (f32[64,2048]{1,0:T(8,128)S(1)}, bf16[64,2048]{1,0:T(8,128)(2,1)S(1)}) custom-call(bf16[32,32,128]{2,1,0:T(8,128)(2,1)S(1)} %all-to-all-done.3.own_ref, bf16[32,32,128]{2,1,0:T(8,128)(2,1)S(1)} %collective-permute-done.2.oth_ref, bf16[3072,128]{1,0:T(8,128)(2,1)} %copy-done, bf16[3072,128]{1,0:T(8,128)(2,1)} %hand_on.5.refs_1_, ...), custom_call_target="tpu_custom_call" | custom-call | tf_op jit(solution)/shard_map/experts/pallas_call | solution.py:687
  211.6 3.1 %collective-permute-start.10 = (bf16[64,2048]{1,0:T(8,128)(2,1)S(1)}, bf16[64,2048]{1,0:T(8,128)(2,1)S(1)}, u32[]{:S(2)}, u32[]{:S(2)}) collective-permute-start(bf16[64,2048]{1,0:T(8,128)(2,1)S(1)} %get-tuple-element.30), channel_id=1, source_target_pairs={{0,256},{256,0},{1,257},{257,1},{2,258},{258,2},{3,259},{259,3},{4... | collective-permute-start | bytes 786440 | tf_op jit(solution)/shard_map/ppermute | solution.py:820
  214.7 5.0 %collective-permute-done.10.arrived_ref = bf16[64,2048]{1,0:T(8,128)(2,1)S(1)} collective-permute-done((bf16[64,2048]{1,0:T(8,128)(2,1)S(1)}, bf16[64,2048]{1,0:T(8,128)(2,1)S(1)}, u32[]{:S(2)}, u32[]{:S(2)}) %collective-permute-start.10) | collective-permute-done | bytes 262176 | tf_op jit(solution)/shard_map/ppermute | solution.py:820
  219.7 0.2 finish.1
  219.9 31.8 %all_to_all.27.ret_ref = bf16[32,32,128]{2,1,0:T(8,128)(2,1)S(1)} all-to-all(bf16[32,32,128]{2,1,0:T(8,128)(2,1)S(1)} %finish.1), channel_id=1, replica_groups=mesh['grp'=2,'sp_0'=16,'sp_1'=2,'tp'=8] {'sp_0','sp_1'}, dimensions={0} | all-to-all | bytes 524288 | tf_op jit(solution)/shard_map/all_to_all | solution.py:754
  251.7 1.3 combine.1
  (24 shorter events, 0.1 us)
Async XLA Ops:
  2.2 45.0 %collective-permute-start = (bf16[2,288,512]{2,1,0:T(8,128)(2,1)S(1)}, bf16[2,288,512]{2,1,0:T(8,128)(2,1)S(1)}, u32[]{:S(2)}, u32[]{:S(2)}) collective-permute-start(bf16[2,288,512]{2,1,0:T(8,128)(2,1)S(1)} %get-tuple-element.24.own_ref), channel_id=1, source_target_pairs={{0,8},{8,0},{1,9},{9,1},{2,10},{10,2},{3,11},{11,3},{4,12},{12,4},... | collective-permute-start | bytes 1769480 | tf_op jit(solution)/shard_map/ppermute | solution.py:783
  90.3 17.2 %collective-permute-start.1 = (bf16[16,72,128]{2,1,0:T(8,128)(2,1)S(1)}, bf16[16,72,128]{2,1,0:T(8,128)(2,1)S(1)}, u32[]{:S(2)}, u32[]{:S(2)}) collective-permute-start(bf16[16,72,128]{2,1,0:T(8,128)(2,1)S(1)} %all_to_all.26.own_ref), channel_id=1, source_target_pairs={{0,8},{8,0},{1,9},{9,1},{2,10},{10,2},{3,11},{11,3},{4,12},{12,4},... | collective-permute-start | bytes 884744 | tf_op jit(solution)/shard_map/ppermute | solution.py:807
  100.3 16.5 %copy-start = (bf16[3072,128]{1,0:T(8,128)(2,1)}, bf16[3072,128]{1,0:T(8,128)(2,1)S(1)}, u32[]{:S(2)}) copy-start(bf16[3072,128]{1,0:T(8,128)(2,1)S(1)} %pack_weights.1.refs_0_) | copy-start | bytes 2359300
  100.3 23.4 %collective-permute-start.3 = (bf16[3072,128]{1,0:T(8,128)(2,1)S(1)}, bf16[3072,128]{1,0:T(8,128)(2,1)S(1)}, u32[]{:S(2)}, u32[]{:S(2)}) collective-permute-start(bf16[3072,128]{1,0:T(8,128)(2,1)S(1)} %pack_weights.1.refs_0_), channel_id=1, source_target_pairs={{0,1},{1,2},{2,3},{3,4},{4,5},{5,6},{6,7},{7,0},{8,9},{9,10},{10,1... | collective-permute-start | bytes 2359304 | tf_op jit(solution)/shard_map/ppermute | solution.py:788
  110.6 55.9 %all-to-all-start.2 = ((bf16[8,32,2048]{2,1,0:T(8,128)(2,1)}), bf16[8,32,2048]{2,1,0:T(8,128)(2,1)S(1)}, u32[]{:S(2)}, u32[]{:S(2)}) async-start(bf16[8,32,2048]{2,1,0:T(8,128)(2,1)} %bitcast.2), calls=%async_computation.2 | async-start | bytes 2097152 | tf_op jit(solution)/shard_map/all_to_all | solution.py:754
  116.8 49.1 %copy-start.9 = (s32[32]{0:T(128)S(1)}, s32[32]{0:T(128)}, u32[]{:S(2)}) copy-start(s32[32]{0:T(128)} %param.32) | copy-start | bytes 388
  116.8 49.1 %copy-start.8 = (s32[32,2]{0,1:T(2,128)S(1)}, s32[32,2]{0,1:T(2,128)}, u32[]{:S(2)}) copy-start(s32[32,2]{0,1:T(2,128)} %param.33) | copy-start | bytes 772
  116.8 49.3 %copy-start.7 = (f32[32,2]{0,1:T(2,128)S(1)}, f32[32,2]{0,1:T(2,128)}, u32[]{:S(2)}) copy-start(f32[32,2]{0,1:T(2,128)} %param.34) | copy-start | bytes 772
  116.8 49.8 %copy-start.1 = (bf16[32,2048]{1,0:T(8,128)(2,1)S(1)}, bf16[32,2048]{1,0:T(8,128)(2,1)}, u32[]{:S(2)}) copy-start(bf16[32,2048]{1,0:T(8,128)(2,1)} %res_ref.1) | copy-start | bytes 393220
  116.8 49.8 %copy-start.2 = (f32[2,2048]{1,0:T(2,128)S(1)}, f32[2,2048]{1,0:T(2,128)}, u32[]{:S(2)}) copy-start(f32[2,2048]{1,0:T(2,128)} %gain_ref.3) | copy-start | bytes 49156
  116.8 41.1 %collective-permute-start.4 = (bf16[3072,128]{1,0:T(8,128)(2,1)S(1)}, bf16[3072,128]{1,0:T(8,128)(2,1)S(1)}, u32[]{:S(2)}, u32[]{:S(2)}) collective-permute-start(bf16[3072,128]{1,0:T(8,128)(2,1)S(1)} %pack_weights.1.refs_0_), channel_id=1, source_target_pairs={{0,7},{1,0},{2,1},{3,2},{4,3},{5,4},{6,5},{7,6},{8,15},{9,8},{10,9... | collective-permute-start | bytes 2359304 | tf_op jit(solution)/shard_map/ppermute | solution.py:788
  123.7 0.9 copy-start.4
  124.6 38.4 %collective-permute-start.5 = (bf16[3072,128]{1,0:T(8,128)(2,1)}, bf16[3072,128]{1,0:T(8,128)(2,1)S(1)}, u32[]{:S(2)}, u32[]{:S(2)}) collective-permute-start(bf16[3072,128]{1,0:T(8,128)(2,1)} %hand_on.5.refs_1_), channel_id=1, source_target_pairs={{0,1},{1,2},{2,3},{3,4},{4,5},{5,6},{6,7},{7,0},{8,9},{9,10},{10,1... | collective-permute-start | bytes 2359304 | tf_op jit(solution)/shard_map/ppermute | solution.py:788
  158.0 0.9 copy-start.5
  158.8 19.9 %collective-permute-start.7 = (bf16[3072,128]{1,0:T(8,128)(2,1)}, bf16[3072,128]{1,0:T(8,128)(2,1)S(1)}, u32[]{:S(2)}, u32[]{:S(2)}) collective-permute-start(bf16[3072,128]{1,0:T(8,128)(2,1)} %hand_on.6.refs_2_), channel_id=1, source_target_pairs={{0,7},{1,0},{2,1},{3,2},{4,3},{5,4},{6,5},{7,6},{8,15},{9,8},{10,9... | collective-permute-start | bytes 2359304 | tf_op jit(solution)/shard_map/ppermute | solution.py:788
  163.0 0.9 copy-start.6
  163.9 21.8 %collective-permute-start.6 = (bf16[3072,128]{1,0:T(8,128)(2,1)}, bf16[3072,128]{1,0:T(8,128)(2,1)}, u32[]{:S(2)}, u32[]{:S(2)}) collective-permute-start(bf16[3072,128]{1,0:T(8,128)(2,1)} %hand_on.7.refs_3_), channel_id=1, source_target_pairs={{0,1},{1,2},{2,3},{3,4},{4,5},{5,6},{6,7},{7,0},{8,9},{9,10},{10,1... | collective-permute-start | bytes 2359304 | tf_op jit(solution)/shard_map/ppermute | solution.py:788
  167.9 29.7 %all-to-all-start.3 = ((bf16[32,32,128]{2,1,0:T(8,128)(2,1)}), bf16[32,32,128]{2,1,0:T(8,128)(2,1)S(1)}, u32[]{:S(2)}, u32[]{:S(2)}) async-start(bf16[32,32,128]{2,1,0:T(8,128)(2,1)} %get-tuple-element.28), calls=%async_computation.3 | async-start | bytes 524288 | tf_op jit(solution)/shard_map/all_to_all | solution.py:754
  178.8 0.9 copy-start.3
  179.6 22.5 %collective-permute-start.9 = (bf16[3072,128]{1,0:T(8,128)(2,1)}, bf16[3072,128]{1,0:T(8,128)(2,1)S(1)}, u32[]{:S(2)}, u32[]{:S(2)}) collective-permute-start(bf16[3072,128]{1,0:T(8,128)(2,1)} %hand_on.9.refs_5_), channel_id=1, source_target_pairs={{0,7},{1,0},{2,1},{3,2},{4,3},{5,4},{6,5},{7,6},{8,15},{9,8},{10,9... | collective-permute-start | bytes 2359304 | tf_op jit(solution)/shard_map/ppermute | solution.py:788
  185.7 20.9 %collective-permute-start.8 = (bf16[3072,128]{1,0:T(8,128)(2,1)}, bf16[3072,128]{1,0:T(8,128)(2,1)S(1)}, u32[]{:S(2)}, u32[]{:S(2)}) collective-permute-start(bf16[3072,128]{1,0:T(8,128)(2,1)} %hand_on.8.refs_4_), channel_id=1, source_target_pairs={{0,1},{1,2},{2,3},{3,4},{4,5},{5,6},{6,7},{7,0},{8,9},{9,10},{10,1... | collective-permute-start | bytes 2359304 | tf_op jit(solution)/shard_map/ppermute | solution.py:788
  197.7 10.5 %collective-permute-start.2 = (bf16[32,32,128]{2,1,0:T(8,128)(2,1)S(1)}, bf16[32,32,128]{2,1,0:T(8,128)(2,1)S(1)}, u32[]{:S(2)}, u32[]{:S(2)}) collective-permute-start(bf16[32,32,128]{2,1,0:T(8,128)(2,1)S(1)} %all-to-all-done.3.own_ref), channel_id=1, source_target_pairs={{0,256},{256,0},{1,257},{257,1},{2,258},{258,2},{3,259},{259,3},{4... | collective-permute-start | bytes 786440 | tf_op jit(solution)/shard_map/ppermute | solution.py:818
  211.6 8.2 %collective-permute-start.10 = (bf16[64,2048]{1,0:T(8,128)(2,1)S(1)}, bf16[64,2048]{1,0:T(8,128)(2,1)S(1)}, u32[]{:S(2)}, u32[]{:S(2)}) collective-permute-start(bf16[64,2048]{1,0:T(8,128)(2,1)S(1)} %get-tuple-element.30), channel_id=1, source_target_pairs={{0,256},{256,0},{1,257},{257,1},{2,258},{258,2},{3,259},{259,3},{4... | collective-permute-start | bytes 786440 | tf_op jit(solution)/shard_map/ppermute | solution.py:820

commit v9 on v8

--- a/solution.py
+++ b/solution.py
@@ -619,12 +619,11 @@
     )(part, far(gate), far(up), far(down))
 
 
-def expert_body(own_ref, oth_ref, *refs):
-    *held, mine_ref, send_ref, x_scr, blocks, acc_ref, sems = refs
+def expert_body(x_ref, *refs):
+    *held, out_ref, x_scr, blocks, acc_ref, sems = refs
     fetched, _, units = blocks.shape
     count = len(held)
-    rows = mine_ref.shape[0]
-    width = mine_ref.shape[1]
+    rows, width = out_ref.shape
     half = units // 2
     copies = [pltpu.make_async_copy(held[k], blocks.at[k], sems.at[k]) for k in range(fetched)]
     for copy in copies:
@@ -635,10 +634,8 @@
             return blocks[k, at : at + size, :]
         return held[k][at : at + size, :]
 
-    x = jnp.concatenate(
-        [load_chunks(own_ref, rows, x_scr), load_chunks(oth_ref, rows, x_scr)], axis=0
-    )
-    left = iota((2 * rows, units), 1) < half
+    x = load_chunks(x_ref, rows, x_scr)
+    left = iota((rows, units), 1) < half
 
     def silu(v):
         return v / (1.0 + jnp.exp(-v))
@@ -674,34 +671,29 @@
             elif first < count - group:
                 acc_ref[:, cut] += part
             else:
-                part = acc_ref[:, cut] + part
-                mine_ref[:, cut] = part[:rows]
-                send_ref[:, cut] = part[rows:].astype(BF16)
-
-
-def experts(own, other, blocks, late):
+                out_ref[:, cut] = (acc_ref[:, cut] + part).astype(out_ref.dtype)
+
+
+def experts(x, blocks, late, dtype):
     depth, units = blocks[0].shape
     width = depth * 2 // 3
-    lines = own.shape[0] * own.shape[1]
+    lines = x.shape[0] * x.shape[1]
     rows = lines * LANES // width
     return pl.pallas_call(
         expert_body,
-        out_shape=(
-            near_shape((rows, width), F32),
-            near_shape((rows, width), BF16),
-        ),
-        in_specs=vmem(2) + [ANY_SPEC] * len(blocks) + vmem(len(late)),
-        out_specs=tuple(vmem(2)),
+        out_shape=near_shape((rows, width), dtype),
+        in_specs=vmem(1) + [ANY_SPEC] * len(blocks) + vmem(len(late)),
+        out_specs=vmem(1)[0],
         scratch_shapes=[
             pltpu.VMEM((lines, LANES), F32),
             pltpu.VMEM((len(blocks), depth, units), BF16),
-            pltpu.VMEM((2 * rows, width), F32),
+            pltpu.VMEM((rows, width), F32),
             pltpu.SemaphoreType.DMA((len(blocks),)),
         ],
         interpret=INTERPRET,
         compiler_params=PARAMS,
         name="experts",
-    )(near(own), near(other), *map(far, blocks), *map(near, late))
+    )(near(x), *map(far, blocks), *map(near, late))
 
 
 def finish_body(mine_ref, arrived_ref, out_ref, scr):
@@ -816,8 +808,9 @@
     above = start(arrive(above), up_ring)
     below = start(arrive(below), down_ring)
     received_other = lax.ppermute(received, "grp", partner)
-    mine, send = experts(received, received_other, blocks, [above, below])
+    send = experts(received_other, blocks, [above, below], BF16)
     arrived_sums = lax.ppermute(send, "grp", partner)
+    mine = experts(received, blocks, [above, below], F32)
     back = finish(mine, arrived_sums, sp_count)
     returned = exchange(back, SP)
     return combine(returned, hidden, norm_gain, weights)

time: 254 us -> 254 us (level)
  Pallas kernels: 17.9 us -> 21.4 us
  waiting for transfers between devices: 61.5 us -> 58.1 us
    pallas_call x1 -> x2, Pallas kernels: 3.38 us -> 6.82 us  [experts(): pl.pallas_call(expert_body, out_shape=near_shape((rows, width), dtype), i...]
    ppermute x1, waiting for transfers between devices: 5.04 us -> 1.66 us  [shards(): arrived_sums = lax.ppermute(send, 'grp', partner)]
  transfers between devices with their start and end apart: 13 -> 13, of which waited for: 10 -> 10; matrix products, arithmetic and copies ran while one was open for 0% -> 0% of each run, Pallas kernels for 4% -> 6%
where the time goes in v9:
time: 254 us; the launch traced here: 253 us
  starting transfers between devices  94.8 us (37%)
  blocking collectives  74.4 us (29%)
  waiting for transfers between devices  58.1 us (23%)
  Pallas kernels  21.4 us (8%)
  local copies, waits for them, and re-layouts  3.99 us (2%)
    all_to_all x3, blocking collectives, exchange(): return lax.all_to_all(array, axis, split_axis=0, concat_axis=0, tiled=True)  74.4 us
    ppermute x1, starting transfers between devices, shards(): pay_other = lax.ppermute(pay, 'sp_1', swap)  43.4 us
    ppermute x7, waiting for transfers between devices, start(): return lax.ppermute(array, 'tp', ring)  43.1 us
    ppermute x7, starting transfers between devices, start(): return lax.ppermute(array, 'tp', ring)  22.1 us
    all_to_all x2, starting transfers between devices, exchange(): return lax.all_to_all(array, axis, split_axis=0, concat_axis=0, tiled=True)  13.8 us
    all_to_all x2, waiting for transfers between devices, exchange(): return lax.all_to_all(array, axis, split_axis=0, concat_axis=0, tiled=True)  10 us
    ppermute x1, starting transfers between devices, shards(): carried_other = lax.ppermute(carried, 'sp_1', swap)  8.1 us
    pallas_call x2, Pallas kernels, experts(): pl.pallas_call(expert_body, out_shape=near_shape((rows, width), dtype), i...  6.82 us
  transfers between devices with their start and end apart: 13, of which 10 were waited for; matrix products, arithmetic and copies ran while one was open for 0% of the time, Pallas kernels for 6%

profile of v9, /device:TPU:65, one launch (start us, length us, event | category | flops | bytes accessed | tf_op | source)
XLA Modules:
  0.0 253.0 jit_solution(15523373629762106660)
XLA Ops:
  0.0 2.2 retention_state.1
  2.2 43.4 %collective-permute-start = (bf16[2,288,512]{2,1,0:T(8,128)(2,1)S(1)}, bf16[2,288,512]{2,1,0:T(8,128)(2,1)S(1)}, u32[]{:S(2)}, u32[]{:S(2)}) collective-permute-start(bf16[2,288,512]{2,1,0:T(8,128)(2,1)S(1)} %get-tuple-element.22.own_ref), channel_id=1, source_target_pairs={{0,8},{8,0},{1,9},{9,1},{2,10},{10,2},{3,11},{11,3},{4,12},{12,4},... | collective-permute-start | bytes 1769480 | tf_op jit(solution)/shard_map/ppermute | solution.py:775
  45.6 1.6 collective-permute-done.oth_ref.pay_ref
  47.2 0.2 pack_states.1
  47.4 17.3 %all_to_all.25.refs_1_ = bf16[16,72,128]{2,1,0:T(8,128)(2,1)S(1)} all-to-all(bf16[16,72,128]{2,1,0:T(8,128)(2,1)S(1)} %pack_states.1), channel_id=1, replica_groups=mesh['grp'=2,'sp_0'=16,'sp_1'=2,'tp'=8] {'sp_0'}, dimensions={0} | all-to-all | bytes 589824 | tf_op jit(solution)/shard_map/all_to_all | solution.py:746
  64.7 0.2 scan_states.1
  65.0 25.4 %all_to_all.26.own_ref = bf16[16,72,128]{2,1,0:T(8,128)(2,1)S(1)} all-to-all(bf16[16,72,128]{2,1,0:T(8,128)(2,1)S(1)} %scan_states.1), channel_id=1, replica_groups=mesh['grp'=2,'sp_0'=16,'sp_1'=2,'tp'=8] {'sp_0'}, dimensions={0} | all-to-all | bytes 589824 | tf_op jit(solution)/shard_map/all_to_all | solution.py:746
  90.3 8.1 %collective-permute-start.1 = (bf16[16,72,128]{2,1,0:T(8,128)(2,1)S(1)}, bf16[16,72,128]{2,1,0:T(8,128)(2,1)S(1)}, u32[]{:S(2)}, u32[]{:S(2)}) collective-permute-start(bf16[16,72,128]{2,1,0:T(8,128)(2,1)S(1)} %all_to_all.26.own_ref), channel_id=1, source_target_pairs={{0,8},{8,0},{1,9},{9,1},{2,10},{10,2},{3,11},{11,3},{4,12},{12,4},... | collective-permute-start | bytes 884744 | tf_op jit(solution)/shard_map/ppermute | solution.py:799
  98.4 1.9 pack_weights.1.refs_0_
  100.3 3.3 %collective-permute-start.2 = (bf16[3072,128]{1,0:T(8,128)(2,1)S(1)}, bf16[3072,128]{1,0:T(8,128)(2,1)S(1)}, u32[]{:S(2)}, u32[]{:S(2)}) collective-permute-start(bf16[3072,128]{1,0:T(8,128)(2,1)S(1)} %pack_weights.1.refs_0_), channel_id=1, source_target_pairs={{0,1},{1,2},{2,3},{3,4},{4,5},{5,6},{6,7},{7,0},{8,9},{9,10},{10,1... | collective-permute-start | bytes 2359304 | tf_op jit(solution)/shard_map/ppermute | solution.py:780
  103.6 1.7 fetch.1
  105.3 2.2 retention_pairs.1.loc_ref
  107.5 3.1 %mix_project.1 = bf16[256,2048]{1,0:T(8,128)(2,1)} custom-call(s32[1]{0:T(128)} %bitcast.core_ref.refs_0_, bf16[256,256]{1,0:T(8,128)(2,1)S(1)} %get-tuple-element.17.qa_ref, bf16[256,128]{1,0:T(8,128)(2,1)S(1)} %get-tuple-element.18.qb_ref, f32[256,640]{1,0:T(8,128)S(1)} %retention_pairs.1.loc_ref, bf16[16,72,128]{2,1,0:T(8,128)(2,1)S(1)} %all_to_all.26.own_ref, ...), custom_call_target="tpu_custom_call" | custom-call | tf_op jit(solution)/shard_map/mix_project/pallas_call | solution.py:452
  110.6 6.1 %all-to-all-start.2 = ((bf16[8,32,2048]{2,1,0:T(8,128)(2,1)}), bf16[8,32,2048]{2,1,0:T(8,128)(2,1)S(1)}, u32[]{:S(2)}, u32[]{:S(2)}) async-start(bf16[8,32,2048]{2,1,0:T(8,128)(2,1)} %bitcast.2), calls=%async_computation.2 | async-start | bytes 2097152 | tf_op jit(solution)/shard_map/all_to_all | solution.py:746
  116.8 4.7 %collective-permute-start.3 = (bf16[3072,128]{1,0:T(8,128)(2,1)S(1)}, bf16[3072,128]{1,0:T(8,128)(2,1)S(1)}, u32[]{:S(2)}, u32[]{:S(2)}) collective-permute-start(bf16[3072,128]{1,0:T(8,128)(2,1)S(1)} %pack_weights.1.refs_0_), channel_id=1, source_target_pairs={{0,7},{1,0},{2,1},{3,2},{4,3},{5,4},{6,5},{7,6},{8,15},{9,8},{10,9... | collective-permute-start | bytes 2359304 | tf_op jit(solution)/shard_map/ppermute | solution.py:780
  121.6 2.1 collective-permute-done.2.refs_0_
  123.7 0.9 copy-done.4
  124.6 1.9 collective-permute-start.4
  126.5 31.5 %collective-permute-done.3.refs_0_ = bf16[3072,128]{1,0:T(8,128)(2,1)S(1)} collective-permute-done((bf16[3072,128]{1,0:T(8,128)(2,1)S(1)}, bf16[3072,128]{1,0:T(8,128)(2,1)S(1)}, u32[]{:S(2)}, u32[]{:S(2)}) %collective-permute-start.3) | collective-permute-done | bytes 786464 | tf_op jit(solution)/shard_map/ppermute | solution.py:780
  158.0 0.9 copy-done.5
  158.9 3.4 %collective-permute-start.6 = (bf16[3072,128]{1,0:T(8,128)(2,1)}, bf16[3072,128]{1,0:T(8,128)(2,1)S(1)}, u32[]{:S(2)}, u32[]{:S(2)}) collective-permute-start(bf16[3072,128]{1,0:T(8,128)(2,1)} %hand_on.6.refs_2_), channel_id=1, source_target_pairs={{0,7},{1,0},{2,1},{3,2},{4,3},{5,4},{6,5},{7,6},{8,15},{9,8},{10,9... | collective-permute-start | bytes 2359304 | tf_op jit(solution)/shard_map/ppermute | solution.py:780
  162.3 0.7 collective-permute-done.4.refs_0_
  163.0 0.9 copy-done.6
  163.9 1.9 collective-permute-start.5
  165.9 0.1 copy.28
  166.0 0.1 reshape.23.ids_ref
  166.1 0.1 copy.29
  166.2 0.1 reshape.24.w_ref
  166.3 0.3 route.1
  166.5 0.0 copy-done.1
  166.6 1.4 dispatch.1
  168.0 7.6 %all-to-all-start.3 = ((bf16[32,32,128]{2,1,0:T(8,128)(2,1)}), bf16[32,32,128]{2,1,0:T(8,128)(2,1)S(1)}, u32[]{:S(2)}, u32[]{:S(2)}) async-start(bf16[32,32,128]{2,1,0:T(8,128)(2,1)} %get-tuple-element.26), calls=%async_computation.3 | async-start | bytes 524288 | tf_op jit(solution)/shard_map/all_to_all | solution.py:746
  175.6 3.2 %collective-permute-done.6.refs_0_ = bf16[3072,128]{1,0:T(8,128)(2,1)S(1)} collective-permute-done((bf16[3072,128]{1,0:T(8,128)(2,1)}, bf16[3072,128]{1,0:T(8,128)(2,1)S(1)}, u32[]{:S(2)}, u32[]{:S(2)}) %collective-permute-start.6) | collective-permute-done | bytes 786464 | tf_op jit(solution)/shard_map/ppermute | solution.py:780
  178.8 0.9 copy-done.3
  179.7 4.8 %collective-permute-start.8 = (bf16[3072,128]{1,0:T(8,128)(2,1)}, bf16[3072,128]{1,0:T(8,128)(2,1)S(1)}, u32[]{:S(2)}, u32[]{:S(2)}) collective-permute-start(bf16[3072,128]{1,0:T(8,128)(2,1)} %hand_on.9.refs_5_), channel_id=1, source_target_pairs={{0,7},{1,0},{2,1},{3,2},{4,3},{5,4},{6,5},{7,6},{8,15},{9,8},{10,9... | collective-permute-start | bytes 2359304 | tf_op jit(solution)/shard_map/ppermute | solution.py:780
  184.5 1.2 collective-permute-done.5.refs_0_
  185.7 1.9 collective-permute-start.7
  187.7 10.0 %all-to-all-done.3.x_ref = bf16[32,32,128]{2,1,0:T(8,128)(2,1)S(1)} async-done(((bf16[32,32,128]{2,1,0:T(8,128)(2,1)}), bf16[32,32,128]{2,1,0:T(8,128)(2,1)S(1)}, u32[]{:S(2)}, u32[]{:S(2)}) %all-to-all-start.3) | async-done | bytes 262176 | tf_op jit(solution)/shard_map/all_to_all | solution.py:746
  197.7 4.4 %collective-permute-start.9 = (bf16[32,32,128]{2,1,0:T(8,128)(2,1)S(1)}, bf16[32,32,128]{2,1,0:T(8,128)(2,1)S(1)}, u32[]{:S(2)}, u32[]{:S(2)}) collective-permute-start(bf16[32,32,128]{2,1,0:T(8,128)(2,1)S(1)} %all-to-all-done.3.x_ref), channel_id=1, source_target_pairs={{0,256},{256,0},{1,257},{257,1},{2,258},{258,2},{3,259},{259,3},{4... | collective-permute-start | bytes 786440 | tf_op jit(solution)/shard_map/ppermute | solution.py:810
  202.1 4.4 %collective-permute-done.7.refs_6_ = bf16[3072,128]{1,0:T(8,128)(2,1)S(1)} collective-permute-done((bf16[3072,128]{1,0:T(8,128)(2,1)}, bf16[3072,128]{1,0:T(8,128)(2,1)S(1)}, u32[]{:S(2)}, u32[]{:S(2)}) %collective-permute-start.7) | collective-permute-done | bytes 786464 | tf_op jit(solution)/shard_map/ppermute | solution.py:780
  206.6 1.6 collective-permute-done.9.x_ref
  208.2 3.4 %experts.3 = bf16[64,2048]{1,0:T(8,128)(2,1)S(1)} custom-call(bf16[32,32,128]{2,1,0:T(8,128)(2,1)S(1)} %collective-permute-done.9.x_ref, bf16[3072,128]{1,0:T(8,128)(2,1)} %copy-done, bf16[3072,128]{1,0:T(8,128)(2,1)} %hand_on.5.refs_1_, bf16[3072,128]{1,0:T(8,128)(2,1)} %hand_on.6.refs_2_, bf16[3072,128]{1,0:T(8,128)(2,1)} %hand_on.7.refs_3_, ...), custom_call_target="tpu_custom_call" | custom-call | tf_op jit(solution)/shard_map/experts/pallas_call | solution.py:682
  211.6 3.1 %collective-permute-start.10 = (bf16[64,2048]{1,0:T(8,128)(2,1)S(1)}, bf16[64,2048]{1,0:T(8,128)(2,1)S(1)}, u32[]{:S(2)}, u32[]{:S(2)}) collective-permute-start(bf16[64,2048]{1,0:T(8,128)(2,1)S(1)} %experts.3), channel_id=1, source_target_pairs={{0,256},{256,0},{1,257},{257,1},{2,258},{258,2},{3,259},{259,3},{4... | collective-permute-start | bytes 786440 | tf_op jit(solution)/shard_map/ppermute | solution.py:812
  214.7 3.4 %experts.2.mine_ref = f32[64,2048]{1,0:T(8,128)S(1)} custom-call(bf16[32,32,128]{2,1,0:T(8,128)(2,1)S(1)} %all-to-all-done.3.x_ref, bf16[3072,128]{1,0:T(8,128)(2,1)} %copy-done, bf16[3072,128]{1,0:T(8,128)(2,1)} %hand_on.5.refs_1_, bf16[3072,128]{1,0:T(8,128)(2,1)} %hand_on.6.refs_2_, bf16[3072,128]{1,0:T(8,128)(2,1)} %hand_on.7.refs_3_, ...), custom_call_target="tpu_custom_call" | custom-call | tf_op jit(solution)/shard_map/experts/pallas_call | solution.py:682
  218.1 1.7 collective-permute-done.10.arrived_ref
  219.8 0.2 finish.1
  220.0 31.8 %all_to_all.27.ret_ref = bf16[32,32,128]{2,1,0:T(8,128)(2,1)S(1)} all-to-all(bf16[32,32,128]{2,1,0:T(8,128)(2,1)S(1)} %finish.1), channel_id=1, replica_groups=mesh['grp'=2,'sp_0'=16,'sp_1'=2,'tp'=8] {'sp_0','sp_1'}, dimensions={0} | all-to-all | bytes 524288 | tf_op jit(solution)/shard_map/all_to_all | solution.py:746
  251.8 1.3 combine.1
  (25 shorter events, 0.1 us)
Async XLA Ops:
  2.2 45.0 %collective-permute-start = (bf16[2,288,512]{2,1,0:T(8,128)(2,1)S(1)}, bf16[2,288,512]{2,1,0:T(8,128)(2,1)S(1)}, u32[]{:S(2)}, u32[]{:S(2)}) collective-permute-start(bf16[2,288,512]{2,1,0:T(8,128)(2,1)S(1)} %get-tuple-element.22.own_ref), channel_id=1, source_target_pairs={{0,8},{8,0},{1,9},{9,1},{2,10},{10,2},{3,11},{11,3},{4,12},{12,4},... | collective-permute-start | bytes 1769480 | tf_op jit(solution)/shard_map/ppermute | solution.py:775
  90.3 17.2 %collective-permute-start.1 = (bf16[16,72,128]{2,1,0:T(8,128)(2,1)S(1)}, bf16[16,72,128]{2,1,0:T(8,128)(2,1)S(1)}, u32[]{:S(2)}, u32[]{:S(2)}) collective-permute-start(bf16[16,72,128]{2,1,0:T(8,128)(2,1)S(1)} %all_to_all.26.own_ref), channel_id=1, source_target_pairs={{0,8},{8,0},{1,9},{9,1},{2,10},{10,2},{3,11},{11,3},{4,12},{12,4},... | collective-permute-start | bytes 884744 | tf_op jit(solution)/shard_map/ppermute | solution.py:799
  100.3 16.5 %copy-start = (bf16[3072,128]{1,0:T(8,128)(2,1)}, bf16[3072,128]{1,0:T(8,128)(2,1)S(1)}, u32[]{:S(2)}) copy-start(bf16[3072,128]{1,0:T(8,128)(2,1)S(1)} %pack_weights.1.refs_0_) | copy-start | bytes 2359300
  100.3 23.4 %collective-permute-start.2 = (bf16[3072,128]{1,0:T(8,128)(2,1)S(1)}, bf16[3072,128]{1,0:T(8,128)(2,1)S(1)}, u32[]{:S(2)}, u32[]{:S(2)}) collective-permute-start(bf16[3072,128]{1,0:T(8,128)(2,1)S(1)} %pack_weights.1.refs_0_), channel_id=1, source_target_pairs={{0,1},{1,2},{2,3},{3,4},{4,5},{5,6},{6,7},{7,0},{8,9},{9,10},{10,1... | collective-permute-start | bytes 2359304 | tf_op jit(solution)/shard_map/ppermute | solution.py:780
  110.6 55.9 %all-to-all-start.2 = ((bf16[8,32,2048]{2,1,0:T(8,128)(2,1)}), bf16[8,32,2048]{2,1,0:T(8,128)(2,1)S(1)}, u32[]{:S(2)}, u32[]{:S(2)}) async-start(bf16[8,32,2048]{2,1,0:T(8,128)(2,1)} %bitcast.2), calls=%async_computation.2 | async-start | bytes 2097152 | tf_op jit(solution)/shard_map/all_to_all | solution.py:746
  116.8 49.1 %copy-start.9 = (s32[32]{0:T(128)S(1)}, s32[32]{0:T(128)}, u32[]{:S(2)}) copy-start(s32[32]{0:T(128)} %param.32) | copy-start | bytes 388
  116.8 49.1 %copy-start.8 = (s32[32,2]{0,1:T(2,128)S(1)}, s32[32,2]{0,1:T(2,128)}, u32[]{:S(2)}) copy-start(s32[32,2]{0,1:T(2,128)} %param.33) | copy-start | bytes 772
  116.8 49.3 %copy-start.7 = (f32[32,2]{0,1:T(2,128)S(1)}, f32[32,2]{0,1:T(2,128)}, u32[]{:S(2)}) copy-start(f32[32,2]{0,1:T(2,128)} %param.34) | copy-start | bytes 772
  116.8 49.7 %copy-start.1 = (bf16[32,2048]{1,0:T(8,128)(2,1)S(1)}, bf16[32,2048]{1,0:T(8,128)(2,1)}, u32[]{:S(2)}) copy-start(bf16[32,2048]{1,0:T(8,128)(2,1)} %res_ref.1) | copy-start | bytes 393220
  116.8 49.7 %copy-start.2 = (f32[2,2048]{1,0:T(2,128)S(1)}, f32[2,2048]{1,0:T(2,128)}, u32[]{:S(2)}) copy-start(f32[2,2048]{1,0:T(2,128)} %gain_ref.3) | copy-start | bytes 49156
  116.8 41.1 %collective-permute-start.3 = (bf16[3072,128]{1,0:T(8,128)(2,1)S(1)}, bf16[3072,128]{1,0:T(8,128)(2,1)S(1)}, u32[]{:S(2)}, u32[]{:S(2)}) collective-permute-start(bf16[3072,128]{1,0:T(8,128)(2,1)S(1)} %pack_weights.1.refs_0_), channel_id=1, source_target_pairs={{0,7},{1,0},{2,1},{3,2},{4,3},{5,4},{6,5},{7,6},{8,15},{9,8},{10,9... | collective-permute-start | bytes 2359304 | tf_op jit(solution)/shard_map/ppermute | solution.py:780
  123.7 0.9 copy-start.4
  124.6 38.4 %collective-permute-start.4 = (bf16[3072,128]{1,0:T(8,128)(2,1)}, bf16[3072,128]{1,0:T(8,128)(2,1)S(1)}, u32[]{:S(2)}, u32[]{:S(2)}) collective-permute-start(bf16[3072,128]{1,0:T(8,128)(2,1)} %hand_on.5.refs_1_), channel_id=1, source_target_pairs={{0,1},{1,2},{2,3},{3,4},{4,5},{5,6},{6,7},{7,0},{8,9},{9,10},{10,1... | collective-permute-start | bytes 2359304 | tf_op jit(solution)/shard_map/ppermute | solution.py:780
  158.0 0.9 copy-start.5
  158.9 19.9 %collective-permute-start.6 = (bf16[3072,128]{1,0:T(8,128)(2,1)}, bf16[3072,128]{1,0:T(8,128)(2,1)S(1)}, u32[]{:S(2)}, u32[]{:S(2)}) collective-permute-start(bf16[3072,128]{1,0:T(8,128)(2,1)} %hand_on.6.refs_2_), channel_id=1, source_target_pairs={{0,7},{1,0},{2,1},{3,2},{4,3},{5,4},{6,5},{7,6},{8,15},{9,8},{10,9... | collective-permute-start | bytes 2359304 | tf_op jit(solution)/shard_map/ppermute | solution.py:780
  163.0 0.9 copy-start.6
  163.9 21.8 %collective-permute-start.5 = (bf16[3072,128]{1,0:T(8,128)(2,1)}, bf16[3072,128]{1,0:T(8,128)(2,1)}, u32[]{:S(2)}, u32[]{:S(2)}) collective-permute-start(bf16[3072,128]{1,0:T(8,128)(2,1)} %hand_on.7.refs_3_), channel_id=1, source_target_pairs={{0,1},{1,2},{2,3},{3,4},{4,5},{5,6},{6,7},{7,0},{8,9},{9,10},{10,1... | collective-permute-start | bytes 2359304 | tf_op jit(solution)/shard_map/ppermute | solution.py:780
  168.0 29.7 %all-to-all-start.3 = ((bf16[32,32,128]{2,1,0:T(8,128)(2,1)}), bf16[32,32,128]{2,1,0:T(8,128)(2,1)S(1)}, u32[]{:S(2)}, u32[]{:S(2)}) async-start(bf16[32,32,128]{2,1,0:T(8,128)(2,1)} %get-tuple-element.26), calls=%async_computation.3 | async-start | bytes 524288 | tf_op jit(solution)/shard_map/all_to_all | solution.py:746
  178.8 0.9 copy-start.3
  179.7 22.5 %collective-permute-start.8 = (bf16[3072,128]{1,0:T(8,128)(2,1)}, bf16[3072,128]{1,0:T(8,128)(2,1)S(1)}, u32[]{:S(2)}, u32[]{:S(2)}) collective-permute-start(bf16[3072,128]{1,0:T(8,128)(2,1)} %hand_on.9.refs_5_), channel_id=1, source_target_pairs={{0,7},{1,0},{2,1},{3,2},{4,3},{5,4},{6,5},{7,6},{8,15},{9,8},{10,9... | collective-permute-start | bytes 2359304 | tf_op jit(solution)/shard_map/ppermute | solution.py:780
  185.7 20.9 %collective-permute-start.7 = (bf16[3072,128]{1,0:T(8,128)(2,1)}, bf16[3072,128]{1,0:T(8,128)(2,1)S(1)}, u32[]{:S(2)}, u32[]{:S(2)}) collective-permute-start(bf16[3072,128]{1,0:T(8,128)(2,1)} %hand_on.8.refs_4_), channel_id=1, source_target_pairs={{0,1},{1,2},{2,3},{3,4},{4,5},{5,6},{6,7},{7,0},{8,9},{9,10},{10,1... | collective-permute-start | bytes 2359304 | tf_op jit(solution)/shard_map/ppermute | solution.py:780
  197.7 10.5 %collective-permute-start.9 = (bf16[32,32,128]{2,1,0:T(8,128)(2,1)S(1)}, bf16[32,32,128]{2,1,0:T(8,128)(2,1)S(1)}, u32[]{:S(2)}, u32[]{:S(2)}) collective-permute-start(bf16[32,32,128]{2,1,0:T(8,128)(2,1)S(1)} %all-to-all-done.3.x_ref), channel_id=1, source_target_pairs={{0,256},{256,0},{1,257},{257,1},{2,258},{258,2},{3,259},{259,3},{4... | collective-permute-start | bytes 786440 | tf_op jit(solution)/shard_map/ppermute | solution.py:810
  211.6 8.2 %collective-permute-start.10 = (bf16[64,2048]{1,0:T(8,128)(2,1)S(1)}, bf16[64,2048]{1,0:T(8,128)(2,1)S(1)}, u32[]{:S(2)}, u32[]{:S(2)}) collective-permute-start(bf16[64,2048]{1,0:T(8,128)(2,1)S(1)} %experts.3), channel_id=1, source_target_pairs={{0,256},{256,0},{1,257},{257,1},{2,258},{258,2},{3,259},{259,3},{4... | collective-permute-start | bytes 786440 | tf_op jit(solution)/shard_map/ppermute | solution.py:812
